TPU v7x, 256 devices: a whole 4x4x8 slice. The times are simulated.
256 devices in a mesh: kv: 32 (over z, x), tp: 8 (over y, core).
Axes of the slice: x: 4, y: 4, z: 8, core: 2. Of those that a mesh axis runs over, the one named last changes fastest.
Arguments:
- tokens: bfloat16 [4096, 2048], P('kv', 'tp'), may hold values from -6 to 6
- states: float32 [4096, 16, 64, 64], P('kv', 'tp'), may hold values from -6 to 6
- mix_gain: bfloat16 [2048], replicated, may hold values from 0.099609375 to 1.8984375
- w_query: bfloat16 [2048, 1024], P(None, 'tp'), may hold values from -0.125 to 0.125
- w_key: bfloat16 [2048, 1024], P(None, 'tp'), may hold values from -0.125 to 0.125
- w_value: bfloat16 [2048, 1024], P(None, 'tp'), may hold values from -0.125 to 0.125
- w_gate: bfloat16 [2048, 1024], P(None, 'tp'), may hold values from -0.125 to 0.125
- head_gain: bfloat16 [1024], P('tp'), may hold values from 0.099609375 to 1.8984375
- w_output: bfloat16 [1024, 2048], P('tp'), may hold values from -0.1875 to 0.1875
- channel_gain: bfloat16 [2048], replicated, may hold values from 0.099609375 to 1.8984375
- w_up: bfloat16 [2048, 8192], P(None, 'kv'), may hold values from -0.125 to 0.125
- w_down: bfloat16 [8192, 2048], P('kv'), may hold values from -0.0625 to 0.0625
Outputs:
- layer_out: bfloat16 [4096, 2048], P('kv', 'tp')
- new_states: float32 [4096, 16, 64, 64], P('kv', 'tp')
All inputs are finite; a program needn't handle non-finite values.
Results may differ from a plain program's by a relative error of at most 0.019.
Values may be sent and summed in bfloat16 or wider, within the bound.
No kernel may reach another device: no remote copies, remote signals or barrier semaphores. Data moves between devices by JAX's collectives and lax.ppermute only.
A program may use at most 64 MiB of HBM per device.

v0:
```python
import jax
import jax.numpy as jnp
from jax import lax
from jax.sharding import Mesh
from jax.sharding import PartitionSpec as P

HEADS = 16
POS = 16384
KV = ("kv_0", "kv_1")


EPSILON = 1e-06
ROTARY_BASE = 10000.0


def in_order(tiles, dim):
    tiles = jnp.moveaxis(tiles, 0, dim)
    dims = tiles.shape
    return tiles.reshape(*dims[:dim], dims[dim] * dims[dim + 1], *dims[dim + 2 :])


def copy_for_each(array, axis):
    count = lax.axis_size(axis)
    return lax.all_to_all(
        jnp.broadcast_to(array[None], (count, *array.shape)), axis, 0, 0, tiled=True
    )


def gathered_copies(array, axis, dim):
    return in_order(copy_for_each(array, axis), dim)


def in_blocks(array, dim, count):
    dims = array.shape
    tiles = array.reshape(*dims[:dim], count, dims[dim] // count, *dims[dim + 1 :])
    return jnp.moveaxis(tiles, dim, 0)


def summed_on_arrival(array, axis, dim):
    count = lax.axis_size(axis)
    tiles = lax.all_to_all(in_blocks(array, dim, count), axis, 0, 0, tiled=True)
    return jnp.sum(tiles.astype(jnp.float32), axis=0)


def gathered_by_axis(array, axes, dim):
    if not axes:
        return array
    nearer = lax.all_gather(array, axes[-1], axis=dim, tiled=True)
    return gathered_by_axis(nearer, axes[:-1], dim)


def rotate(vectors):
    half_size = vectors.shape[-1] // 2
    frequency = ROTARY_BASE ** (-jnp.arange(half_size, dtype=jnp.float32) / half_size)
    angles = POS * frequency
    cosine = jnp.cos(angles)
    sines = jnp.sin(angles)
    first_half = vectors[..., :half_size]
    second = vectors[..., half_size:]
    return jnp.concatenate(
        [first_half * cosine - second * sines, first_half * sines + second * cosine], axis=-1
    )


def retain(normed, states, w_query, w_key, w_value, w_gate, head_gain, head_ids):
    row_count = states.shape[0]
    head_count = states.shape[1]
    head_size = states.shape[2]

    def project(weight):
        return jnp.dot(normed, weight, preferred_element_type=jnp.float32).reshape(
            row_count, head_count, head_size
        )

    queries = rotate(project(w_query)) * head_size ** (-0.5)
    keys_now = rotate(project(w_key))
    values = project(w_value)
    gating = jnp.dot(normed, w_gate, preferred_element_type=jnp.float32)
    decays = 1.0 - jnp.exp2(-1.0 - 11.0 * head_ids / (HEADS - 1))
    new_states = (
        decays[None, :, None, None] * states + keys_now[:, :, :, None] * values[:, :, None, :]
    )
    output = jnp.einsum("bhk,bhkv->bhv", queries, new_states, precision=lax.Precision.HIGHEST)
    center = output - jnp.mean(output, axis=-1, keepdims=True)
    spread = jnp.mean(center * center, axis=-1, keepdims=True)
    scaled = (
        center
        * lax.rsqrt(spread + EPSILON)
        * head_gain.astype(jnp.float32).reshape(head_count, head_size)
    )
    gated_out = (scaled.reshape(row_count, head_count * head_size) * jax.nn.silu(gating)).astype(
        jnp.bfloat16
    )
    return (gated_out, new_states)


def activate(everyone, channel_gain, w_up):
    spread_rows = everyone.astype(jnp.float32)
    second_rms = lax.rsqrt(jnp.mean(spread_rows * spread_rows, axis=1, keepdims=True) + EPSILON)
    scaled = (spread_rows * channel_gain.astype(jnp.float32)).astype(jnp.bfloat16)
    hidden = jnp.dot(scaled, w_up, preferred_element_type=jnp.float32) * second_rms
    return jnp.square(jax.nn.relu(hidden)).astype(jnp.bfloat16)


def local(
    tokens,
    states,
    mix_gain,
    w_query,
    w_key,
    w_value,
    w_gate,
    head_gain,
    w_output,
    channel_gain,
    w_up,
    w_down,
):
    full_rows = gathered_copies(tokens, "tp", 1)
    widened = full_rows.astype(jnp.float32)
    inverse_rms = lax.rsqrt(jnp.mean(widened * widened, axis=1, keepdims=True) + EPSILON)
    normed = (widened * inverse_rms * mix_gain.astype(jnp.float32)).astype(jnp.bfloat16)
    local_heads = states.shape[1]
    tp_index = lax.axis_index("tp")
    head_ids = (tp_index * local_heads + jnp.arange(local_heads)).astype(jnp.float32)
    gated_out, new_states = retain(
        normed, states, w_query, w_key, w_value, w_gate, head_gain, head_ids
    )
    partial_value = jnp.dot(gated_out, w_output, preferred_element_type=jnp.float32)
    attended = summed_on_arrival(partial_value.astype(jnp.bfloat16), "tp", 0)
    share_rows = attended.shape[0]
    own_rows = lax.dynamic_slice_in_dim(full_rows, tp_index * share_rows, share_rows, 0)
    middle = (own_rows.astype(jnp.float32) + attended).astype(jnp.bfloat16)
    everyone = gathered_by_axis(middle, KV, 0)
    activated = activate(everyone, channel_gain, w_up)
    down_sum = summed_on_arrival(
        jnp.dot(activated, w_down, preferred_element_type=jnp.float32).astype(jnp.bfloat16), KV, 0
    )
    finished = (middle.astype(jnp.float32) + down_sum).astype(jnp.bfloat16)
    layer_out = lax.all_to_all(finished, "tp", split_axis=1, concat_axis=0, tiled=True)
    return (layer_out, new_states)


def solution(mesh):
    torus = Mesh(mesh.devices.reshape(8, 4, mesh.shape["tp"]), ("kv_0", "kv_1", "tp"))
    in_specs = (
        P(KV, "tp"),
        P(KV, "tp", None, None),
        P(),
        P(None, "tp"),
        P(None, "tp"),
        P(None, "tp"),
        P(None, "tp"),
        P("tp"),
        P("tp", None),
        P(),
        P(None, KV),
        P(KV, None),
    )
    out_specs = (P(KV, "tp"), P(KV, "tp", None, None))
    return jax.shard_map(local, mesh=torus, in_specs=in_specs, out_specs=out_specs, check_vma=False)
```

profile of v0, /device:TPU:1, one launch (start us, length us, event | category | flops | bytes accessed | tf_op | source)
XLA Modules:
  0.0 178.3 jit_solution(15148791007178584661)
XLA Ops:
  7.2 1.8 broadcast_in_dim.2
  8.9 6.6 %all-to-all-start = ((bf16[8,128,256]{2,1,0:T(8,128)(2,1)}), bf16[8,128,256]{2,1,0:T(8,128)(2,1)S(1)}, u32[]{:S(2)}, u32[]{:S(2)}) async-start(bf16[8,128,256]{2,1,0:T(8,128)(2,1)} %broadcast_in_dim.2), calls=%async_computation | async-start | bytes 1048576 | tf_op jit(solution)/shard_map/all_to_all | solution.py:24
  15.5 0.7 mul.214
  16.2 0.7 convert_element_type.71
  16.9 0.7 reshape.120
  17.6 2.0 %copy.43 = bf16[2048,128]{0,1:T(8,128)(2,1)} copy(bf16[2048,128]{1,0:T(8,128)(2,1)} %param.15) | data formatting | bytes 1048576 | tf_op args[3]
  19.7 1.2 copy.45
  20.9 1.2 copy.47
  22.3 2.6 %all-to-all-done = bf16[8,128,256]{2,1,0:T(8,128)(2,1)S(1)} async-done(((bf16[8,128,256]{2,1,0:T(8,128)(2,1)}), bf16[8,128,256]{2,1,0:T(8,128)(2,1)S(1)}, u32[]{:S(2)}, u32[]{:S(2)}) %all-to-all-start) | async-done | bytes 524320 | tf_op jit(solution)/shard_map/all_to_all | solution.py:24
  24.9 0.3 copy.41
  25.2 0.3 fusion.19
  25.5 0.3 fusion.21
  25.8 1.7 fusion.32
  27.5 0.3 fusion.33
  27.8 0.3 fusion.34
  28.1 0.1 multiply_subtract_fusion
  28.2 3.1 %multiply_reduce_fusion = (f32[128,2,64]{0,2,1:T(8,128)S(1)}, f32[128,2,64,64]{0,3,2,1:T(8,128)}) fusion(f32[128,2,64]{0,2,1:T(8,128)S(1)} %get-tuple-element.10, f32[128,2,64]{0,2,1:T(8,128)S(1)} %fusion.34, f32[128,2,64]{0,2,1:T(8,128)S(1)} %get-tuple-element.11, f32[128,2,64,64]{0,3,2,1:T(8,128)S(1)} %copy-done.1, f32[2]{0:T(128)S(1)} %exponential_subtract_fusion), kind=kLoop, calls=%fused_computation.4 | loop fusion | flops 5226496 | bytes 8650760 | tf_op jit(solution)/shard_map/bhk,bhkv->bhv/dot_general | solution.py:83
  31.5 0.1 multiply_multiply_fusion
  31.6 0.1 copy.49
  31.7 1.7 convolution_convert_fusion.1
  33.4 4.3 %all-to-all-start.1 = ((bf16[8,16,2048]{2,1,0:T(8,128)(2,1)}), bf16[8,16,2048]{2,1,0:T(8,128)(2,1)S(1)}, u32[]{:S(2)}, u32[]{:S(2)}) async-start(bf16[8,16,2048]{2,1,0:T(8,128)(2,1)} %bitcast.14), calls=%async_computation.1 | async-start | bytes 1048576 | tf_op jit(solution)/shard_map/all_to_all | solution.py:41
  37.7 0.2 constant_dynamic-slice_fusion
  37.9 0.2 copy.62
  38.1 9.0 %all-to-all-done.1 = bf16[8,16,2048]{2,1,0:T(8,128)(2,1)S(1)} async-done(((bf16[8,16,2048]{2,1,0:T(8,128)(2,1)}), bf16[8,16,2048]{2,1,0:T(8,128)(2,1)S(1)}, u32[]{:S(2)}, u32[]{:S(2)}) %all-to-all-start.1) | async-done | bytes 524320 | tf_op jit(solution)/shard_map/all_to_all | solution.py:41
  47.2 10.7 %all_gather.6 = bf16[64,2048]{1,0:T(8,128)(2,1)} all-gather(bf16[16,2048]{1,0:T(8,128)(2,1)S(1)} %add_convert_fusion.1), channel_id=1, replica_groups=mesh['kv_0'=8,'kv_1'=4,'tp'=8] {'kv_1'}, dimensions={0}, use_global_device_ids=true | all-gather | bytes 327680 | tf_op jit(solution)/shard_map/all_gather | solution.py:48
  57.9 39.5 %all-gather.2.cloned.1.call-done = bf16[512,2048]{1,0:T(8,128)(2,1)} async-done(((bf16[64,2048]{1,0:T(8,128)(2,1)}), bf16[512,2048]{1,0:T(8,128)(2,1)}) %all-gather.2.cloned.1.call-update) | async-done | bytes 2097168 | tf_op jit(solution)/shard_map/all_gather | solution.py:48
  97.4 2.1 %fusion.1 = f32[512]{0:T(512)S(1)} fusion(bf16[512,2048]{1,0:T(8,128)(2,1)} %all-gather.2.cloned.1.call-done), kind=kLoop, calls=%fused_computation.3 | loop fusion | flops 3145216 | bytes 2099200 | tf_op jit(solution)/shard_map/reduce_sum | solution.py:99
  99.5 4.2 %convolution_convert_fusion = bf16[512,2048]{1,0:T(8,128)(2,1)S(1)} fusion(bf16[256,2048]{1,0:T(8,128)(2,1)S(1)} %copy-done, bf16[2048,256]{1,0:T(8,128)(2,1)} %param.22, bf16[512,2048]{1,0:T(8,128)(2,1)} %all-gather.2.cloned.1.call-done, f32[2048]{0:T(1024)S(1)} %convert_element_type.83, f32[512]{0:T(512)S(1)} %add_rsqrt_fusion), kind=kOutput, calls=%fused_computation.7 | convolution fusion | flops 1078460416 | bytes 6301696 | tf_op jit(solution)/shard_map/dot_general | solution.py:137
  103.7 50.8 %all_to_all.34 = bf16[32,16,2048]{2,1,0:T(8,128)(2,1)S(1)} all-to-all(bf16[32,16,2048]{2,1,0:T(8,128)(2,1)S(1)} %bitcast.44), channel_id=1, replica_groups=mesh['kv_0'=8,'kv_1'=4,'tp'=8] {'kv_0','kv_1'}, dimensions={0} | all-to-all | bytes 4194304 | tf_op jit(solution)/shard_map/all_to_all | solution.py:41
  154.4 0.3 convert_reduce_fusion
  154.8 16.1 %all_to_all.35 = bf16[16,8,256]{2,0,1:T(8,128)(2,1)S(1)} all-to-all(bf16[16,8,256]{2,0,1:T(8,128)(2,1)S(1)} %bitcast.50), channel_id=1, replica_groups=mesh['kv_0'=8,'kv_1'=4,'tp'=8] {'tp'}, dimensions={1} | all-to-all | bytes 131072 | tf_op jit(solution)/shard_map/all_to_all | solution.py:140
  170.9 0.6 copy.68
  (27 shorter events, 0.4 us)
Async XLA Ops:
  7.2 92.3 %copy-start = (bf16[256,2048]{1,0:T(8,128)(2,1)S(1)}, bf16[256,2048]{1,0:T(8,128)(2,1)}, u32[]{:S(2)}) copy-start(bf16[256,2048]{1,0:T(8,128)(2,1)} %param.23) | copy-start | bytes 3145732
  8.9 16.0 %all-to-all-start = ((bf16[8,128,256]{2,1,0:T(8,128)(2,1)}), bf16[8,128,256]{2,1,0:T(8,128)(2,1)S(1)}, u32[]{:S(2)}, u32[]{:S(2)}) async-start(bf16[8,128,256]{2,1,0:T(8,128)(2,1)} %broadcast_in_dim.2), calls=%async_computation | async-start | bytes 1048576 | tf_op jit(solution)/shard_map/all_to_all | solution.py:24
  25.2 3.0 %copy-start.1 = (f32[128,2,64,64]{0,3,2,1:T(8,128)S(1)}, f32[128,2,64,64]{0,3,2,1:T(8,128)}, u32[]{:S(2)}) copy-start(f32[128,2,64,64]{0,3,2,1:T(8,128)} %param.13) | copy-start | bytes 12582916
  28.2 3.4 %copy-start.2 = (bf16[128,2048]{1,0:T(8,128)(2,1)S(1)}, bf16[128,2048]{1,0:T(8,128)(2,1)}, u32[]{:S(2)}) copy-start(bf16[128,2048]{1,0:T(8,128)(2,1)} %param.20) | copy-start | bytes 1572868
  28.2 3.4 %copy-start.3 = (bf16[2048,128]{1,0:T(8,128)(2,1)S(1)}, bf16[2048,128]{1,0:T(8,128)(2,1)}, u32[]{:S(2)}) copy-start(bf16[2048,128]{1,0:T(8,128)(2,1)} %param.18) | copy-start | bytes 1572868
  31.4 26.5 %copy-start.4 = (bf16[2048]{0:T(1024)(128)(2,1)S(1)}, bf16[2048]{0:T(1024)(128)(2,1)}, u32[]{:S(2)}) copy-start(bf16[2048]{0:T(1024)(128)(2,1)} %param.21) | copy-start | bytes 12292
  33.4 13.7 %all-to-all-start.1 = ((bf16[8,16,2048]{2,1,0:T(8,128)(2,1)}), bf16[8,16,2048]{2,1,0:T(8,128)(2,1)S(1)}, u32[]{:S(2)}, u32[]{:S(2)}) async-start(bf16[8,16,2048]{2,1,0:T(8,128)(2,1)} %bitcast.14), calls=%async_computation.1 | async-start | bytes 1048576 | tf_op jit(solution)/shard_map/all_to_all | solution.py:41
  37.7 59.7 %all-gather.2.cloned.1.call-start = ((), (), s32[]{:S(2)}) async-start(), calls=%async_computation.4 | async-start | bytes 2359296 | tf_op jit(solution)/shard_map/all_gather | solution.py:48
Sparse Core Ops, SparseCore 0:
  58.0 39.3 all-gather.1
where the time goes:
time: 179 us; the launch traced here: 178 us
  blocking collectives  77.5 us (43%)
  waiting for transfers between devices  51 us (28%)
  between operations  14.2 us (8%)
  starting transfers between devices  10.9 us (6%)
  local copies, waits for them, and re-layouts  9.14 us (5%)
  matrix products  8.12 us (5%)
  other arithmetic  7.33 us (4%)
    all_to_all x1, blocking collectives, summed_on_arrival(): tiles = lax.all_to_all(in_blocks(array, dim, count), axis, 0, 0, tiled=True)  50.8 us
    all_gather x1, waiting for transfers between devices, gathered_by_axis(): nearer = lax.all_gather(array, axes[-1], axis=dim, tiled=True)  39.5 us
    all_to_all x1, blocking collectives, local(): lax.all_to_all(finished, 'tp', split_axis=1, concat_axis=0, tiled=True)  16.1 us
    all_gather x1, blocking collectives, gathered_by_axis(): nearer = lax.all_gather(array, axes[-1], axis=dim, tiled=True)  10.7 us
    all_to_all x1, waiting for transfers between devices, summed_on_arrival(): tiles = lax.all_to_all(in_blocks(array, dim, count), axis, 0, 0, tiled=True)  8.98 us
    all_to_all x1, starting transfers between devices, copy_for_each(): lax.all_to_all(jnp.broadcast_to(array[None], (count, *array.shape)), axis...  6.6 us
    unnamed x15, local copies, waits for them, and re-layouts  5.38 us
    all_to_all x1, starting transfers between devices, summed_on_arrival(): tiles = lax.all_to_all(in_blocks(array, dim, count), axis, 0, 0, tiled=True)  4.34 us
  transfers between devices with their start and end apart: 3, of which 3 were waited for; matrix products, arithmetic and copies ran while one was open for 4% of the time, Pallas kernels for 0%

commit v1 on v0

v1 whole, which is shorter than its diff:
```python
import jax
import jax.numpy as jnp
from jax import lax
from jax.experimental import pallas as pl
from jax.experimental.pallas import tpu as pltpu
from jax.sharding import Mesh
from jax.sharding import PartitionSpec as P

HEADS = 16
HEAD = 64
POS = 16384
D = 2048
EPSILON = 1e-06
ROTARY_BASE = 10000.0
ROWS = 128
Z, X, Y, C = 8, 4, 4, 2
TP = Y * C
SHARE = ROWS // TP
F32 = jnp.float32
BF16 = jnp.bfloat16


def copy_all(copies):
    for copy in copies:
        copy.start()
    for copy in copies:
        copy.wait()


def pack_kernel(up, down, packed, sems):
    at = pl.multiple_of(lax.axis_index("c") * 128, 128)
    copies = [
        pltpu.make_async_copy(
            up.at[pl.ds(8 * i, 8), :, pl.ds(at, 128)],
            packed.at[pl.ds(0, 8), :, pl.ds(128 * i, 128)],
            sems.at[i],
        )
        for i in range(2)
    ]
    copies += [
        pltpu.make_async_copy(
            down.at[pl.ds(at, 128), pl.ds(256 * j, 256)], packed.at[8 + j], sems.at[2 + j]
        )
        for j in range(8)
    ]
    copy_all(copies)


def pack(w_up, w_down):
    return pl.pallas_call(
        pack_kernel,
        out_shape=jax.ShapeDtypeStruct((16, 128, 256), BF16),
        in_specs=[pl.BlockSpec(memory_space=pl.ANY)] * 2,
        out_specs=pl.BlockSpec(memory_space=pl.ANY),
        scratch_shapes=[pltpu.SemaphoreType.DMA((10,))],
        name="pack",
    )(w_up.reshape(16, 128, 256), w_down)


CHUNKS = 8
PER_HEAD = CHUNKS // 2
STEP = HEAD // PER_HEAD


def retain_kernel(
    decays, tokens, states, wq, wk, wv, wg, mix_gain, head_gain, cosine, sines,
    new_states, gated, weights, old, new, qt, kt, ret, w_sems, in_sems, out_sems,
):
    def part(ref, i):
        return ref.at[i // PER_HEAD, pl.ds((i % PER_HEAD) * STEP, STEP)]

    w_copies = [
        pltpu.make_async_copy(w, weights.at[:, pl.ds(128 * i, 128)], w_sems.at[i])
        for i, w in enumerate((wq, wk, wv, wg))
    ]
    in_copies = [
        pltpu.make_async_copy(part(states, i), part(old, i), in_sems.at[i]) for i in range(CHUNKS)
    ]
    out_copies = [
        pltpu.make_async_copy(part(new, i), part(new_states, i), out_sems.at[i])
        for i in range(CHUNKS)
    ]
    for copy in w_copies + in_copies:
        copy.start()

    squares = jnp.zeros((ROWS, 256), F32)
    for j in range(TP):
        block = tokens[j].astype(F32)
        squares += block * block
    inverse_rms = lax.rsqrt(jnp.sum(squares, axis=1, keepdims=True) / D + EPSILON)
    normed = [
        (tokens[j].astype(F32) * inverse_rms * mix_gain[:, 256 * j : 256 * j + 256].astype(F32))
        .astype(BF16)
        for j in range(TP)
    ]
    for copy in w_copies:
        copy.wait()
    projected = jnp.zeros((ROWS, 512), F32)
    for j in range(TP):
        projected += jnp.dot(
            normed[j], weights[256 * j : 256 * j + 256, :], preferred_element_type=F32
        )
    half = HEAD // 2

    def turned(flat):
        rows = []
        for h in range(2):
            a = flat[h * HEAD : h * HEAD + half]
            b = flat[h * HEAD + half : (h + 1) * HEAD]
            rows += [a * cosine[...] - b * sines[...], a * sines[...] + b * cosine[...]]
        return jnp.concatenate(rows, axis=0)

    qt[...] = turned(projected[:, 0:128].T) * HEAD**-0.5
    kt[...] = turned(projected[:, 128:256].T)
    vt = projected[:, 256:384].T
    gating = projected[:, 384:512]

    for h in range(2):
        values = vt[h * HEAD : (h + 1) * HEAD]
        decay = decays[h]
        total = jnp.zeros((HEAD, ROWS), F32)
        for i in range(h * PER_HEAD, (h + 1) * PER_HEAD):
            in_copies[i].wait()
            first = (i % PER_HEAD) * STEP

            def step(s, total):
                k = first + s
                row = h * HEAD + k
                fresh = decay * old[h, k] + kt[pl.ds(row, 1), :] * values
                new[h, k] = fresh
                return total + qt[pl.ds(row, 1), :] * fresh

            total = lax.fori_loop(0, STEP, step, total, unroll=8)
            out_copies[i].start()
        center = total - jnp.mean(total, axis=0, keepdims=True)
        spread = jnp.mean(center * center, axis=0, keepdims=True)
        ret[h * HEAD : (h + 1) * HEAD, :] = center * lax.rsqrt(spread + EPSILON)

    out = (ret[...].T * head_gain[...].astype(F32) * (gating * jax.nn.sigmoid(gating))).astype(BF16)
    out = out.reshape(TP, SHARE, 128)
    for z in range(Z):
        gated[z] = out
    for copy in out_copies:
        copy.wait()


def retain(tokens, states, wq, wk, wv, wg, mix_gain, head_gain, decays, cosine, sines):
    any_space = pl.BlockSpec(memory_space=pl.ANY)
    vmem = pl.BlockSpec(memory_space=pltpu.VMEM)
    return pl.pallas_call(
        retain_kernel,
        out_shape=(
            jax.ShapeDtypeStruct((2, HEAD, HEAD, ROWS), F32),
            jax.ShapeDtypeStruct((Z, TP, SHARE, 128), BF16),
        ),
        in_specs=[pl.BlockSpec(memory_space=pltpu.SMEM), vmem] + [any_space] * 5 + [vmem] * 4,
        out_specs=(any_space, vmem),
        scratch_shapes=[
            pltpu.VMEM((D, 512), BF16),
            pltpu.VMEM((2, HEAD, HEAD, ROWS), F32),
            pltpu.VMEM((2, HEAD, HEAD, ROWS), F32),
            pltpu.VMEM((128, ROWS), F32),
            pltpu.VMEM((128, ROWS), F32),
            pltpu.VMEM((128, ROWS), F32),
            pltpu.SemaphoreType.DMA((4,)),
            pltpu.SemaphoreType.DMA((CHUNKS,)),
            pltpu.SemaphoreType.DMA((CHUNKS,)),
        ],
        compiler_params=pltpu.CompilerParams(vmem_limit_bytes=40 * 2**20),
        name="retain",
    )(decays, tokens, states, wq, wk, wv, wg, mix_gain, head_gain, cosine, sines)


def mixer_kernel(*refs):
    gated, tokens, channel_gain, own_up, own_down = refs[:5]
    outs_mine, outs_other, packs = refs[5:9], refs[9], refs[10:16]
    out, heads, w_out, up, down, sems, o_sems = refs[16:]
    core = lax.axis_index("c")
    y = lax.axis_index("y")
    copies = []
    for k in range(Y):
        from_y = lax.rem(y + (Y - k), Y)
        copies.append(
            pltpu.make_async_copy(outs_mine[k], w_out.at[2 * from_y + core], o_sems.at[2 * k])
        )
        copies.append(
            pltpu.make_async_copy(
                outs_other.at[k], w_out.at[2 * from_y + (1 - core)], o_sems.at[2 * k + 1]
            )
        )
    up_copies = [pltpu.make_async_copy(own_up, up.at[:, :, pl.ds(0, 256)], sems.at[0])]
    down_copies = [
        pltpu.make_async_copy(
            own_down.at[:, pl.ds(256 * j, 256)], down.at[j, pl.ds(0, 256)], sems.at[1 + j]
        )
        for j in range(8)
    ]
    for p, packed in enumerate(packs):
        at = 256 + 128 * p
        for i in range(2):
            up_copies.append(
                pltpu.make_async_copy(
                    packed.at[pl.ds(0, 8), :, pl.ds(128 * i, 128)],
                    up.at[pl.ds(8 * i, 8), :, pl.ds(at, 128)],
                    sems.at[9 + 3 * p + i],
                )
            )
        down_copies.append(
            pltpu.make_async_copy(
                packed.at[pl.ds(8, 8)], down.at[:, pl.ds(at, 128), :], sems.at[9 + 3 * p + 2]
            )
        )
    for copy in copies + up_copies + down_copies:
        copy.start()
    for z in range(Z):
        for t in range(TP):
            heads[SHARE * z : SHARE * (z + 1), 128 * t : 128 * (t + 1)] = gated[z, t]
    for copy in copies:
        copy.wait()
    squares = jnp.zeros((ROWS, 256), F32)
    middle = []
    scaled = []
    for j in range(TP):
        at = slice(256 * j, 256 * j + 256)
        attended = jnp.dot(
            heads[...], w_out[:, :, at].reshape(1024, 256), preferred_element_type=F32
        )
        rounded = (tokens[:, j].reshape(ROWS, 256).astype(F32) + attended).astype(BF16)
        wide = rounded.astype(F32)
        squares += wide * wide
        middle.append(rounded)
        scaled.append((wide * channel_gain[:, at].astype(F32)).astype(BF16))
    second_rms = lax.rsqrt(jnp.sum(squares, axis=1, keepdims=True) / D + EPSILON)
    scaled = jnp.concatenate(scaled, axis=1)
    for copy in up_copies:
        copy.wait()
    activated = []
    for n in range(4):
        hidden = second_rms * jnp.dot(
            scaled,
            up[:, :, 256 * n : 256 * n + 256].reshape(D, 256),
            preferred_element_type=F32,
        )
        activated.append(jnp.square(jax.nn.relu(hidden)).astype(BF16))
    activated = jnp.concatenate(activated, axis=1)
    for copy in down_copies:
        copy.wait()
    row = lax.broadcasted_iota(jnp.int32, (ROWS, 1), 0)
    mine = row // SHARE == lax.axis_index("z")
    for j in range(TP):
        part = jnp.dot(activated, down[j], preferred_element_type=F32)
        part = part + jnp.where(mine, middle[j].astype(F32), 0.0)
        out[:, j] = part.astype(BF16).reshape(Z, SHARE, 256)


def mixer(gated, tokens, channel_gain, own_up, own_down, outs_mine, outs_other, packs):
    any_space = pl.BlockSpec(memory_space=pl.ANY)
    vmem = pl.BlockSpec(memory_space=pltpu.VMEM)
    return pl.pallas_call(
        mixer_kernel,
        out_shape=jax.ShapeDtypeStruct((Z, TP, SHARE, 256), BF16),
        in_specs=[vmem] * 3 + [any_space] * 13,
        out_specs=vmem,
        scratch_shapes=[
            pltpu.VMEM((ROWS, 1024), BF16),
            pltpu.VMEM((TP, 128, D), BF16),
            pltpu.VMEM((16, 128, 1024), BF16),
            pltpu.VMEM((8, 1024, 256), BF16),
            pltpu.SemaphoreType.DMA((27,)),
            pltpu.SemaphoreType.DMA((8,)),
        ],
        compiler_params=pltpu.CompilerParams(vmem_limit_bytes=40 * 2**20),
        name="mixer",
    )(gated, tokens, channel_gain, own_up.reshape(16, 128, 256), own_down,
      *outs_mine, outs_other, *packs)


def shift(count, by):
    return [(i, (i + by) % count) for i in range(count)]


def to_all(array, axes):
    return lax.all_to_all(array, axes, 0, 0, tiled=True)


def local(
    tokens, states, mix_gain, w_query, w_key, w_value, w_gate, head_gain, w_output,
    channel_gain, w_up, w_down,
):
    tp_index = lax.axis_index("y") * C + lax.axis_index("c")
    rows = to_all(jnp.broadcast_to(tokens[None], (TP, ROWS, 256)), ("y", "c"))
    packed = pack(w_up, w_down)
    near = [lax.ppermute(packed, "x", shift(X, by)) for by in (1, 3, 2)]
    outs = [w_output] + [lax.ppermute(w_output, "y", shift(Y, by)) for by in (1, 2, 3)]
    column = to_all(
        jnp.broadcast_to(
            tokens.reshape(1, TP, SHARE, 256), (Z, TP, SHARE, 256)
        ).reshape(Z * TP, SHARE, 256),
        ("z", "y", "c"),
    ).reshape(Z, TP, SHARE, 256)
    half = HEAD // 2
    frequency = ROTARY_BASE ** (-jnp.arange(half, dtype=F32) / half)
    angles = POS * frequency
    cosine = jnp.broadcast_to(jnp.cos(angles)[:, None], (half, ROWS))
    sines = jnp.broadcast_to(jnp.sin(angles)[:, None], (half, ROWS))
    head_ids = (tp_index * 2 + jnp.arange(2)).astype(F32)
    decays = 1.0 - jnp.exp2(-1.0 - 11.0 * head_ids / (HEADS - 1))
    new_states, gated = retain(
        rows, states.transpose(1, 2, 3, 0), w_query, w_key, w_value, w_gate,
        mix_gain.reshape(1, D), head_gain.reshape(1, 128), decays, cosine, sines,
    )
    gated = to_all(gated.reshape(Z * TP, SHARE, 128), ("z", "y", "c"))
    swap = [(0, 1), (1, 0)]
    outs_other = lax.ppermute(jnp.stack(outs), "c", swap)
    far = [lax.ppermute(p, "c", swap) for p in near]
    down = mixer(
        gated.reshape(Z, TP, SHARE, 128), column, channel_gain.reshape(1, D), w_up, w_down,
        outs, outs_other, near + far,
    )
    down = to_all(down.reshape(Z * TP, SHARE, 256), ("z", "y", "c"))
    layer_out = jnp.sum(down.reshape(Z, ROWS, 256).astype(F32), axis=0).astype(BF16)
    return (layer_out, new_states.transpose(3, 0, 1, 2))


def solution(mesh):
    torus = Mesh(mesh.devices.reshape(Z, X, Y, C), ("z", "x", "y", "c"))
    kv, tp = ("z", "x"), ("y", "c")
    in_specs = (
        P(kv, tp), P(kv, tp, None, None), P(), P(None, tp), P(None, tp), P(None, tp), P(None, tp),
        P(tp), P(tp, None), P(), P(None, kv), P(kv, None),
    )
    out_specs = (P(kv, tp), P(kv, tp, None, None))
    return jax.shard_map(local, mesh=torus, in_specs=in_specs, out_specs=out_specs, check_vma=False)
```

time: 179 us -> 150 us (0.84)
  blocking collectives: 77.5 us -> 23.2 us
  Pallas kernels: 0 us -> 42.4 us
  starting transfers between devices: 10.9 us -> 40 us
  waiting for transfers between devices: 51 us -> 31.5 us
  between operations: 14.2 us -> 0.9 us
  matrix products: 8.12 us -> 0 us
  other arithmetic: 7.33 us -> 2.4 us
    all_to_all x2 -> x1, blocking collectives: 66.9 us -> 23.2 us  [to_all(): return lax.all_to_all(array, axes, 0, 0, tiled=True)]
    pallas_call x0 -> x3, Pallas kernels: none -> 42.4 us  [the longest x1 33 us: pack(): pl.pallas_call(pack_kernel, out_shape=jax.ShapeDtypeStruct((16, 128, 256)...]
    all_gather x1 -> x0, waiting for transfers between devices: 39.5 us -> none  [gathered_by_axis(): nearer = lax.all_gather(array, axes[-1], axis=dim, tiled=True)]
    ppermute x0 -> x10, starting transfers between devices: none -> 21 us  [the longest x3 8.44 us: local(): far = [lax.ppermute(p, 'c', swap) for p in near]]
    all_to_all x2 -> x3, waiting for transfers between devices: 11.6 us -> 31.5 us  [to_all(): return lax.all_to_all(array, axes, 0, 0, tiled=True)]
    all_gather x1 -> x0, blocking collectives: 10.7 us -> none  [gathered_by_axis(): nearer = lax.all_gather(array, axes[-1], axis=dim, tiled=True)]
    dot_general x5 -> x0, matrix products: 8.12 us -> none  [the longest x1 4.16 us: local(): jnp.dot(activated, w_down, preferred_element_type=jnp.float32)]
    all_to_all x2 -> x3, starting transfers between devices: 10.9 us -> 18.9 us  [to_all(): return lax.all_to_all(array, axes, 0, 0, tiled=True)]
  transfers between devices with their start and end apart: 3 -> 13, of which waited for: 3 -> 3; matrix products, arithmetic and copies ran while one was open for 4% -> 2% of each run, Pallas kernels for 0% -> 25%
where the time goes in v1:
time: 150 us
  Pallas kernels  42.4 us (28%)
  starting transfers between devices  40 us (27%)
  waiting for transfers between devices  31.5 us (21%)
  blocking collectives  23.2 us (15%)
  local copies, waits for them, and re-layouts  9.3 us (6%)
  other arithmetic  2.4 us (2%)
    pallas_call x1, Pallas kernels, pack(): pl.pallas_call(pack_kernel, out_shape=jax.ShapeDtypeStruct((16, 128, 256)...  33 us
    all_to_all x3, waiting for transfers between devices, to_all(): return lax.all_to_all(array, axes, 0, 0, tiled=True)  31.5 us
    all_to_all x1, blocking collectives, to_all(): return lax.all_to_all(array, axes, 0, 0, tiled=True)  23.2 us
    all_to_all x3, starting transfers between devices, to_all(): return lax.all_to_all(array, axes, 0, 0, tiled=True)  18.9 us
    ppermute x3, starting transfers between devices, local(): far = [lax.ppermute(p, 'c', swap) for p in near]  8.44 us
    unnamed x36, local copies, waits for them, and re-layouts  7.45 us
    ppermute x3, starting transfers between devices, local(): lax.ppermute(w_output, 'y', shift(Y, by))  5.88 us
    pallas_call x1, Pallas kernels, retain(): pl.pallas_call(retain_kernel, out_shape=(jax.ShapeDtypeStruct((2, HEAD, H...  4.93 us
  transfers between devices with their start and end apart: 13, of which 3 were waited for; matrix products, arithmetic and copies ran while one was open for 2% of the time, Pallas kernels for 25%

profile of v1, /device:TPU:1, one launch (start us, length us, event | category | flops | bytes accessed | tf_op | source)
XLA Modules:
  0.0 149.7 jit_solution(121149943947870980)
XLA Ops:
  0.6 2.2 %collective-permute-start = (bf16[128,2048]{1,0:T(8,128)(2,1)}, bf16[128,2048]{1,0:T(8,128)(2,1)S(1)}, u32[]{:S(2)}, u32[]{:S(2)}) collective-permute-start(bf16[128,2048]{1,0:T(8,128)(2,1)} %refs_5_.1), channel_id=1, source_target_pairs={{0,2},{2,4},{4,6},{6,0},{1,3},{3,5},{5,7},{7,1},{8,10},{10,12},{12... | collective-permute-start | bytes 1572872 | tf_op jit(solution)/shard_map/ppermute | solution.py:294
  2.8 2.6 %collective-permute-start.1 = (bf16[128,2048]{1,0:T(8,128)(2,1)}, bf16[128,2048]{1,0:T(8,128)(2,1)S(1)}, u32[]{:S(2)}, u32[]{:S(2)}) collective-permute-start(bf16[128,2048]{1,0:T(8,128)(2,1)} %refs_5_.1), channel_id=1, source_target_pairs={{0,4},{2,6},{4,0},{6,2},{1,5},{3,7},{5,1},{7,3},{8,12},{10,14},{12... | collective-permute-start | bytes 1572872 | tf_op jit(solution)/shard_map/ppermute | solution.py:294
  5.5 1.1 collective-permute-start.2
  6.5 33.0 %pack.1 = bf16[16,128,256]{2,1,0:T(8,128)(2,1)} custom-call(bf16[16,128,256]{2,1,0:T(8,128)(2,1)} %bitcast.17, bf16[256,2048]{1,0:T(8,128)(2,1)} %refs_4_.1), custom_call_target="tpu_custom_call" | custom-call | tf_op jit(solution)/shard_map/pack/pallas_call | solution.py:50
  39.5 1.3 collective-permute-start.4
  40.8 1.5 collective-permute-start.5
  42.2 1.5 %collective-permute-start.6 = (bf16[16,128,256]{2,1,0:T(8,128)(2,1)}, bf16[16,128,256]{2,1,0:T(8,128)(2,1)}, u32[]{:S(2)}, u32[]{:S(2)}) collective-permute-start(bf16[16,128,256]{2,1,0:T(8,128)(2,1)} %pack.1), channel_id=1, source_target_pairs={{0,16},{8,24},{16,0},{24,8},{1,17},{9,25},{17,1},{25,9},{2,18},{10... | collective-permute-start | bytes 3145736 | tf_op jit(solution)/shard_map/ppermute | solution.py:293
  43.9 1.6 %pad_maximum_fusion = bf16[4,128,2048]{2,1,0:T(8,128)(2,1)} fusion(bf16[1,128,2048]{2,1,0:T(8,128)(2,1)S(1)} %bitcast.25, bf16[1,128,2048]{2,1,0:T(8,128)(2,1)S(1)} %bitcast.24, bf16[1,128,2048]{2,1,0:T(8,128)(2,1)S(1)} %bitcast.23, bf16[1,128,2048]{2,1,0:T(8,128)(2,1)S(1)} %bitcast.22), kind=kLoop, calls=%fused_computation | loop fusion | flops 3145728 | bytes 4194304 | tf_op jit(solution)/shard_map/stack | solution.py:314
  45.5 2.4 %collective-permute-start.3 = (bf16[4,128,2048]{2,1,0:T(8,128)(2,1)}, bf16[4,128,2048]{2,1,0:T(8,128)(2,1)}, u32[]{:S(2)}, u32[]{:S(2)}) collective-permute-start(bf16[4,128,2048]{2,1,0:T(8,128)(2,1)} %pad_maximum_fusion), channel_id=1, source_target_pairs={{0,1},{1,0},{2,3},{3,2},{4,5},{5,4},{6,7},{7,6},{8,9},{9,8},{10,11... | collective-permute-start | bytes 6291464 | tf_op jit(solution)/shard_map/ppermute | solution.py:314
  47.9 0.8 broadcast_in_dim.10
  48.7 3.4 %all-to-all-start = ((bf16[8,128,256]{2,1,0:T(8,128)(2,1)}), bf16[8,128,256]{2,1,0:T(8,128)(2,1)S(1)}, u32[]{:S(2)}, u32[]{:S(2)}) async-start(bf16[8,128,256]{2,1,0:T(8,128)(2,1)} %broadcast_in_dim.10), calls=%async_computation | async-start | bytes 1048576 | tf_op jit(solution)/shard_map/all_to_all | solution.py:283
  52.3 9.2 %all-to-all-done.tokens = bf16[8,128,256]{2,1,0:T(8,128)(2,1)S(1)} async-done(((bf16[8,128,256]{2,1,0:T(8,128)(2,1)}), bf16[8,128,256]{2,1,0:T(8,128)(2,1)S(1)}, u32[]{:S(2)}, u32[]{:S(2)}) %all-to-all-start) | async-done | bytes 524320 | tf_op jit(solution)/shard_map/all_to_all | solution.py:283
  61.5 0.1 broadcast_in_dim.11.cosine
  61.6 0.1 broadcast_in_dim.12.sines
  61.7 2.2 %copy-done.2 = f32[128,2,64,64]{0,3,2,1:T(8,128)S(1)} copy-done((f32[128,2,64,64]{0,3,2,1:T(8,128)S(1)}, f32[128,2,64,64]{0,3,2,1:T(8,128)}, u32[]{:S(2)}) %copy-start.2) | copy-done | bytes 4194328
  63.9 1.0 copy-done.12
  64.9 1.0 copy-done.13
  66.0 4.9 %retain.1 = (f32[2,64,64,128]{3,2,1,0:T(8,128)}, bf16[8,8,16,128]{3,2,1,0:T(8,128)(2,1)}) custom-call(f32[2]{0:T(128)S(1)} %exponential_subtract_fusion.decays, bf16[8,128,256]{2,1,0:T(8,128)(2,1)S(1)} %all-to-all-done.tokens, f32[2,64,64,128]{3,2,1,0:T(8,128)S(1)} %bitcast.19, bf16[2048,128]{1,0:T(8,128)(2,1)S(1)} %copy-done.10, ...), custom_call_target="tpu_custom_call" | custom-call | tf_op jit(solution)/shard_map/retain/pallas_call | solution.py:150
  70.9 10.7 %all-to-all-start.1 = ((bf16[64,16,128]{2,1,0:T(8,128)(2,1)}), bf16[64,16,128]{2,1,0:T(8,128)(2,1)S(1)}, u32[]{:S(2)}, u32[]{:S(2)}) async-start(bf16[64,16,128]{2,1,0:T(8,128)(2,1)} %bitcast.2), calls=%async_computation.1 | async-start | bytes 524288 | tf_op jit(solution)/shard_map/all_to_all | solution.py:283
  81.7 0.5 collective-permute-start.7
  82.2 6.2 %collective-permute-start.8 = (bf16[16,128,256]{2,1,0:T(8,128)(2,1)}, bf16[16,128,256]{2,1,0:T(8,128)(2,1)}, u32[]{:S(2)}, u32[]{:S(2)}) collective-permute-start(bf16[16,128,256]{2,1,0:T(8,128)(2,1)} %collective-permute-done.5.refs_11_), channel_id=1, source_target_pairs={{0,1},{1,0},{2,3},{3,2},{4,5},{5,4},{6,7},{7,6},{8,9},{9,8},{10,11... | collective-permute-start | bytes 3145736 | tf_op jit(solution)/shard_map/ppermute | solution.py:315
  88.4 1.7 %collective-permute-start.9 = (bf16[16,128,256]{2,1,0:T(8,128)(2,1)}, bf16[16,128,256]{2,1,0:T(8,128)(2,1)}, u32[]{:S(2)}, u32[]{:S(2)}) collective-permute-start(bf16[16,128,256]{2,1,0:T(8,128)(2,1)} %collective-permute-done.6.refs_12_), channel_id=1, source_target_pairs={{0,1},{1,0},{2,3},{3,2},{4,5},{5,4},{6,7},{7,6},{8,9},{9,8},{10,11... | collective-permute-start | bytes 3145736 | tf_op jit(solution)/shard_map/ppermute | solution.py:315
  90.1 4.6 %all-to-all-done.1 = bf16[64,16,128]{2,1,0:T(8,128)(2,1)S(1)} async-done(((bf16[64,16,128]{2,1,0:T(8,128)(2,1)}), bf16[64,16,128]{2,1,0:T(8,128)(2,1)S(1)}, u32[]{:S(2)}, u32[]{:S(2)}) %all-to-all-start.1) | async-done | bytes 262176 | tf_op jit(solution)/shard_map/all_to_all | solution.py:283
  94.7 0.9 broadcast_in_dim.14
  95.6 4.8 %all-to-all-start.2 = ((bf16[64,16,256]{2,1,0:T(8,128)(2,1)}), bf16[64,16,256]{2,1,0:T(8,128)(2,1)S(1)}, u32[]{:S(2)}, u32[]{:S(2)}) async-start(bf16[64,16,256]{2,1,0:T(8,128)(2,1)} %bitcast.28), calls=%async_computation.2 | async-start | bytes 1048576 | tf_op jit(solution)/shard_map/all_to_all | solution.py:283
  100.4 17.7 %all-to-all-done.2 = bf16[64,16,256]{2,1,0:T(8,128)(2,1)S(1)} async-done(((bf16[64,16,256]{2,1,0:T(8,128)(2,1)}), bf16[64,16,256]{2,1,0:T(8,128)(2,1)S(1)}, u32[]{:S(2)}, u32[]{:S(2)}) %all-to-all-start.2) | async-done | bytes 524320 | tf_op jit(solution)/shard_map/all_to_all | solution.py:283
  118.1 1.0 copy-done.5
  119.2 1.0 copy-done.7
  120.2 1.0 copy-done.9
  121.2 4.5 %mixer.1 = bf16[8,8,16,256]{3,2,1,0:T(8,128)(2,1)S(1)} custom-call(bf16[8,8,16,128]{3,2,1,0:T(8,128)(2,1)S(1)} %bitcast.26, bf16[8,8,16,256]{3,2,1,0:T(8,128)(2,1)S(1)} %bitcast.20, bf16[1,2048]{1,0:T(2,128)(2,1)S(1)} %reshape.55.refs_2_, bf16[16,128,256]{2,1,0:T(8,128)(2,1)S(1)} %bitcast.18, bf16[256,2048]{1,0:T(8,128)(2,1)S(1)} %copy-done.1, ...), custom_call_target="tpu_custom_call" | custom-call | tf_op jit(solution)/shard_map/mixer/pallas_call | solution.py:259
  125.8 23.2 %all_to_all.20 = bf16[64,16,256]{2,1,0:T(8,128)(2,1)S(1)} all-to-all(bf16[64,16,256]{2,1,0:T(8,128)(2,1)S(1)} %bitcast.21), channel_id=1, replica_groups=mesh['z'=8,'x'=4,'y'=4,'c'=2] {'z','y','c'}, dimensions={0} | all-to-all | bytes 1048576 | tf_op jit(solution)/shard_map/all_to_all | solution.py:283
  149.0 0.7 bitcast_reduce_fusion
  (45 shorter events, 0.2 us)
Async XLA Ops:
  0.6 43.2 %copy-start.3 = (bf16[128,2048]{1,0:T(8,128)(2,1)S(1)}, bf16[128,2048]{1,0:T(8,128)(2,1)}, u32[]{:S(2)}) copy-start(bf16[128,2048]{1,0:T(8,128)(2,1)} %refs_5_.1) | copy-start | bytes 1572868
  0.6 41.6 %collective-permute-start = (bf16[128,2048]{1,0:T(8,128)(2,1)}, bf16[128,2048]{1,0:T(8,128)(2,1)S(1)}, u32[]{:S(2)}, u32[]{:S(2)}) collective-permute-start(bf16[128,2048]{1,0:T(8,128)(2,1)} %refs_5_.1), channel_id=1, source_target_pairs={{0,2},{2,4},{4,6},{6,0},{1,3},{3,5},{5,7},{7,1},{8,10},{10,12},{12... | collective-permute-start | bytes 1572872 | tf_op jit(solution)/shard_map/ppermute | solution.py:294
  2.8 40.9 %collective-permute-start.1 = (bf16[128,2048]{1,0:T(8,128)(2,1)}, bf16[128,2048]{1,0:T(8,128)(2,1)S(1)}, u32[]{:S(2)}, u32[]{:S(2)}) collective-permute-start(bf16[128,2048]{1,0:T(8,128)(2,1)} %refs_5_.1), channel_id=1, source_target_pairs={{0,4},{2,6},{4,0},{6,2},{1,5},{3,7},{5,1},{7,3},{8,12},{10,14},{12... | collective-permute-start | bytes 1572872 | tf_op jit(solution)/shard_map/ppermute | solution.py:294
  5.5 38.3 %collective-permute-start.2 = (bf16[128,2048]{1,0:T(8,128)(2,1)}, bf16[128,2048]{1,0:T(8,128)(2,1)S(1)}, u32[]{:S(2)}, u32[]{:S(2)}) collective-permute-start(bf16[128,2048]{1,0:T(8,128)(2,1)} %refs_5_.1), channel_id=1, source_target_pairs={{0,6},{2,0},{4,2},{6,4},{1,7},{3,1},{5,3},{7,5},{8,14},{10,8},{12,... | collective-permute-start | bytes 1572872 | tf_op jit(solution)/shard_map/ppermute | solution.py:294
  39.5 42.2 %collective-permute-start.4 = (bf16[16,128,256]{2,1,0:T(8,128)(2,1)}, bf16[16,128,256]{2,1,0:T(8,128)(2,1)}, u32[]{:S(2)}, u32[]{:S(2)}) collective-permute-start(bf16[16,128,256]{2,1,0:T(8,128)(2,1)} %pack.1), channel_id=1, source_target_pairs={{0,8},{8,16},{16,24},{24,0},{1,9},{9,17},{17,25},{25,1},{2,10},{10... | collective-permute-start | bytes 3145736 | tf_op jit(solution)/shard_map/ppermute | solution.py:293
  40.8 41.4 %collective-permute-start.5 = (bf16[16,128,256]{2,1,0:T(8,128)(2,1)}, bf16[16,128,256]{2,1,0:T(8,128)(2,1)}, u32[]{:S(2)}, u32[]{:S(2)}) collective-permute-start(bf16[16,128,256]{2,1,0:T(8,128)(2,1)} %pack.1), channel_id=1, source_target_pairs={{0,24},{8,0},{16,8},{24,16},{1,25},{9,1},{17,9},{25,17},{2,26},{10... | collective-permute-start | bytes 3145736 | tf_op jit(solution)/shard_map/ppermute | solution.py:293
  42.2 3.2 %copy-start.4 = (bf16[128,2048]{1,0:T(8,128)(2,1)}, bf16[128,2048]{1,0:T(8,128)(2,1)S(1)}, u32[]{:S(2)}) copy-start(bf16[128,2048]{1,0:T(8,128)(2,1)S(1)} %collective-permute-done.refs_6_) | copy-start | bytes 1572868
  42.2 46.2 %collective-permute-start.6 = (bf16[16,128,256]{2,1,0:T(8,128)(2,1)}, bf16[16,128,256]{2,1,0:T(8,128)(2,1)}, u32[]{:S(2)}, u32[]{:S(2)}) collective-permute-start(bf16[16,128,256]{2,1,0:T(8,128)(2,1)} %pack.1), channel_id=1, source_target_pairs={{0,16},{8,24},{16,0},{24,8},{1,17},{9,25},{17,1},{25,9},{2,18},{10... | collective-permute-start | bytes 3145736 | tf_op jit(solution)/shard_map/ppermute | solution.py:293
  43.8 1.7 %copy-start.6 = (bf16[128,2048]{1,0:T(8,128)(2,1)}, bf16[128,2048]{1,0:T(8,128)(2,1)S(1)}, u32[]{:S(2)}) copy-start(bf16[128,2048]{1,0:T(8,128)(2,1)S(1)} %collective-permute-done.1.refs_7_) | copy-start | bytes 1572868
  43.8 1.7 %copy-start.8 = (bf16[128,2048]{1,0:T(8,128)(2,1)}, bf16[128,2048]{1,0:T(8,128)(2,1)S(1)}, u32[]{:S(2)}) copy-start(bf16[128,2048]{1,0:T(8,128)(2,1)S(1)} %collective-permute-done.2.refs_8_) | copy-start | bytes 1572868
  43.8 4.1 %copy-start.15 = (bf16[128,256]{1,0:T(8,128)(2,1)S(1)}, bf16[128,256]{1,0:T(8,128)(2,1)}, u32[]{:S(2)}) copy-start(bf16[128,256]{1,0:T(8,128)(2,1)} %param.12) | copy-start | bytes 196612
  43.8 8.4 %copy-start.16 = (bf16[2048]{0:T(1024)(128)(2,1)S(1)}, bf16[2048]{0:T(1024)(128)(2,1)}, u32[]{:S(2)}) copy-start(bf16[2048]{0:T(1024)(128)(2,1)} %param.14) | copy-start | bytes 12292
  43.8 17.8 %copy-start.10 = (bf16[2048,128]{1,0:T(8,128)(2,1)S(1)}, bf16[2048,128]{1,0:T(8,128)(2,1)}, u32[]{:S(2)}) copy-start(bf16[2048,128]{1,0:T(8,128)(2,1)} %wq.1) | copy-start | bytes 1572868
  43.8 17.8 %copy-start.11 = (bf16[2048,128]{1,0:T(8,128)(2,1)S(1)}, bf16[2048,128]{1,0:T(8,128)(2,1)}, u32[]{:S(2)}) copy-start(bf16[2048,128]{1,0:T(8,128)(2,1)} %wk.1) | copy-start | bytes 1572868
  43.9 17.8 %copy-start.14 = (bf16[128]{0:T(256)(128)(2,1)S(1)}, bf16[128]{0:T(256)(128)(2,1)}, u32[]{:S(2)}) copy-start(bf16[128]{0:T(256)(128)(2,1)} %param.19) | copy-start | bytes 772
  45.5 72.6 %collective-permute-start.3 = (bf16[4,128,2048]{2,1,0:T(8,128)(2,1)}, bf16[4,128,2048]{2,1,0:T(8,128)(2,1)}, u32[]{:S(2)}, u32[]{:S(2)}) collective-permute-start(bf16[4,128,2048]{2,1,0:T(8,128)(2,1)} %pad_maximum_fusion), channel_id=1, source_target_pairs={{0,1},{1,0},{2,3},{3,2},{4,5},{5,4},{6,7},{7,6},{8,9},{9,8},{10,11... | collective-permute-start | bytes 6291464 | tf_op jit(solution)/shard_map/ppermute | solution.py:314
  48.7 12.8 %all-to-all-start = ((bf16[8,128,256]{2,1,0:T(8,128)(2,1)}), bf16[8,128,256]{2,1,0:T(8,128)(2,1)S(1)}, u32[]{:S(2)}, u32[]{:S(2)}) async-start(bf16[8,128,256]{2,1,0:T(8,128)(2,1)} %broadcast_in_dim.10), calls=%async_computation | async-start | bytes 1048576 | tf_op jit(solution)/shard_map/all_to_all | solution.py:283
  61.7 2.2 %copy-start.2 = (f32[128,2,64,64]{0,3,2,1:T(8,128)S(1)}, f32[128,2,64,64]{0,3,2,1:T(8,128)}, u32[]{:S(2)}) copy-start(f32[128,2,64,64]{0,3,2,1:T(8,128)} %param.13) | copy-start | bytes 12582916
  63.9 1.0 copy-start.12
  64.9 1.0 copy-start.13
  70.9 29.5 %copy-start.17 = (bf16[2048]{0:T(1024)(128)(2,1)S(1)}, bf16[2048]{0:T(1024)(128)(2,1)}, u32[]{:S(2)}) copy-start(bf16[2048]{0:T(1024)(128)(2,1)} %param.21) | copy-start | bytes 12292
  70.9 47.2 %copy-start = (bf16[2048,256]{1,0:T(8,128)(2,1)S(1)}, bf16[2048,256]{1,0:T(8,128)(2,1)}, u32[]{:S(2)}) copy-start(bf16[2048,256]{1,0:T(8,128)(2,1)} %param.22) | copy-start | bytes 3145732
  70.9 47.2 %copy-start.1 = (bf16[256,2048]{1,0:T(8,128)(2,1)S(1)}, bf16[256,2048]{1,0:T(8,128)(2,1)}, u32[]{:S(2)}) copy-start(bf16[256,2048]{1,0:T(8,128)(2,1)} %refs_4_.1) | copy-start | bytes 3145732
  70.9 23.8 %all-to-all-start.1 = ((bf16[64,16,128]{2,1,0:T(8,128)(2,1)}), bf16[64,16,128]{2,1,0:T(8,128)(2,1)S(1)}, u32[]{:S(2)}, u32[]{:S(2)}) async-start(bf16[64,16,128]{2,1,0:T(8,128)(2,1)} %bitcast.2), calls=%async_computation.1 | async-start | bytes 524288 | tf_op jit(solution)/shard_map/all_to_all | solution.py:283
  81.7 36.4 %collective-permute-start.7 = (bf16[16,128,256]{2,1,0:T(8,128)(2,1)}, bf16[16,128,256]{2,1,0:T(8,128)(2,1)}, u32[]{:S(2)}, u32[]{:S(2)}) collective-permute-start(bf16[16,128,256]{2,1,0:T(8,128)(2,1)} %collective-permute-done.4.refs_10_), channel_id=1, source_target_pairs={{0,1},{1,0},{2,3},{3,2},{4,5},{5,4},{6,7},{7,6},{8,9},{9,8},{10,11... | collective-permute-start | bytes 3145736 | tf_op jit(solution)/shard_map/ppermute | solution.py:315
  82.2 35.9 %collective-permute-start.8 = (bf16[16,128,256]{2,1,0:T(8,128)(2,1)}, bf16[16,128,256]{2,1,0:T(8,128)(2,1)}, u32[]{:S(2)}, u32[]{:S(2)}) collective-permute-start(bf16[16,128,256]{2,1,0:T(8,128)(2,1)} %collective-permute-done.5.refs_11_), channel_id=1, source_target_pairs={{0,1},{1,0},{2,3},{3,2},{4,5},{5,4},{6,7},{7,6},{8,9},{9,8},{10,11... | collective-permute-start | bytes 3145736 | tf_op jit(solution)/shard_map/ppermute | solution.py:315
  88.4 29.7 %collective-permute-start.9 = (bf16[16,128,256]{2,1,0:T(8,128)(2,1)}, bf16[16,128,256]{2,1,0:T(8,128)(2,1)}, u32[]{:S(2)}, u32[]{:S(2)}) collective-permute-start(bf16[16,128,256]{2,1,0:T(8,128)(2,1)} %collective-permute-done.6.refs_12_), channel_id=1, source_target_pairs={{0,1},{1,0},{2,3},{3,2},{4,5},{5,4},{6,7},{7,6},{8,9},{9,8},{10,11... | collective-permute-start | bytes 3145736 | tf_op jit(solution)/shard_map/ppermute | solution.py:315
  95.6 22.5 %all-to-all-start.2 = ((bf16[64,16,256]{2,1,0:T(8,128)(2,1)}), bf16[64,16,256]{2,1,0:T(8,128)(2,1)S(1)}, u32[]{:S(2)}, u32[]{:S(2)}) async-start(bf16[64,16,256]{2,1,0:T(8,128)(2,1)} %bitcast.28), calls=%async_computation.2 | async-start | bytes 1048576 | tf_op jit(solution)/shard_map/all_to_all | solution.py:283
  118.1 1.0 copy-start.5
  119.2 1.0 copy-start.7
  120.2 1.0 copy-start.9

commit v2 on v1

v2 whole, which is shorter than its diff:
```python
import jax
import jax.numpy as jnp
import numpy as np
from jax import lax
from jax.experimental import pallas as pl
from jax.experimental.pallas import tpu as pltpu
from jax.sharding import Mesh
from jax.sharding import PartitionSpec as P


HEADS = 16
HEAD = 64
POS = 16384
D = 2048
EPSILON = 1e-06
ROTARY_BASE = 10000.0
ROWS = 128
Z, X, Y, C = 8, 4, 4, 2
TP = Y * C
SHARE = ROWS // TP
RETAIN_LIMIT = 58 * 2**20
MIXER_LIMIT = 40 * 2**20
F32 = jnp.float32
BF16 = jnp.bfloat16


def copy_all(copies):
    for copy in copies:
        copy.start()
    for copy in copies:
        copy.wait()


def pack_kernel(up, down, packed, sems):
    at = pl.multiple_of(lax.axis_index("c") * 128, 128)
    copies = [
        pltpu.make_async_copy(
            up.at[pl.ds(8 * i, 8), :, pl.ds(at, 128)],
            packed.at[pl.ds(0, 8), :, pl.ds(128 * i, 128)],
            sems.at[i],
        )
        for i in range(2)
    ]
    copies += [
        pltpu.make_async_copy(
            down.at[pl.ds(at, 128), pl.ds(256 * j, 256)], packed.at[8 + j], sems.at[2 + j]
        )
        for j in range(8)
    ]
    copy_all(copies)


def pack(w_up, w_down):
    return pl.pallas_call(
        pack_kernel,
        out_shape=jax.ShapeDtypeStruct((16, 128, 256), BF16),
        in_specs=[pl.BlockSpec(memory_space=pltpu.HBM)] * 2,
        out_specs=pl.BlockSpec(memory_space=pltpu.VMEM),
        scratch_shapes=[pltpu.SemaphoreType.DMA((10,))],
        name="pack",
    )(w_up.reshape(16, 128, 256), w_down)


CHUNKS = 8
PER_HEAD = CHUNKS // 2
STEP = HEAD // PER_HEAD
ANGLES = POS * ROTARY_BASE ** (-np.arange(HEAD // 2) / (HEAD // 2))
COSINE = np.broadcast_to(np.cos(ANGLES)[:, None], (HEAD // 2, ROWS)).astype(np.float32)
SINES = np.broadcast_to(np.sin(ANGLES)[:, None], (HEAD // 2, ROWS)).astype(np.float32)
DECAYS = (1.0 - 2.0 ** (-1.0 - 11.0 * np.arange(HEADS) / (HEADS - 1))).astype(np.float32)


def gain_row(gain, j):
    wide = gain[...].astype(F32)
    return jnp.concatenate([wide[2 * j : 2 * j + 1], wide[2 * j + 1 : 2 * j + 2]], axis=1)


def retain_kernel(
    decays, tokens, states, wq, wk, wv, wg, wo, mix_gain, head_gain, cosine, sines,
    new_states, partial, weights, w_out, old, new, qt, kt, ret, w_sems, in_sems, out_sems,
):
    def part(ref, i):
        return ref.at[i // PER_HEAD, pl.ds((i % PER_HEAD) * STEP, STEP)]

    first_head = 2 * (lax.axis_index("y") * C + lax.axis_index("c"))
    w_copies = [
        pltpu.make_async_copy(w, weights.at[:, pl.ds(128 * i, 128)], w_sems.at[i])
        for i, w in enumerate((wq, wk, wv, wg))
    ]
    wo_copy = pltpu.make_async_copy(wo, w_out, w_sems.at[4])
    in_copies = [
        pltpu.make_async_copy(part(states, i), part(old, i), in_sems.at[i]) for i in range(CHUNKS)
    ]
    out_copies = [
        pltpu.make_async_copy(part(new, i), part(new_states, i), out_sems.at[i])
        for i in range(CHUNKS)
    ]
    for copy in w_copies + in_copies + [wo_copy]:
        copy.start()

    squares = jnp.zeros((ROWS, 256), F32)
    for j in range(TP):
        block = tokens[j].astype(F32)
        squares += block * block
    inverse_rms = lax.rsqrt(jnp.sum(squares, axis=1, keepdims=True) / D + EPSILON)
    normed = jnp.concatenate(
        [
            (tokens[j].astype(F32) * inverse_rms * gain_row(mix_gain, j)).astype(BF16)
            for j in range(TP)
        ],
        axis=1,
    )
    for copy in w_copies:
        copy.wait()
    projected = jnp.dot(normed, weights[...], preferred_element_type=F32)
    half = HEAD // 2

    def turned(flat):
        rows = []
        for h in range(2):
            a = flat[h * HEAD : h * HEAD + half]
            b = flat[h * HEAD + half : (h + 1) * HEAD]
            rows += [a * cosine[...] - b * sines[...], a * sines[...] + b * cosine[...]]
        return jnp.concatenate(rows, axis=0)

    qt[...] = turned(projected[:, 0:128].T) * HEAD**-0.5
    kt[...] = turned(projected[:, 128:256].T)
    vt = projected[:, 256:384].T
    gating = projected[:, 384:512]

    for h in range(2):
        values = vt[h * HEAD : (h + 1) * HEAD]
        decay = decays[first_head + h]
        total = jnp.zeros((HEAD, ROWS), F32)
        for i in range(h * PER_HEAD, (h + 1) * PER_HEAD):
            in_copies[i].wait()
            first = (i % PER_HEAD) * STEP

            def step(s, total):
                k = first + s
                row = h * HEAD + k
                fresh = decay * old[h, k] + kt[pl.ds(row, 1), :] * values
                new[h, k] = fresh
                return total + qt[pl.ds(row, 1), :] * fresh

            total = lax.fori_loop(0, STEP, step, total, unroll=8)
            out_copies[i].start()
        center = total - jnp.mean(total, axis=0, keepdims=True)
        spread = jnp.mean(center * center, axis=0, keepdims=True)
        ret[h * HEAD : (h + 1) * HEAD, :] = center * lax.rsqrt(spread + EPSILON)

    out = (ret[...].T * head_gain[...].astype(F32) * (gating * jax.nn.sigmoid(gating))).astype(BF16)
    wo_copy.wait()
    partial[...] = (
        jnp.dot(out, w_out[...], preferred_element_type=F32).astype(BF16).reshape(TP, SHARE, D)
    )
    for copy in out_copies:
        copy.wait()


def retain(tokens, states, wq, wk, wv, wg, wo, mix_gain, head_gain):
    any_space = pl.BlockSpec(memory_space=pl.ANY)
    vmem = pl.BlockSpec(memory_space=pltpu.VMEM)
    return pl.pallas_call(
        retain_kernel,
        out_shape=(
            jax.ShapeDtypeStruct((2, HEAD, HEAD, ROWS), F32),
            jax.ShapeDtypeStruct((TP, SHARE, D), BF16),
        ),
        in_specs=[pl.BlockSpec(memory_space=pltpu.SMEM), vmem] + [any_space] * 6 + [vmem] * 4,
        out_specs=(any_space, vmem),
        scratch_shapes=[
            pltpu.VMEM((D, 512), BF16),
            pltpu.VMEM((128, D), BF16),
            pltpu.VMEM((2, HEAD, HEAD, ROWS), F32),
            pltpu.VMEM((2, HEAD, HEAD, ROWS), F32),
            pltpu.VMEM((128, ROWS), F32),
            pltpu.VMEM((128, ROWS), F32),
            pltpu.VMEM((128, ROWS), F32),
            pltpu.SemaphoreType.DMA((5,)),
            pltpu.SemaphoreType.DMA((CHUNKS,)),
            pltpu.SemaphoreType.DMA((CHUNKS,)),
        ],
        compiler_params=pltpu.CompilerParams(vmem_limit_bytes=RETAIN_LIMIT),
        name="retain",
    )(
        DECAYS, tokens, states, wq, wk, wv, wg, wo, mix_gain.reshape(16, 128),
        head_gain.reshape(1, 128), COSINE, SINES,
    )


def middle_kernel(parts, tokens, out):
    at = pl.multiple_of((lax.axis_index("y") * C + lax.axis_index("c")) * SHARE, SHARE)
    total = parts[0].astype(F32)
    for t in range(1, TP):
        total += parts[t].astype(F32)
    own = jnp.concatenate([tokens[j, pl.ds(at, SHARE), :] for j in range(TP)], axis=1)
    middle = (own.astype(F32) + total).astype(BF16)
    for z in range(Z):
        out[z] = middle


def middle_rows(parts, tokens):
    vmem = pl.BlockSpec(memory_space=pltpu.VMEM)
    return pl.pallas_call(
        middle_kernel,
        out_shape=jax.ShapeDtypeStruct((Z, SHARE, D), BF16),
        in_specs=[vmem] * 2,
        out_specs=vmem,
        compiler_params=pltpu.CompilerParams(vmem_limit_bytes=8 * 2**20),
        name="middle",
    )(parts, tokens)


def mixer_kernel(*refs):
    rows, channel_gain, own_up, own_down = refs[:4]
    ups, downs = refs[4:10], refs[10:16]
    out, up, down, sems = refs[16:]
    up_copies = [pltpu.make_async_copy(own_up, up.at[:, :, pl.ds(0, 256)], sems.at[0])]
    down_copies = [
        pltpu.make_async_copy(
            own_down.at[:, pl.ds(256 * j, 256)], down.at[j, pl.ds(0, 256)], sems.at[1 + j]
        )
        for j in range(8)
    ]
    for p in range(6):
        at = 256 + 128 * p
        for i in range(2):
            up_copies.append(
                pltpu.make_async_copy(
                    ups[p].at[pl.ds(0, 8), :, pl.ds(128 * i, 128)],
                    up.at[pl.ds(8 * i, 8), :, pl.ds(at, 128)],
                    sems.at[9 + 3 * p + i],
                )
            )
        last = downs[p].shape[0] - 8
        down_copies.append(
            pltpu.make_async_copy(
                downs[p].at[pl.ds(last, 8)], down.at[:, pl.ds(at, 128), :], sems.at[9 + 3 * p + 2]
            )
        )
    for copy in up_copies + down_copies:
        copy.start()
    squares = jnp.zeros((ROWS, 256), F32)
    scaled = []
    for j in range(TP):
        wide = rows[:, :, 256 * j : 256 * j + 256].reshape(ROWS, 256).astype(F32)
        squares += wide * wide
        scaled.append((wide * gain_row(channel_gain, j)).astype(BF16))
    second_rms = lax.rsqrt(jnp.sum(squares, axis=1, keepdims=True) / D + EPSILON)
    scaled = jnp.concatenate(scaled, axis=1)
    activated = []
    for n in range(4):
        for copy in up_copies[0:1] if n == 0 else up_copies[4 * n - 3 : 4 * n + 1]:
            copy.wait()
        hidden = second_rms * jnp.dot(
            scaled,
            up[:, :, 256 * n : 256 * n + 256].reshape(D, 256),
            preferred_element_type=F32,
        )
        activated.append(jnp.square(jax.nn.relu(hidden)).astype(BF16))
    activated = jnp.concatenate(activated, axis=1)
    for copy in down_copies:
        copy.wait()
    row = lax.broadcasted_iota(jnp.int32, (ROWS, 1), 0)
    mine = row // SHARE == lax.axis_index("z")
    for j in range(TP):
        part = jnp.dot(activated, down[j], preferred_element_type=F32)
        own = rows[:, :, 256 * j : 256 * j + 256].reshape(ROWS, 256).astype(F32)
        part = part + jnp.where(mine, own, 0.0)
        out[:, j] = part.astype(BF16).reshape(Z, SHARE, 256)


def mixer(rows, channel_gain, own_up, own_down, ups, downs):
    any_space = pl.BlockSpec(memory_space=pl.ANY)
    vmem = pl.BlockSpec(memory_space=pltpu.VMEM)
    return pl.pallas_call(
        mixer_kernel,
        out_shape=jax.ShapeDtypeStruct((Z, TP, SHARE, 256), BF16),
        in_specs=[vmem] * 2 + [any_space] * 14,
        out_specs=vmem,
        scratch_shapes=[
            pltpu.VMEM((16, 128, 1024), BF16),
            pltpu.VMEM((8, 1024, 256), BF16),
            pltpu.SemaphoreType.DMA((27,)),
        ],
        compiler_params=pltpu.CompilerParams(vmem_limit_bytes=MIXER_LIMIT),
        name="mixer",
    )(rows, channel_gain.reshape(16, 128), own_up.reshape(16, 128, 256), own_down, *ups, *downs)


def shift(count, by):
    return [(i, (i + by) % count) for i in range(count)]


def to_all(array, axes):
    return lax.all_to_all(array, axes, 0, 0, tiled=True)


def local(
    tokens, states, mix_gain, w_query, w_key, w_value, w_gate, head_gain, w_output,
    channel_gain, w_up, w_down,
):
    rows = to_all(jnp.broadcast_to(tokens[None], (TP, ROWS, 256)), ("y", "c"))
    packed = pack(w_up, w_down)
    left = lax.ppermute(packed, "x", shift(X, 1))
    right = lax.ppermute(packed, "x", shift(X, 3))
    new_states, partial = retain(
        rows, states.transpose(1, 2, 3, 0), w_query, w_key, w_value, w_gate, w_output,
        mix_gain, head_gain,
    )
    parts = to_all(partial, ("y", "c"))
    far_up = lax.ppermute(left[:8], "x", shift(X, 1))
    far_down = lax.ppermute(right[8:], "x", shift(X, 3))
    middle = middle_rows(parts, rows)
    everyone = to_all(middle, "z")
    swap = [(0, 1), (1, 0)]
    left_other = lax.ppermute(left, "c", swap)
    right_other = lax.ppermute(right, "c", swap)
    up_other = lax.ppermute(far_up, "c", swap)
    down_other = lax.ppermute(far_down, "c", swap)
    down = mixer(
        everyone, channel_gain, w_up, w_down,
        (left, left_other, right, right_other, far_up, up_other),
        (left, left_other, right, right_other, far_down, down_other),
    )
    down = to_all(down.reshape(Z * TP, SHARE, 256), ("z", "y", "c"))
    layer_out = jnp.sum(down.reshape(Z, ROWS, 256).astype(F32), axis=0).astype(BF16)
    return (layer_out, new_states.transpose(3, 0, 1, 2))


def solution(mesh):
    torus = Mesh(mesh.devices.reshape(Z, X, Y, C), ("z", "x", "y", "c"))
    kv, tp = ("z", "x"), ("y", "c")
    in_specs = (
        P(kv, tp), P(kv, tp, None, None), P(), P(None, tp), P(None, tp), P(None, tp), P(None, tp),
        P(tp), P(tp, None), P(), P(None, kv), P(kv, None),
    )
    out_specs = (P(kv, tp), P(kv, tp, None, None))
    return jax.shard_map(local, mesh=torus, in_specs=in_specs, out_specs=out_specs, check_vma=False)
```

time: 150 us -> 99.4 us (0.66)
  Pallas kernels: 42.4 us -> 13.3 us
  starting transfers between devices: 40 us -> 20.3 us
  blocking collectives: 23.2 us -> 37.9 us
  waiting for transfers between devices: 31.5 us -> 20.1 us
  local copies, waits for them, and re-layouts: 9.3 us -> 5.79 us
  other arithmetic: 2.4 us -> 0.7 us
    pallas_call x1, Pallas kernels: 33 us -> 2.23 us  [pack(): pl.pallas_call(pack_kernel, out_shape=jax.ShapeDtypeStruct((16, 128, 256)...]
    all_to_all x1 -> x2, blocking collectives: 23.2 us -> 37.9 us  [to_all(): return lax.all_to_all(array, axes, 0, 0, tiled=True)]
    ppermute x10 -> x8, starting transfers between devices: 21 us -> 8.09 us  [the longest x1 2.67 us: local(): far_down = lax.ppermute(right[8:], 'x', shift(X, 3))]
    all_to_all x3 -> x2, waiting for transfers between devices: 31.5 us -> 20.1 us  [to_all(): return lax.all_to_all(array, axes, 0, 0, tiled=True)]
    all_to_all x3 -> x2, starting transfers between devices: 18.9 us -> 12.2 us  [to_all(): return lax.all_to_all(array, axes, 0, 0, tiled=True)]
    unnamed x36 -> x10, local copies, waits for them, and re-layouts: 7.45 us -> 3.24 us
    pallas_call x1, Pallas kernels: 4.93 us -> 7.24 us  [retain(): pl.pallas_call(retain_kernel, out_shape=(jax.ShapeDtypeStruct((2, HEAD, H...]
    slice x0 -> x2, local copies, waits for them, and re-layouts: none -> 1.67 us  [the longest x1 0.84 us: local(): far_down = lax.ppermute(right[8:], 'x', shift(X, 3))]
  transfers between devices with their start and end apart: 13 -> 10, of which waited for: 3 -> 2; matrix products, arithmetic and copies ran while one was open for 2% -> 3% of each run, Pallas kernels for 25% -> 7%
where the time goes in v2:
time: 99.4 us; the launch traced here: 98.9 us
  blocking collectives  37.9 us (38%)
  starting transfers between devices  20.3 us (20%)
  waiting for transfers between devices  20.1 us (20%)
  Pallas kernels  13.3 us (13%)
  local copies, waits for them, and re-layouts  5.79 us (6%)
    all_to_all x2, blocking collectives, to_all(): return lax.all_to_all(array, axes, 0, 0, tiled=True)  37.9 us
    all_to_all x2, waiting for transfers between devices, to_all(): return lax.all_to_all(array, axes, 0, 0, tiled=True)  20.1 us
    all_to_all x2, starting transfers between devices, to_all(): return lax.all_to_all(array, axes, 0, 0, tiled=True)  12.2 us
    pallas_call x1, Pallas kernels, retain(): pl.pallas_call(retain_kernel, out_shape=(jax.ShapeDtypeStruct((2, HEAD, H...  7.24 us
    pallas_call x1, Pallas kernels, mixer(): pl.pallas_call(mixer_kernel, out_shape=jax.ShapeDtypeStruct((Z, TP, SHARE...  3.8 us
    unnamed x10, local copies, waits for them, and re-layouts  3.24 us
    ppermute x1, starting transfers between devices, local(): far_down = lax.ppermute(right[8:], 'x', shift(X, 3))  2.67 us
    pallas_call x1, Pallas kernels, pack(): pl.pallas_call(pack_kernel, out_shape=jax.ShapeDtypeStruct((16, 128, 256)...  2.23 us
  transfers between devices with their start and end apart: 10, of which 2 were waited for; matrix products, arithmetic and copies ran while one was open for 3% of the time, Pallas kernels for 7%

profile of v2, /device:TPU:1, one launch (start us, length us, event | category | flops | bytes accessed | tf_op | source)
XLA Modules:
  0.0 98.9 jit_solution(8202116259816083208)
XLA Ops:
  0.6 2.2 %pack.1 = bf16[16,128,256]{2,1,0:T(8,128)(2,1)} custom-call(bf16[16,128,256]{2,1,0:T(8,128)(2,1)} %bitcast.10, bf16[256,2048]{1,0:T(8,128)(2,1)} %refs_3_.1), custom_call_target="tpu_custom_call" | custom-call | tf_op jit(solution)/shard_map/pack/pallas_call | solution.py:54
  2.9 2.1 %collective-permute-start = (bf16[16,128,256]{2,1,0:T(8,128)(2,1)}, bf16[16,128,256]{2,1,0:T(8,128)(2,1)S(1)}, u32[]{:S(2)}, u32[]{:S(2)}) collective-permute-start(bf16[16,128,256]{2,1,0:T(8,128)(2,1)} %pack.1), channel_id=1, source_target_pairs={{0,8},{8,16},{16,24},{24,0},{1,9},{9,17},{17,25},{25,1},{2,10},{10... | collective-permute-start | bytes 3145736 | tf_op jit(solution)/shard_map/ppermute | solution.py:306
  5.0 1.4 %collective-permute-start.2 = (bf16[16,128,256]{2,1,0:T(8,128)(2,1)}, bf16[16,128,256]{2,1,0:T(8,128)(2,1)S(1)}, u32[]{:S(2)}, u32[]{:S(2)}) collective-permute-start(bf16[16,128,256]{2,1,0:T(8,128)(2,1)} %pack.1), channel_id=1, source_target_pairs={{0,24},{8,0},{16,8},{24,16},{1,25},{9,1},{17,9},{25,17},{2,26},{10... | collective-permute-start | bytes 3145736 | tf_op jit(solution)/shard_map/ppermute | solution.py:307
  6.3 0.9 broadcast_in_dim.2
  7.2 15.4 %all_to_all.20.tokens = bf16[8,128,256]{2,1,0:T(8,128)(2,1)} all-to-all(bf16[8,128,256]{2,1,0:T(8,128)(2,1)S(1)} %broadcast_in_dim.2), channel_id=1, replica_groups=mesh['z'=8,'x'=4,'y'=4,'c'=2] {'y','c'}, dimensions={0} | all-to-all | bytes 1048576 | tf_op jit(solution)/shard_map/all_to_all | solution.py:297
  22.7 7.2 %retain.1 = (f32[2,64,64,128]{3,2,1,0:T(8,128)}, bf16[8,16,2048]{2,1,0:T(8,128)(2,1)}) custom-call(f32[16]{0:T(128)} %constant.9.clone.decays, bf16[8,128,256]{2,1,0:T(8,128)(2,1)} %all_to_all.20.tokens, f32[2,64,64,128]{3,2,1,0:T(8,128)} %bitcast.14, bf16[2048,128]{1,0:T(8,128)(2,1)} %wq.1, bf16[2048,128]{1,0:T(8,128)(2,1)} %wk.1, bf16[2048,128]{1,0:T(8,128)(2,1)} %wv.1, ...), custom_call_target="tpu_custom_call" | custom-call | tf_op jit(solution)/shard_map/retain/pallas_call | solution.py:164
  29.9 0.0 copy-start.4
  29.9 4.4 %all-to-all-start.1 = ((bf16[8,16,2048]{2,1,0:T(8,128)(2,1)}), bf16[8,16,2048]{2,1,0:T(8,128)(2,1)S(1)}, u32[]{:S(2)}, u32[]{:S(2)}) async-start(bf16[8,16,2048]{2,1,0:T(8,128)(2,1)} %get-tuple-element.4), calls=%async_computation.1 | async-start | bytes 1048576 | tf_op jit(solution)/shard_map/all_to_all | solution.py:297
  34.4 0.0 collective-permute-done.refs_4_.refs_10_
  34.4 0.8 slice.8
  35.2 0.1 collective-permute-start.1
  35.3 0.0 collective-permute-done.2.refs_6_.refs_12_
  35.3 0.4 collective-permute-start.3
  35.7 0.8 slice.9
  36.5 2.7 %collective-permute-start.6 = (bf16[8,128,256]{2,1,0:T(8,128)(2,1)}, bf16[8,128,256]{2,1,0:T(8,128)(2,1)}, u32[]{:S(2)}, u32[]{:S(2)}) collective-permute-start(bf16[8,128,256]{2,1,0:T(8,128)(2,1)} %slice.9), channel_id=1, source_target_pairs={{0,24},{8,0},{16,8},{24,16},{1,25},{9,1},{17,9},{25,17},{2,26},{10... | collective-permute-start | bytes 1572872 | tf_op jit(solution)/shard_map/ppermute | solution.py:314
  39.2 4.5 %all-to-all-done.1.parts = bf16[8,16,2048]{2,1,0:T(8,128)(2,1)S(1)} async-done(((bf16[8,16,2048]{2,1,0:T(8,128)(2,1)}), bf16[8,16,2048]{2,1,0:T(8,128)(2,1)S(1)}, u32[]{:S(2)}, u32[]{:S(2)}) %all-to-all-start.1) | async-done | bytes 524320 | tf_op jit(solution)/shard_map/all_to_all | solution.py:297
  43.7 0.1 middle.1
  43.8 0.8 copy-done.3
  44.6 7.8 %all-to-all-start.2 = ((bf16[8,16,2048]{2,1,0:T(8,128)(2,1)}), bf16[8,16,2048]{2,1,0:T(8,128)(2,1)S(1)}, u32[]{:S(2)}, u32[]{:S(2)}) async-start(bf16[8,16,2048]{2,1,0:T(8,128)(2,1)} %copy-done.3), calls=%async_computation.2 | async-start | bytes 1048576 | tf_op jit(solution)/shard_map/all_to_all | solution.py:297
  52.4 0.0 collective-permute-done.4.refs_8_
  52.4 1.3 %collective-permute-start.5 = (bf16[8,128,256]{2,1,0:T(8,128)(2,1)}, bf16[8,128,256]{2,1,0:T(8,128)(2,1)S(1)}, u32[]{:S(2)}, u32[]{:S(2)}) collective-permute-start(bf16[8,128,256]{2,1,0:T(8,128)(2,1)} %collective-permute-done.4.refs_8_), channel_id=1, source_target_pairs={{0,1},{1,0},{2,3},{3,2},{4,5},{5,4},{6,7},{7,6},{8,9},{9,8},{10,11... | collective-permute-start | bytes 1572872 | tf_op jit(solution)/shard_map/ppermute | solution.py:320
  53.7 0.1 collective-permute-start.7
  53.8 15.6 %all-to-all-done.2.refs_0_ = bf16[8,16,2048]{2,1,0:T(8,128)(2,1)S(1)} async-done(((bf16[8,16,2048]{2,1,0:T(8,128)(2,1)}), bf16[8,16,2048]{2,1,0:T(8,128)(2,1)S(1)}, u32[]{:S(2)}, u32[]{:S(2)}) %all-to-all-start.2) | async-done | bytes 524320 | tf_op jit(solution)/shard_map/all_to_all | solution.py:297
  69.4 0.0 collective-permute-done.1.refs_5_.refs_11_
  69.4 0.0 collective-permute-done.3.refs_7_.refs_13_
  69.4 0.0 collective-permute-done.5.refs_9_
  69.5 0.0 copy-start.1
  69.5 1.2 %copy-done.1 = bf16[2048,256]{1,0:T(8,128)(2,1)S(1)} copy-done((bf16[2048,256]{1,0:T(8,128)(2,1)S(1)}, bf16[2048,256]{1,0:T(8,128)(2,1)}, u32[]{:S(2)}) %copy-start.1) | copy-done | bytes 1048600
  70.7 1.2 %copy-done.2 = bf16[256,2048]{1,0:T(8,128)(2,1)S(1)} copy-done((bf16[256,2048]{1,0:T(8,128)(2,1)S(1)}, bf16[256,2048]{1,0:T(8,128)(2,1)}, u32[]{:S(2)}) %copy-start.2) | copy-done | bytes 1048600
  71.9 3.8 %mixer.1 = bf16[8,8,16,256]{3,2,1,0:T(8,128)(2,1)S(1)} custom-call(bf16[8,16,2048]{2,1,0:T(8,128)(2,1)S(1)} %all-to-all-done.2.refs_0_, bf16[16,128]{1,0:T(8,128)(2,1)S(1)} %bitcast.13, bf16[16,128,256]{2,1,0:T(8,128)(2,1)S(1)} %bitcast.11, bf16[256,2048]{1,0:T(8,128)(2,1)S(1)} %copy-done.2, bf16[16,128,256]{2,1,0:T(8,128)(2,1)S(1)} %collective-permute-done.refs_4_.refs_10_, ...), custom_call_target="tpu_custom_call" | custom-call | tf_op jit(solution)/shard_map/mixer/pallas_call | solution.py:277
  75.7 22.5 %all_to_all.21 = bf16[64,16,256]{2,1,0:T(8,128)(2,1)S(1)} all-to-all(bf16[64,16,256]{2,1,0:T(8,128)(2,1)S(1)} %bitcast.12), channel_id=1, replica_groups=mesh['z'=8,'x'=4,'y'=4,'c'=2] {'z','y','c'}, dimensions={0} | all-to-all | bytes 1048576 | tf_op jit(solution)/shard_map/all_to_all | solution.py:297
  98.2 0.7 bitcast_reduce_fusion
  (8 shorter events, 0.0 us)
Async XLA Ops:
  2.9 31.5 %collective-permute-start = (bf16[16,128,256]{2,1,0:T(8,128)(2,1)}, bf16[16,128,256]{2,1,0:T(8,128)(2,1)S(1)}, u32[]{:S(2)}, u32[]{:S(2)}) collective-permute-start(bf16[16,128,256]{2,1,0:T(8,128)(2,1)} %pack.1), channel_id=1, source_target_pairs={{0,8},{8,16},{16,24},{24,0},{1,9},{9,17},{17,25},{25,1},{2,10},{10... | collective-permute-start | bytes 3145736 | tf_op jit(solution)/shard_map/ppermute | solution.py:306
  5.0 30.3 %collective-permute-start.2 = (bf16[16,128,256]{2,1,0:T(8,128)(2,1)}, bf16[16,128,256]{2,1,0:T(8,128)(2,1)S(1)}, u32[]{:S(2)}, u32[]{:S(2)}) collective-permute-start(bf16[16,128,256]{2,1,0:T(8,128)(2,1)} %pack.1), channel_id=1, source_target_pairs={{0,24},{8,0},{16,8},{24,16},{1,25},{9,1},{17,9},{25,17},{2,26},{10... | collective-permute-start | bytes 3145736 | tf_op jit(solution)/shard_map/ppermute | solution.py:307
  22.7 21.1 %copy-start = (bf16[8,128,256]{2,1,0:T(8,128)(2,1)S(1)}, bf16[8,128,256]{2,1,0:T(8,128)(2,1)}, u32[]{:S(2)}) copy-start(bf16[8,128,256]{2,1,0:T(8,128)(2,1)} %all_to_all.20.tokens) | copy-start | bytes 1572868
  29.9 39.5 %copy-start.4 = (bf16[2048]{0:T(1024)(128)(2,1)S(1)}, bf16[2048]{0:T(1024)(128)(2,1)}, u32[]{:S(2)}) copy-start(bf16[2048]{0:T(1024)(128)(2,1)} %param.24) | copy-start | bytes 12292
  29.9 13.8 %all-to-all-start.1 = ((bf16[8,16,2048]{2,1,0:T(8,128)(2,1)}), bf16[8,16,2048]{2,1,0:T(8,128)(2,1)S(1)}, u32[]{:S(2)}, u32[]{:S(2)}) async-start(bf16[8,16,2048]{2,1,0:T(8,128)(2,1)} %get-tuple-element.4), calls=%async_computation.1 | async-start | bytes 1048576 | tf_op jit(solution)/shard_map/all_to_all | solution.py:297
  35.2 17.2 %collective-permute-start.4 = (bf16[8,128,256]{2,1,0:T(8,128)(2,1)}, bf16[8,128,256]{2,1,0:T(8,128)(2,1)}, u32[]{:S(2)}, u32[]{:S(2)}) collective-permute-start(bf16[8,128,256]{2,1,0:T(8,128)(2,1)} %slice.8), channel_id=1, source_target_pairs={{0,8},{8,16},{16,24},{24,0},{1,9},{9,17},{17,25},{25,1},{2,10},{10... | collective-permute-start | bytes 1572872 | tf_op jit(solution)/shard_map/ppermute | solution.py:313
  35.2 34.2 %collective-permute-start.1 = (bf16[16,128,256]{2,1,0:T(8,128)(2,1)S(1)}, bf16[16,128,256]{2,1,0:T(8,128)(2,1)}, u32[]{:S(2)}, u32[]{:S(2)}) collective-permute-start(bf16[16,128,256]{2,1,0:T(8,128)(2,1)S(1)} %collective-permute-done.refs_4_.refs_10_), channel_id=1, source_target_pairs={{0,1},{1,0},{2,3},{3,2},{4,5},{5,4},{6,7},{7,6},{8,9},{9,8},{10,11... | collective-permute-start | bytes 3145736 | tf_op jit(solution)/shard_map/ppermute | solution.py:318
  35.3 34.1 %collective-permute-start.3 = (bf16[16,128,256]{2,1,0:T(8,128)(2,1)S(1)}, bf16[16,128,256]{2,1,0:T(8,128)(2,1)}, u32[]{:S(2)}, u32[]{:S(2)}) collective-permute-start(bf16[16,128,256]{2,1,0:T(8,128)(2,1)S(1)} %collective-permute-done.2.refs_6_.refs_12_), channel_id=1, source_target_pairs={{0,1},{1,0},{2,3},{3,2},{4,5},{5,4},{6,7},{7,6},{8,9},{9,8},{10,11... | collective-permute-start | bytes 3145736 | tf_op jit(solution)/shard_map/ppermute | solution.py:319
  36.5 17.2 %collective-permute-start.6 = (bf16[8,128,256]{2,1,0:T(8,128)(2,1)}, bf16[8,128,256]{2,1,0:T(8,128)(2,1)}, u32[]{:S(2)}, u32[]{:S(2)}) collective-permute-start(bf16[8,128,256]{2,1,0:T(8,128)(2,1)} %slice.9), channel_id=1, source_target_pairs={{0,24},{8,0},{16,8},{24,16},{1,25},{9,1},{17,9},{25,17},{2,26},{10... | collective-permute-start | bytes 1572872 | tf_op jit(solution)/shard_map/ppermute | solution.py:314
  43.8 0.8 copy-start.3
  44.6 24.8 %all-to-all-start.2 = ((bf16[8,16,2048]{2,1,0:T(8,128)(2,1)}), bf16[8,16,2048]{2,1,0:T(8,128)(2,1)S(1)}, u32[]{:S(2)}, u32[]{:S(2)}) async-start(bf16[8,16,2048]{2,1,0:T(8,128)(2,1)} %copy-done.3), calls=%async_computation.2 | async-start | bytes 1048576 | tf_op jit(solution)/shard_map/all_to_all | solution.py:297
  52.4 17.0 %collective-permute-start.5 = (bf16[8,128,256]{2,1,0:T(8,128)(2,1)}, bf16[8,128,256]{2,1,0:T(8,128)(2,1)S(1)}, u32[]{:S(2)}, u32[]{:S(2)}) collective-permute-start(bf16[8,128,256]{2,1,0:T(8,128)(2,1)} %collective-permute-done.4.refs_8_), channel_id=1, source_target_pairs={{0,1},{1,0},{2,3},{3,2},{4,5},{5,4},{6,7},{7,6},{8,9},{9,8},{10,11... | collective-permute-start | bytes 1572872 | tf_op jit(solution)/shard_map/ppermute | solution.py:320
  53.7 15.7 %collective-permute-start.7 = (bf16[8,128,256]{2,1,0:T(8,128)(2,1)}, bf16[8,128,256]{2,1,0:T(8,128)(2,1)}, u32[]{:S(2)}, u32[]{:S(2)}) collective-permute-start(bf16[8,128,256]{2,1,0:T(8,128)(2,1)} %collective-permute-done.6.refs_14_), channel_id=1, source_target_pairs={{0,1},{1,0},{2,3},{3,2},{4,5},{5,4},{6,7},{7,6},{8,9},{9,8},{10,11... | collective-permute-start | bytes 1572872 | tf_op jit(solution)/shard_map/ppermute | solution.py:321
  69.5 1.2 %copy-start.1 = (bf16[2048,256]{1,0:T(8,128)(2,1)S(1)}, bf16[2048,256]{1,0:T(8,128)(2,1)}, u32[]{:S(2)}) copy-start(bf16[2048,256]{1,0:T(8,128)(2,1)} %param.25) | copy-start | bytes 3145732
  70.7 1.2 %copy-start.2 = (bf16[256,2048]{1,0:T(8,128)(2,1)S(1)}, bf16[256,2048]{1,0:T(8,128)(2,1)}, u32[]{:S(2)}) copy-start(bf16[256,2048]{1,0:T(8,128)(2,1)} %refs_3_.1) | copy-start | bytes 3145732

commit v3 on v2

--- a/solution.py
+++ b/solution.py
@@ -18,10 +18,18 @@
 Z, X, Y, C = 8, 4, 4, 2
 TP = Y * C
 SHARE = ROWS // TP
-RETAIN_LIMIT = 58 * 2**20
-MIXER_LIMIT = 40 * 2**20
+RETAIN_LIMIT = 20 * 2**20
+MIXER_LIMIT = 20 * 2**20
 F32 = jnp.float32
 BF16 = jnp.bfloat16
+
+
+def in_hbm(array):
+    return pltpu.with_memory_space_constraint(array, pltpu.HBM)
+
+
+def in_vmem(array):
+    return pltpu.with_memory_space_constraint(array, pltpu.VMEM)
 
 
 def copy_all(copies):
@@ -54,11 +62,12 @@
     return pl.pallas_call(
         pack_kernel,
         out_shape=jax.ShapeDtypeStruct((16, 128, 256), BF16),
-        in_specs=[pl.BlockSpec(memory_space=pltpu.HBM)] * 2,
+        in_specs=[pl.BlockSpec(memory_space=pl.ANY)] * 2,
         out_specs=pl.BlockSpec(memory_space=pltpu.VMEM),
         scratch_shapes=[pltpu.SemaphoreType.DMA((10,))],
+        compiler_params=pltpu.CompilerParams(vmem_limit_bytes=8 * 2**20),
         name="pack",
-    )(w_up.reshape(16, 128, 256), w_down)
+    )(in_hbm(w_up.reshape(16, 128, 256)), in_hbm(w_down))
 
 
 CHUNKS = 8
@@ -75,10 +84,18 @@
     return jnp.concatenate([wide[2 * j : 2 * j + 1], wide[2 * j + 1 : 2 * j + 2]], axis=1)
 
 
-def retain_kernel(
-    decays, tokens, states, wq, wk, wv, wg, wo, mix_gain, head_gain, cosine, sines,
-    new_states, partial, weights, w_out, old, new, qt, kt, ret, w_sems, in_sems, out_sems,
-):
+def place(k, other):
+    y, c = lax.axis_index("y"), lax.axis_index("c")
+    return 2 * lax.rem(y + (Y - k), Y) + (1 - c if other else c)
+
+
+def retain_kernel(decays, *refs):
+    blocks = refs[:TP]
+    states, wq, wk, wv, wg, wo, mix_gain, head_gain, cosine, sines = refs[TP : TP + 10]
+    new_states, mine, others, own = refs[TP + 10 : TP + 14]
+    tokens, weights, w_out, old, new, qt, kt, ret, shares = refs[TP + 14 : TP + 23]
+    w_sems, in_sems, out_sems = refs[TP + 23 :]
+
     def part(ref, i):
         return ref.at[i // PER_HEAD, pl.ds((i % PER_HEAD) * STEP, STEP)]
 
@@ -99,8 +116,10 @@
         copy.start()
 
     squares = jnp.zeros((ROWS, 256), F32)
-    for j in range(TP):
-        block = tokens[j].astype(F32)
+    for i in range(TP):
+        block = blocks[i][...]
+        tokens[place(i % Y, i >= Y)] = block
+        block = block.astype(F32)
         squares += block * block
     inverse_rms = lax.rsqrt(jnp.sum(squares, axis=1, keepdims=True) / D + EPSILON)
     normed = jnp.concatenate(
@@ -151,25 +170,33 @@
 
     out = (ret[...].T * head_gain[...].astype(F32) * (gating * jax.nn.sigmoid(gating))).astype(BF16)
     wo_copy.wait()
-    partial[...] = (
-        jnp.dot(out, w_out[...], preferred_element_type=F32).astype(BF16).reshape(TP, SHARE, D)
-    )
+    partial = jnp.dot(out, w_out[...], preferred_element_type=F32)
+    shares[...] = partial.reshape(Y, C, SHARE, D)
+    core = lax.axis_index("c")
+    mine[...] = shares[:, core]
+    others[...] = shares[:, 1 - core].astype(BF16)
+    at = pl.multiple_of(place(0, False) * SHARE, SHARE)
+    own[...] = jnp.concatenate([tokens[j, pl.ds(at, SHARE), :] for j in range(TP)], axis=1)
     for copy in out_copies:
         copy.wait()
 
 
-def retain(tokens, states, wq, wk, wv, wg, wo, mix_gain, head_gain):
+def retain(blocks, states, wq, wk, wv, wg, wo, mix_gain, head_gain):
     any_space = pl.BlockSpec(memory_space=pl.ANY)
     vmem = pl.BlockSpec(memory_space=pltpu.VMEM)
     return pl.pallas_call(
         retain_kernel,
         out_shape=(
             jax.ShapeDtypeStruct((2, HEAD, HEAD, ROWS), F32),
-            jax.ShapeDtypeStruct((TP, SHARE, D), BF16),
+            jax.ShapeDtypeStruct((Y, SHARE, D), F32),
+            jax.ShapeDtypeStruct((Y, SHARE, D), BF16),
+            jax.ShapeDtypeStruct((SHARE, D), BF16),
         ),
-        in_specs=[pl.BlockSpec(memory_space=pltpu.SMEM), vmem] + [any_space] * 6 + [vmem] * 4,
-        out_specs=(any_space, vmem),
+        in_specs=[pl.BlockSpec(memory_space=pltpu.SMEM)]
+        + [vmem] * TP + [any_space] * 6 + [vmem] * 4,
+        out_specs=(any_space, vmem, vmem, vmem),
         scratch_shapes=[
+            pltpu.VMEM((TP, ROWS, 256), BF16),
             pltpu.VMEM((D, 512), BF16),
             pltpu.VMEM((128, D), BF16),
             pltpu.VMEM((2, HEAD, HEAD, ROWS), F32),
@@ -177,6 +204,7 @@
             pltpu.VMEM((128, ROWS), F32),
             pltpu.VMEM((128, ROWS), F32),
             pltpu.VMEM((128, ROWS), F32),
+            pltpu.VMEM((Y, C, SHARE, D), F32),
             pltpu.SemaphoreType.DMA((5,)),
             pltpu.SemaphoreType.DMA((CHUNKS,)),
             pltpu.SemaphoreType.DMA((CHUNKS,)),
@@ -184,32 +212,49 @@
         compiler_params=pltpu.CompilerParams(vmem_limit_bytes=RETAIN_LIMIT),
         name="retain",
     )(
-        DECAYS, tokens, states, wq, wk, wv, wg, wo, mix_gain.reshape(16, 128),
-        head_gain.reshape(1, 128), COSINE, SINES,
-    )
-
-
-def middle_kernel(parts, tokens, out):
-    at = pl.multiple_of((lax.axis_index("y") * C + lax.axis_index("c")) * SHARE, SHARE)
-    total = parts[0].astype(F32)
-    for t in range(1, TP):
-        total += parts[t].astype(F32)
-    own = jnp.concatenate([tokens[j, pl.ds(at, SHARE), :] for j in range(TP)], axis=1)
-    middle = (own.astype(F32) + total).astype(BF16)
+        in_hbm(DECAYS), in_hbm(blocks[0]), *map(in_vmem, blocks[1:]), *map(in_hbm, (states, wq, wk, wv, wg, wo)),
+        *map(in_hbm, (mix_gain.reshape(16, 128), head_gain.reshape(1, 128), COSINE, SINES)),
+    )
+
+
+def pair_kernel(mine, others, *outs):
+    y = lax.axis_index("y")
+    for k in range(Y):
+        to = lax.rem(y + k, Y)
+        outs[k][...] = (mine[to] + others[to].astype(F32)).astype(outs[k].dtype)
+
+
+def pair(mine, others):
+    vmem = pl.BlockSpec(memory_space=pltpu.VMEM)
+    return pl.pallas_call(
+        pair_kernel,
+        out_shape=[jax.ShapeDtypeStruct((SHARE, D), BF16 if k else F32) for k in range(Y)],
+        in_specs=[vmem] * 2,
+        out_specs=[vmem] * Y,
+        compiler_params=pltpu.CompilerParams(vmem_limit_bytes=8 * 2**20),
+        name="pair",
+    )(in_vmem(mine), in_vmem(others))
+
+
+def middle_kernel(own, first, *refs):
+    total = first[...]
+    for part in refs[:-1]:
+        total += part[...].astype(F32)
+    middle = (own[...].astype(F32) + total).astype(BF16)
     for z in range(Z):
-        out[z] = middle
-
-
-def middle_rows(parts, tokens):
+        refs[-1][z] = middle
+
+
+def middle_rows(own, parts):
     vmem = pl.BlockSpec(memory_space=pltpu.VMEM)
     return pl.pallas_call(
         middle_kernel,
         out_shape=jax.ShapeDtypeStruct((Z, SHARE, D), BF16),
-        in_specs=[vmem] * 2,
+        in_specs=[vmem] * (Y + 1),
         out_specs=vmem,
         compiler_params=pltpu.CompilerParams(vmem_limit_bytes=8 * 2**20),
         name="middle",
-    )(parts, tokens)
+    )(*map(in_vmem, (own, *parts)))
 
 
 def mixer_kernel(*refs):
@@ -233,10 +278,11 @@
                     sems.at[9 + 3 * p + i],
                 )
             )
-        last = downs[p].shape[0] - 8
         down_copies.append(
             pltpu.make_async_copy(
-                downs[p].at[pl.ds(last, 8)], down.at[:, pl.ds(at, 128), :], sems.at[9 + 3 * p + 2]
+                downs[p].at[pl.ds(downs[p].shape[0] - 8, 8)],
+                down.at[:, pl.ds(at, 128), :],
+                sems.at[9 + 3 * p + 2],
             )
         )
     for copy in up_copies + down_copies:
@@ -276,7 +322,7 @@
     vmem = pl.BlockSpec(memory_space=pltpu.VMEM)
     return pl.pallas_call(
         mixer_kernel,
-        out_shape=jax.ShapeDtypeStruct((Z, TP, SHARE, 256), BF16),
+        out_shape=pltpu.VMEM((Z, TP, SHARE, 256), BF16),
         in_specs=[vmem] * 2 + [any_space] * 14,
         out_specs=vmem,
         scratch_shapes=[
@@ -286,7 +332,10 @@
         ],
         compiler_params=pltpu.CompilerParams(vmem_limit_bytes=MIXER_LIMIT),
         name="mixer",
-    )(rows, channel_gain.reshape(16, 128), own_up.reshape(16, 128, 256), own_down, *ups, *downs)
+    )(
+        in_vmem(rows), in_hbm(channel_gain.reshape(16, 128)), in_hbm(own_up.reshape(16, 128, 256)),
+        in_hbm(own_down), *map(in_hbm, ups), *map(in_hbm, downs),
+    )
 
 
 def shift(count, by):
@@ -301,28 +350,29 @@
     tokens, states, mix_gain, w_query, w_key, w_value, w_gate, head_gain, w_output,
     channel_gain, w_up, w_down,
 ):
-    rows = to_all(jnp.broadcast_to(tokens[None], (TP, ROWS, 256)), ("y", "c"))
+    swap = [(0, 1), (1, 0)]
+    blocks = [tokens] + [lax.ppermute(tokens, "y", shift(Y, by)) for by in (1, 2, 3)]
     packed = pack(w_up, w_down)
     left = lax.ppermute(packed, "x", shift(X, 1))
     right = lax.ppermute(packed, "x", shift(X, 3))
-    new_states, partial = retain(
-        rows, states.transpose(1, 2, 3, 0), w_query, w_key, w_value, w_gate, w_output,
+    blocks += [lax.ppermute(block, "c", swap) for block in blocks]
+    new_states, mine, others, own = retain(
+        blocks, states.transpose(1, 2, 3, 0), w_query, w_key, w_value, w_gate, w_output,
         mix_gain, head_gain,
     )
-    parts = to_all(partial, ("y", "c"))
+    others = lax.ppermute(others, "c", swap)
+    parts = pair(mine, others)
+    parts = [parts[0]] + [lax.ppermute(parts[k], "y", shift(Y, k)) for k in (1, 2, 3)]
+    middle = middle_rows(own, parts)
+    everyone = to_all(middle, "z")
     far_up = lax.ppermute(left[:8], "x", shift(X, 1))
     far_down = lax.ppermute(right[8:], "x", shift(X, 3))
-    middle = middle_rows(parts, rows)
-    everyone = to_all(middle, "z")
-    swap = [(0, 1), (1, 0)]
-    left_other = lax.ppermute(left, "c", swap)
-    right_other = lax.ppermute(right, "c", swap)
-    up_other = lax.ppermute(far_up, "c", swap)
-    down_other = lax.ppermute(far_down, "c", swap)
+    left_other, right_other = [lax.ppermute(w, "c", swap) for w in (left, right)]
+    far_other = [lax.ppermute(w, "c", swap) for w in (far_up, far_down)]
     down = mixer(
         everyone, channel_gain, w_up, w_down,
-        (left, left_other, right, right_other, far_up, up_other),
-        (left, left_other, right, right_other, far_down, down_other),
+        (left, left_other, right, right_other, far_up, far_other[0]),
+        (left, left_other, right, right_other, far_down, far_other[1]),
     )
     down = to_all(down.reshape(Z * TP, SHARE, 256), ("z", "y", "c"))
     layer_out = jnp.sum(down.reshape(Z, ROWS, 256).astype(F32), axis=0).astype(BF16)

time: 99.4 us -> 95.7 us (0.963)
  starting transfers between devices: 20.3 us -> 35.5 us
  blocking collectives: 37.9 us -> 25.3 us
  local copies, waits for them, and re-layouts: 5.79 us -> 1.78 us
  waiting for transfers between devices: 20.1 us -> 17.9 us
    ppermute x4 -> x15, starting transfers between devices: 1.95 us -> 21.2 us  [the longest x4 5.54 us: local(): blocks += [lax.ppermute(block, 'c', swap) for block in blocks]]
    all_to_all x2 -> x1, blocking collectives: 37.9 us -> 25.3 us  [to_all(): return lax.all_to_all(array, axes, 0, 0, tiled=True)]
    all_to_all x2 -> x1, waiting for transfers between devices: 20.1 us -> 13.9 us  [to_all(): return lax.all_to_all(array, axes, 0, 0, tiled=True)]
    ppermute x4 -> x15, waiting for transfers between devices: 0.01 us -> 4.01 us  [the longest x3 1.66 us: local(): lax.ppermute(parts[k], 'y', shift(Y, k))]
    all_to_all x2 -> x1, starting transfers between devices: 12.2 us -> 8.24 us  [to_all(): return lax.all_to_all(array, axes, 0, 0, tiled=True)]
    unnamed x10 -> x6, local copies, waits for them, and re-layouts: 3.24 us -> 0.01 us
    pallas_call x1 -> x2, Pallas kernels: 3.8 us -> 5.09 us  [the longest x1 5.04 us: mixer(): pl.pallas_call(mixer_kernel, out_shape=pltpu.VMEM((Z, TP, SHARE, 256), BF...]
    pallas_call x1, Pallas kernels: 7.24 us -> 6.24 us  [retain(): pl.pallas_call(retain_kernel, out_shape=(jax.ShapeDtypeStruct((2, HEAD, H...]
  transfers between devices with their start and end apart: 10 -> 20, of which waited for: 2 -> 6; matrix products, arithmetic and copies ran while one was open for 3% -> 2% of each run, Pallas kernels for 7% -> 7%
where the time goes in v3:
time: 95.7 us; the launch traced here: 95.4 us
  starting transfers between devices  35.5 us (37%)
  blocking collectives  25.3 us (26%)
  waiting for transfers between devices  17.9 us (19%)
  Pallas kernels  13.4 us (14%)
  local copies, waits for them, and re-layouts  1.78 us (2%)
    all_to_all x1, blocking collectives, to_all(): return lax.all_to_all(array, axes, 0, 0, tiled=True)  25.3 us
    all_to_all x1, waiting for transfers between devices, to_all(): return lax.all_to_all(array, axes, 0, 0, tiled=True)  13.9 us
    all_to_all x1, starting transfers between devices, to_all(): return lax.all_to_all(array, axes, 0, 0, tiled=True)  8.24 us
    pallas_call x1, Pallas kernels, retain(): pl.pallas_call(retain_kernel, out_shape=(jax.ShapeDtypeStruct((2, HEAD, H...  6.24 us
    ppermute x4, starting transfers between devices, local(): blocks += [lax.ppermute(block, 'c', swap) for block in blocks]  5.54 us
    ppermute x3, starting transfers between devices, local(): lax.ppermute(parts[k], 'y', shift(Y, k))  5.41 us
    ppermute x3, starting transfers between devices, local(): lax.ppermute(tokens, 'y', shift(Y, by))  5.09 us
    pallas_call x1, Pallas kernels, mixer(): pl.pallas_call(mixer_kernel, out_shape=pltpu.VMEM((Z, TP, SHARE, 256), BF...  5.04 us
  transfers between devices with their start and end apart: 20, of which 6 were waited for; matrix products, arithmetic and copies ran while one was open for 2% of the time, Pallas kernels for 7%

profile of v3, /device:TPU:1, one launch (start us, length us, event | category | flops | bytes accessed | tf_op | source)
XLA Modules:
  0.0 95.4 jit_solution(7117860112033326026)
XLA Ops:
  0.6 1.2 %pack.1 = bf16[16,128,256]{2,1,0:T(8,128)(2,1)S(1)} custom-call(bf16[16,128,256]{2,1,0:T(8,128)(2,1)} %bitcast.11, bf16[256,2048]{1,0:T(8,128)(2,1)} %refs_3_.1), custom_call_target="tpu_custom_call" | custom-call | tf_op jit(solution)/shard_map/pack/pallas_call | solution.py:62
  1.9 2.1 %collective-permute-start.11 = (bf16[16,128,256]{2,1,0:T(8,128)(2,1)S(1)}, bf16[16,128,256]{2,1,0:T(8,128)(2,1)S(1)}, u32[]{:S(2)}, u32[]{:S(2)}) collective-permute-start(bf16[16,128,256]{2,1,0:T(8,128)(2,1)S(1)} %pack.1), channel_id=1, source_target_pairs={{0,8},{8,16},{16,24},{24,0},{1,9},{9,17},{17,25},{25,1},{2,10},{10... | collective-permute-start | bytes 3145736 | tf_op jit(solution)/shard_map/ppermute | solution.py:356
  4.0 1.4 %collective-permute-start.13 = (bf16[16,128,256]{2,1,0:T(8,128)(2,1)S(1)}, bf16[16,128,256]{2,1,0:T(8,128)(2,1)S(1)}, u32[]{:S(2)}, u32[]{:S(2)}) collective-permute-start(bf16[16,128,256]{2,1,0:T(8,128)(2,1)S(1)} %pack.1), channel_id=1, source_target_pairs={{0,24},{8,0},{16,8},{24,16},{1,25},{9,1},{17,9},{25,17},{2,26},{10... | collective-permute-start | bytes 3145736 | tf_op jit(solution)/shard_map/ppermute | solution.py:357
  5.3 1.4 %collective-permute-start = (bf16[128,256]{1,0:T(8,128)(2,1)}, bf16[128,256]{1,0:T(8,128)(2,1)S(1)}, u32[]{:S(2)}, u32[]{:S(2)}) collective-permute-start(bf16[128,256]{1,0:T(8,128)(2,1)} %refs_0_.1), channel_id=1, source_target_pairs={{0,2},{2,4},{4,6},{6,0},{1,3},{3,5},{5,7},{7,1},{8,10},{10,12},{12... | collective-permute-start | bytes 196616 | tf_op jit(solution)/shard_map/ppermute | solution.py:354
  6.7 2.6 %collective-permute-start.1 = (bf16[128,256]{1,0:T(8,128)(2,1)}, bf16[128,256]{1,0:T(8,128)(2,1)S(1)}, u32[]{:S(2)}, u32[]{:S(2)}) collective-permute-start(bf16[128,256]{1,0:T(8,128)(2,1)} %refs_0_.1), channel_id=1, source_target_pairs={{0,4},{2,6},{4,0},{6,2},{1,5},{3,7},{5,1},{7,3},{8,12},{10,14},{12... | collective-permute-start | bytes 196616 | tf_op jit(solution)/shard_map/ppermute | solution.py:354
  9.4 1.1 %collective-permute-start.2 = (bf16[128,256]{1,0:T(8,128)(2,1)}, bf16[128,256]{1,0:T(8,128)(2,1)S(1)}, u32[]{:S(2)}, u32[]{:S(2)}) collective-permute-start(bf16[128,256]{1,0:T(8,128)(2,1)} %refs_0_.1), channel_id=1, source_target_pairs={{0,6},{2,0},{4,2},{6,4},{1,7},{3,1},{5,3},{7,5},{8,14},{10,8},{12,... | collective-permute-start | bytes 196616 | tf_op jit(solution)/shard_map/ppermute | solution.py:354
  10.4 4.3 %collective-permute-start.3 = (bf16[128,256]{1,0:T(8,128)(2,1)}, bf16[128,256]{1,0:T(8,128)(2,1)S(1)}, u32[]{:S(2)}, u32[]{:S(2)}) collective-permute-start(bf16[128,256]{1,0:T(8,128)(2,1)} %refs_0_.1), channel_id=1, source_target_pairs={{0,1},{1,0},{2,3},{3,2},{4,5},{5,4},{6,7},{7,6},{8,9},{9,8},{10,11... | collective-permute-start | bytes 196616 | tf_op jit(solution)/shard_map/ppermute | solution.py:358
  14.8 0.0 collective-permute-start.4
  14.8 0.8 collective-permute-start.5
  15.6 0.3 collective-permute-done.3.refs_4_
  15.9 0.4 collective-permute-start.6
  16.2 0.3 collective-permute-done.5.refs_6_
  16.5 0.6 collective-permute-done.6.refs_7_
  17.1 6.2 %retain.1 = (f32[2,64,64,128]{3,2,1,0:T(8,128)}, f32[4,16,2048]{2,1,0:T(8,128)S(1)}, bf16[4,16,2048]{2,1,0:T(8,128)(2,1)S(1)}, bf16[16,2048]{1,0:T(8,128)(2,1)S(1)}) custom-call(f32[16]{0:T(128)} %constant.9.clone.decays, bf16[128,256]{1,0:T(8,128)(2,1)} %refs_0_.1, bf16[128,256]{1,0:T(8,128)(2,1)S(1)} %collective-permute-done.refs_1_, ...), custom_call_target="tpu_custom_call" | custom-call | tf_op jit(solution)/shard_map/retain/pallas_call | solution.py:187
  23.4 0.4 collective-permute-start.7
  23.8 1.2 %collective-permute-done.7.others = bf16[4,16,2048]{2,1,0:T(8,128)(2,1)S(1)} collective-permute-done((bf16[4,16,2048]{2,1,0:T(8,128)(2,1)S(1)}, bf16[4,16,2048]{2,1,0:T(8,128)(2,1)S(1)}, u32[]{:S(2)}, u32[]{:S(2)}) %collective-permute-start.7) | collective-permute-done | bytes 262176 | tf_op jit(solution)/shard_map/ppermute | solution.py:363
  25.1 2.2 %collective-permute-start.10 = (bf16[16,2048]{1,0:T(8,128)(2,1)S(1)}, bf16[16,2048]{1,0:T(8,128)(2,1)S(1)}, u32[]{:S(2)}, u32[]{:S(2)}) collective-permute-start(bf16[16,2048]{1,0:T(8,128)(2,1)S(1)} %get-tuple-element.16), channel_id=1, source_target_pairs={{0,6},{2,0},{4,2},{6,4},{1,7},{3,1},{5,3},{7,5},{8,14},{10,8},{12,... | collective-permute-start | bytes 196616 | tf_op jit(solution)/shard_map/ppermute | solution.py:365
  27.3 0.9 slice.8
  28.2 0.5 collective-permute-start.15
  28.7 0.9 slice.9
  29.6 2.2 %collective-permute-start.17 = (bf16[8,128,256]{2,1,0:T(8,128)(2,1)}, bf16[8,128,256]{2,1,0:T(8,128)(2,1)}, u32[]{:S(2)}, u32[]{:S(2)}) collective-permute-start(bf16[8,128,256]{2,1,0:T(8,128)(2,1)} %slice.9), channel_id=1, source_target_pairs={{0,24},{8,0},{16,8},{24,16},{1,25},{9,1},{17,9},{25,17},{2,26},{10... | collective-permute-start | bytes 1572872 | tf_op jit(solution)/shard_map/ppermute | solution.py:369
  31.7 2.6 %collective-permute-start.12 = (bf16[16,128,256]{2,1,0:T(8,128)(2,1)S(1)}, bf16[16,128,256]{2,1,0:T(8,128)(2,1)}, u32[]{:S(2)}, u32[]{:S(2)}) collective-permute-start(bf16[16,128,256]{2,1,0:T(8,128)(2,1)S(1)} %collective-permute-done.11.refs_4_.refs_10_), channel_id=1, source_target_pairs={{0,1},{1,0},{2,3},{3,2},{4,5},{5,4},{6,7},{7,6},{8,9},{9,8},{10,11... | collective-permute-start | bytes 3145736 | tf_op jit(solution)/shard_map/ppermute | solution.py:370
  34.4 3.2 %collective-permute-start.9 = (bf16[16,2048]{1,0:T(8,128)(2,1)S(1)}, bf16[16,2048]{1,0:T(8,128)(2,1)S(1)}, u32[]{:S(2)}, u32[]{:S(2)}) collective-permute-start(bf16[16,2048]{1,0:T(8,128)(2,1)S(1)} %get-tuple-element.15), channel_id=1, source_target_pairs={{0,4},{2,6},{4,0},{6,2},{1,5},{3,7},{5,1},{7,3},{8,12},{10,14},{12... | collective-permute-start | bytes 196616 | tf_op jit(solution)/shard_map/ppermute | solution.py:365
  37.6 1.7 %collective-permute-done.9.refs_1_ = bf16[16,2048]{1,0:T(8,128)(2,1)S(1)} collective-permute-done((bf16[16,2048]{1,0:T(8,128)(2,1)S(1)}, bf16[16,2048]{1,0:T(8,128)(2,1)S(1)}, u32[]{:S(2)}, u32[]{:S(2)}) %collective-permute-start.9) | collective-permute-done | bytes 65568 | tf_op jit(solution)/shard_map/ppermute | solution.py:365
  39.2 0.8 middle.1
  40.1 8.2 %all-to-all-start = ((bf16[8,16,2048]{2,1,0:T(8,128)(2,1)}), bf16[8,16,2048]{2,1,0:T(8,128)(2,1)S(1)}, u32[]{:S(2)}, u32[]{:S(2)}) async-start(bf16[8,16,2048]{2,1,0:T(8,128)(2,1)} %middle.1), calls=%async_computation | async-start | bytes 1048576 | tf_op jit(solution)/shard_map/all_to_all | solution.py:346
  48.3 1.9 %collective-permute-start.16 = (bf16[8,128,256]{2,1,0:T(8,128)(2,1)S(1)}, bf16[8,128,256]{2,1,0:T(8,128)(2,1)}, u32[]{:S(2)}, u32[]{:S(2)}) collective-permute-start(bf16[8,128,256]{2,1,0:T(8,128)(2,1)S(1)} %collective-permute-done.15.refs_8_), channel_id=1, source_target_pairs={{0,1},{1,0},{2,3},{3,2},{4,5},{5,4},{6,7},{7,6},{8,9},{9,8},{10,11... | collective-permute-start | bytes 1572872 | tf_op jit(solution)/shard_map/ppermute | solution.py:371
  50.3 0.1 collective-permute-start.18
  50.4 13.9 %all-to-all-done.refs_0_ = bf16[8,16,2048]{2,1,0:T(8,128)(2,1)S(1)} async-done(((bf16[8,16,2048]{2,1,0:T(8,128)(2,1)}), bf16[8,16,2048]{2,1,0:T(8,128)(2,1)S(1)}, u32[]{:S(2)}, u32[]{:S(2)}) %all-to-all-start) | async-done | bytes 524320 | tf_op jit(solution)/shard_map/all_to_all | solution.py:346
  64.4 5.0 %mixer.1 = bf16[8,8,16,256]{3,2,1,0:T(8,128)(2,1)S(1)} custom-call(bf16[8,16,2048]{2,1,0:T(8,128)(2,1)S(1)} %all-to-all-done.refs_0_, bf16[16,128]{1,0:T(8,128)(2,1)} %bitcast.16, bf16[16,128,256]{2,1,0:T(8,128)(2,1)} %bitcast.12, bf16[256,2048]{1,0:T(8,128)(2,1)} %refs_3_.1, bf16[16,128,256]{2,1,0:T(8,128)(2,1)} %copy-done, ...), custom_call_target="tpu_custom_call" | custom-call | tf_op jit(solution)/shard_map/mixer/pallas_call | solution.py:323
  69.4 25.3 %all_to_all.10 = bf16[64,16,256]{2,1,0:T(8,128)(2,1)S(1)} all-to-all(bf16[64,16,256]{2,1,0:T(8,128)(2,1)S(1)} %bitcast.10), channel_id=1, replica_groups=mesh['z'=8,'x'=4,'y'=4,'c'=2] {'z','y','c'}, dimensions={0} | all-to-all | bytes 1048576 | tf_op jit(solution)/shard_map/all_to_all | solution.py:346
  94.7 0.7 bitcast_reduce_fusion
  (23 shorter events, 0.1 us)
Async XLA Ops:
  1.9 25.4 %collective-permute-start.11 = (bf16[16,128,256]{2,1,0:T(8,128)(2,1)S(1)}, bf16[16,128,256]{2,1,0:T(8,128)(2,1)S(1)}, u32[]{:S(2)}, u32[]{:S(2)}) collective-permute-start(bf16[16,128,256]{2,1,0:T(8,128)(2,1)S(1)} %pack.1), channel_id=1, source_target_pairs={{0,8},{8,16},{16,24},{24,0},{1,9},{9,17},{17,25},{25,1},{2,10},{10... | collective-permute-start | bytes 3145736 | tf_op jit(solution)/shard_map/ppermute | solution.py:356
  4.0 24.7 %collective-permute-start.13 = (bf16[16,128,256]{2,1,0:T(8,128)(2,1)S(1)}, bf16[16,128,256]{2,1,0:T(8,128)(2,1)S(1)}, u32[]{:S(2)}, u32[]{:S(2)}) collective-permute-start(bf16[16,128,256]{2,1,0:T(8,128)(2,1)S(1)} %pack.1), channel_id=1, source_target_pairs={{0,24},{8,0},{16,8},{24,16},{1,25},{9,1},{17,9},{25,17},{2,26},{10... | collective-permute-start | bytes 3145736 | tf_op jit(solution)/shard_map/ppermute | solution.py:357
  5.3 5.1 %collective-permute-start = (bf16[128,256]{1,0:T(8,128)(2,1)}, bf16[128,256]{1,0:T(8,128)(2,1)S(1)}, u32[]{:S(2)}, u32[]{:S(2)}) collective-permute-start(bf16[128,256]{1,0:T(8,128)(2,1)} %refs_0_.1), channel_id=1, source_target_pairs={{0,2},{2,4},{4,6},{6,0},{1,3},{3,5},{5,7},{7,1},{8,10},{10,12},{12... | collective-permute-start | bytes 196616 | tf_op jit(solution)/shard_map/ppermute | solution.py:354
  6.7 8.0 %collective-permute-start.1 = (bf16[128,256]{1,0:T(8,128)(2,1)}, bf16[128,256]{1,0:T(8,128)(2,1)S(1)}, u32[]{:S(2)}, u32[]{:S(2)}) collective-permute-start(bf16[128,256]{1,0:T(8,128)(2,1)} %refs_0_.1), channel_id=1, source_target_pairs={{0,4},{2,6},{4,0},{6,2},{1,5},{3,7},{5,1},{7,3},{8,12},{10,14},{12... | collective-permute-start | bytes 196616 | tf_op jit(solution)/shard_map/ppermute | solution.py:354
  9.4 5.4 %collective-permute-start.2 = (bf16[128,256]{1,0:T(8,128)(2,1)}, bf16[128,256]{1,0:T(8,128)(2,1)S(1)}, u32[]{:S(2)}, u32[]{:S(2)}) collective-permute-start(bf16[128,256]{1,0:T(8,128)(2,1)} %refs_0_.1), channel_id=1, source_target_pairs={{0,6},{2,0},{4,2},{6,4},{1,7},{3,1},{5,3},{7,5},{8,14},{10,8},{12,... | collective-permute-start | bytes 196616 | tf_op jit(solution)/shard_map/ppermute | solution.py:354
  10.4 5.5 %collective-permute-start.3 = (bf16[128,256]{1,0:T(8,128)(2,1)}, bf16[128,256]{1,0:T(8,128)(2,1)S(1)}, u32[]{:S(2)}, u32[]{:S(2)}) collective-permute-start(bf16[128,256]{1,0:T(8,128)(2,1)} %refs_0_.1), channel_id=1, source_target_pairs={{0,1},{1,0},{2,3},{3,2},{4,5},{5,4},{6,7},{7,6},{8,9},{9,8},{10,11... | collective-permute-start | bytes 196616 | tf_op jit(solution)/shard_map/ppermute | solution.py:358
  14.8 1.5 %collective-permute-start.4 = (bf16[128,256]{1,0:T(8,128)(2,1)S(1)}, bf16[128,256]{1,0:T(8,128)(2,1)S(1)}, u32[]{:S(2)}, u32[]{:S(2)}) collective-permute-start(bf16[128,256]{1,0:T(8,128)(2,1)S(1)} %collective-permute-done.refs_1_), channel_id=1, source_target_pairs={{0,1},{1,0},{2,3},{3,2},{4,5},{5,4},{6,7},{7,6},{8,9},{9,8},{10,11... | collective-permute-start | bytes 196616 | tf_op jit(solution)/shard_map/ppermute | solution.py:358
  14.8 1.7 %collective-permute-start.5 = (bf16[128,256]{1,0:T(8,128)(2,1)S(1)}, bf16[128,256]{1,0:T(8,128)(2,1)S(1)}, u32[]{:S(2)}, u32[]{:S(2)}) collective-permute-start(bf16[128,256]{1,0:T(8,128)(2,1)S(1)} %collective-permute-done.1.refs_2_), channel_id=1, source_target_pairs={{0,1},{1,0},{2,3},{3,2},{4,5},{5,4},{6,7},{7,6},{8,9},{9,8},{10,11... | collective-permute-start | bytes 196616 | tf_op jit(solution)/shard_map/ppermute | solution.py:358
  15.9 1.3 %collective-permute-start.6 = (bf16[128,256]{1,0:T(8,128)(2,1)S(1)}, bf16[128,256]{1,0:T(8,128)(2,1)S(1)}, u32[]{:S(2)}, u32[]{:S(2)}) collective-permute-start(bf16[128,256]{1,0:T(8,128)(2,1)S(1)} %collective-permute-done.2.refs_3_), channel_id=1, source_target_pairs={{0,1},{1,0},{2,3},{3,2},{4,5},{5,4},{6,7},{7,6},{8,9},{9,8},{10,11... | collective-permute-start | bytes 196616 | tf_op jit(solution)/shard_map/ppermute | solution.py:358
  23.4 1.6 %collective-permute-start.7 = (bf16[4,16,2048]{2,1,0:T(8,128)(2,1)S(1)}, bf16[4,16,2048]{2,1,0:T(8,128)(2,1)S(1)}, u32[]{:S(2)}, u32[]{:S(2)}) collective-permute-start(bf16[4,16,2048]{2,1,0:T(8,128)(2,1)S(1)} %get-tuple-element.12), channel_id=1, source_target_pairs={{0,1},{1,0},{2,3},{3,2},{4,5},{5,4},{6,7},{7,6},{8,9},{9,8},{10,11... | collective-permute-start | bytes 786440 | tf_op jit(solution)/shard_map/ppermute | solution.py:363
  25.1 9.3 %collective-permute-start.10 = (bf16[16,2048]{1,0:T(8,128)(2,1)S(1)}, bf16[16,2048]{1,0:T(8,128)(2,1)S(1)}, u32[]{:S(2)}, u32[]{:S(2)}) collective-permute-start(bf16[16,2048]{1,0:T(8,128)(2,1)S(1)} %get-tuple-element.16), channel_id=1, source_target_pairs={{0,6},{2,0},{4,2},{6,4},{1,7},{3,1},{5,3},{7,5},{8,14},{10,8},{12,... | collective-permute-start | bytes 196616 | tf_op jit(solution)/shard_map/ppermute | solution.py:365
  27.3 7.1 %collective-permute-start.8 = (bf16[16,2048]{1,0:T(8,128)(2,1)S(1)}, bf16[16,2048]{1,0:T(8,128)(2,1)S(1)}, u32[]{:S(2)}, u32[]{:S(2)}) collective-permute-start(bf16[16,2048]{1,0:T(8,128)(2,1)S(1)} %get-tuple-element.14), channel_id=1, source_target_pairs={{0,2},{2,4},{4,6},{6,0},{1,3},{3,5},{5,7},{7,1},{8,10},{10,12},{12... | collective-permute-start | bytes 196616 | tf_op jit(solution)/shard_map/ppermute | solution.py:365
  27.3 37.0 %copy-start = (bf16[16,128,256]{2,1,0:T(8,128)(2,1)}, bf16[16,128,256]{2,1,0:T(8,128)(2,1)S(1)}, u32[]{:S(2)}) copy-start(bf16[16,128,256]{2,1,0:T(8,128)(2,1)S(1)} %collective-permute-done.11.refs_4_.refs_10_) | copy-start | bytes 3145732
  28.2 20.2 %collective-permute-start.15 = (bf16[8,128,256]{2,1,0:T(8,128)(2,1)}, bf16[8,128,256]{2,1,0:T(8,128)(2,1)S(1)}, u32[]{:S(2)}, u32[]{:S(2)}) collective-permute-start(bf16[8,128,256]{2,1,0:T(8,128)(2,1)} %slice.8), channel_id=1, source_target_pairs={{0,8},{8,16},{16,24},{24,0},{1,9},{9,17},{17,25},{25,1},{2,10},{10... | collective-permute-start | bytes 1572872 | tf_op jit(solution)/shard_map/ppermute | solution.py:368
  28.7 35.7 %copy-start.1 = (bf16[16,128,256]{2,1,0:T(8,128)(2,1)}, bf16[16,128,256]{2,1,0:T(8,128)(2,1)S(1)}, u32[]{:S(2)}) copy-start(bf16[16,128,256]{2,1,0:T(8,128)(2,1)S(1)} %collective-permute-done.13.refs_6_.refs_12_) | copy-start | bytes 3145732
  29.6 20.7 %collective-permute-start.17 = (bf16[8,128,256]{2,1,0:T(8,128)(2,1)}, bf16[8,128,256]{2,1,0:T(8,128)(2,1)}, u32[]{:S(2)}, u32[]{:S(2)}) collective-permute-start(bf16[8,128,256]{2,1,0:T(8,128)(2,1)} %slice.9), channel_id=1, source_target_pairs={{0,24},{8,0},{16,8},{24,16},{1,25},{9,1},{17,9},{25,17},{2,26},{10... | collective-permute-start | bytes 1572872 | tf_op jit(solution)/shard_map/ppermute | solution.py:369
  31.7 32.6 %collective-permute-start.12 = (bf16[16,128,256]{2,1,0:T(8,128)(2,1)S(1)}, bf16[16,128,256]{2,1,0:T(8,128)(2,1)}, u32[]{:S(2)}, u32[]{:S(2)}) collective-permute-start(bf16[16,128,256]{2,1,0:T(8,128)(2,1)S(1)} %collective-permute-done.11.refs_4_.refs_10_), channel_id=1, source_target_pairs={{0,1},{1,0},{2,3},{3,2},{4,5},{5,4},{6,7},{7,6},{8,9},{9,8},{10,11... | collective-permute-start | bytes 3145736 | tf_op jit(solution)/shard_map/ppermute | solution.py:370
  34.4 29.9 %collective-permute-start.14 = (bf16[16,128,256]{2,1,0:T(8,128)(2,1)S(1)}, bf16[16,128,256]{2,1,0:T(8,128)(2,1)}, u32[]{:S(2)}, u32[]{:S(2)}) collective-permute-start(bf16[16,128,256]{2,1,0:T(8,128)(2,1)S(1)} %collective-permute-done.13.refs_6_.refs_12_), channel_id=1, source_target_pairs={{0,1},{1,0},{2,3},{3,2},{4,5},{5,4},{6,7},{7,6},{8,9},{9,8},{10,11... | collective-permute-start | bytes 3145736 | tf_op jit(solution)/shard_map/ppermute | solution.py:370
  34.4 4.8 %collective-permute-start.9 = (bf16[16,2048]{1,0:T(8,128)(2,1)S(1)}, bf16[16,2048]{1,0:T(8,128)(2,1)S(1)}, u32[]{:S(2)}, u32[]{:S(2)}) collective-permute-start(bf16[16,2048]{1,0:T(8,128)(2,1)S(1)} %get-tuple-element.15), channel_id=1, source_target_pairs={{0,4},{2,6},{4,0},{6,2},{1,5},{3,7},{5,1},{7,3},{8,12},{10,14},{12... | collective-permute-start | bytes 196616 | tf_op jit(solution)/shard_map/ppermute | solution.py:365
  40.1 24.2 %all-to-all-start = ((bf16[8,16,2048]{2,1,0:T(8,128)(2,1)}), bf16[8,16,2048]{2,1,0:T(8,128)(2,1)S(1)}, u32[]{:S(2)}, u32[]{:S(2)}) async-start(bf16[8,16,2048]{2,1,0:T(8,128)(2,1)} %middle.1), calls=%async_computation | async-start | bytes 1048576 | tf_op jit(solution)/shard_map/all_to_all | solution.py:346
  48.3 16.0 %copy-start.2 = (bf16[8,128,256]{2,1,0:T(8,128)(2,1)}, bf16[8,128,256]{2,1,0:T(8,128)(2,1)S(1)}, u32[]{:S(2)}) copy-start(bf16[8,128,256]{2,1,0:T(8,128)(2,1)S(1)} %collective-permute-done.15.refs_8_) | copy-start | bytes 1572868
  48.3 16.0 %collective-permute-start.16 = (bf16[8,128,256]{2,1,0:T(8,128)(2,1)S(1)}, bf16[8,128,256]{2,1,0:T(8,128)(2,1)}, u32[]{:S(2)}, u32[]{:S(2)}) collective-permute-start(bf16[8,128,256]{2,1,0:T(8,128)(2,1)S(1)} %collective-permute-done.15.refs_8_), channel_id=1, source_target_pairs={{0,1},{1,0},{2,3},{3,2},{4,5},{5,4},{6,7},{7,6},{8,9},{9,8},{10,11... | collective-permute-start | bytes 1572872 | tf_op jit(solution)/shard_map/ppermute | solution.py:371
  50.3 14.0 %collective-permute-start.18 = (bf16[8,128,256]{2,1,0:T(8,128)(2,1)}, bf16[8,128,256]{2,1,0:T(8,128)(2,1)}, u32[]{:S(2)}, u32[]{:S(2)}) collective-permute-start(bf16[8,128,256]{2,1,0:T(8,128)(2,1)} %collective-permute-done.17.refs_14_), channel_id=1, source_target_pairs={{0,1},{1,0},{2,3},{3,2},{4,5},{5,4},{6,7},{7,6},{8,9},{9,8},{10,11... | collective-permute-start | bytes 1572872 | tf_op jit(solution)/shard_map/ppermute | solution.py:371

commit v4 on v3

--- a/solution.py
+++ b/solution.py
@@ -18,8 +18,8 @@
 Z, X, Y, C = 8, 4, 4, 2
 TP = Y * C
 SHARE = ROWS // TP
-RETAIN_LIMIT = 20 * 2**20
-MIXER_LIMIT = 20 * 2**20
+RETAIN_LIMIT = 14 * 2**20
+MIXER_LIMIT = 14 * 2**20
 F32 = jnp.float32
 BF16 = jnp.bfloat16
 
@@ -39,19 +39,19 @@
         copy.wait()
 
 
-def pack_kernel(up, down, packed, sems):
+def pack_kernel(up, down, packed_up, packed_down, sems):
     at = pl.multiple_of(lax.axis_index("c") * 128, 128)
     copies = [
         pltpu.make_async_copy(
             up.at[pl.ds(8 * i, 8), :, pl.ds(at, 128)],
-            packed.at[pl.ds(0, 8), :, pl.ds(128 * i, 128)],
+            packed_up.at[:, :, pl.ds(128 * i, 128)],
             sems.at[i],
         )
         for i in range(2)
     ]
     copies += [
         pltpu.make_async_copy(
-            down.at[pl.ds(at, 128), pl.ds(256 * j, 256)], packed.at[8 + j], sems.at[2 + j]
+            down.at[pl.ds(at, 128), pl.ds(256 * j, 256)], packed_down.at[j], sems.at[2 + j]
         )
         for j in range(8)
     ]
@@ -61,9 +61,9 @@
 def pack(w_up, w_down):
     return pl.pallas_call(
         pack_kernel,
-        out_shape=jax.ShapeDtypeStruct((16, 128, 256), BF16),
+        out_shape=[jax.ShapeDtypeStruct((8, 128, 256), BF16)] * 2,
         in_specs=[pl.BlockSpec(memory_space=pl.ANY)] * 2,
-        out_specs=pl.BlockSpec(memory_space=pltpu.VMEM),
+        out_specs=[pl.BlockSpec(memory_space=pltpu.VMEM)] * 2,
         scratch_shapes=[pltpu.SemaphoreType.DMA((10,))],
         compiler_params=pltpu.CompilerParams(vmem_limit_bytes=8 * 2**20),
         name="pack",
@@ -89,15 +89,16 @@
     return 2 * lax.rem(y + (Y - k), Y) + (1 - c if other else c)
 
 
+def part(ref, i):
+    return ref.at[i // PER_HEAD, pl.ds((i % PER_HEAD) * STEP, STEP)]
+
+
 def retain_kernel(decays, *refs):
     blocks = refs[:TP]
     states, wq, wk, wv, wg, wo, mix_gain, head_gain, cosine, sines = refs[TP : TP + 10]
-    new_states, mine, others, own = refs[TP + 10 : TP + 14]
-    tokens, weights, w_out, old, new, qt, kt, ret, shares = refs[TP + 14 : TP + 23]
-    w_sems, in_sems, out_sems = refs[TP + 23 :]
-
-    def part(ref, i):
-        return ref.at[i // PER_HEAD, pl.ds((i % PER_HEAD) * STEP, STEP)]
+    mine, others, own, keys, values = refs[TP + 10 : TP + 15]
+    tokens, weights, w_out, old, qt, ret, shares = refs[TP + 15 : TP + 22]
+    w_sems, in_sems = refs[TP + 22 :]
 
     first_head = 2 * (lax.axis_index("y") * C + lax.axis_index("c"))
     w_copies = [
@@ -107,10 +108,6 @@
     wo_copy = pltpu.make_async_copy(wo, w_out, w_sems.at[4])
     in_copies = [
         pltpu.make_async_copy(part(states, i), part(old, i), in_sems.at[i]) for i in range(CHUNKS)
-    ]
-    out_copies = [
-        pltpu.make_async_copy(part(new, i), part(new_states, i), out_sems.at[i])
-        for i in range(CHUNKS)
     ]
     for copy in w_copies + in_copies + [wo_copy]:
         copy.start()
@@ -143,13 +140,12 @@
         return jnp.concatenate(rows, axis=0)
 
     qt[...] = turned(projected[:, 0:128].T) * HEAD**-0.5
-    kt[...] = turned(projected[:, 128:256].T)
-    vt = projected[:, 256:384].T
+    keys[...] = turned(projected[:, 128:256].T)
+    values[...] = projected[:, 256:384].T
     gating = projected[:, 384:512]
 
     for h in range(2):
-        values = vt[h * HEAD : (h + 1) * HEAD]
-        decay = decays[first_head + h]
+        at = slice(h * HEAD, (h + 1) * HEAD)
         total = jnp.zeros((HEAD, ROWS), F32)
         for i in range(h * PER_HEAD, (h + 1) * PER_HEAD):
             in_copies[i].wait()
@@ -157,13 +153,11 @@
 
             def step(s, total):
                 k = first + s
-                row = h * HEAD + k
-                fresh = decay * old[h, k] + kt[pl.ds(row, 1), :] * values
-                new[h, k] = fresh
-                return total + qt[pl.ds(row, 1), :] * fresh
+                return total + qt[pl.ds(h * HEAD + k, 1), :] * old[h, k]
 
             total = lax.fori_loop(0, STEP, step, total, unroll=8)
-            out_copies[i].start()
+        match = jnp.sum(qt[at, :] * keys[at, :], axis=0, keepdims=True)
+        total = decays[first_head + h] * total + match * values[at, :]
         center = total - jnp.mean(total, axis=0, keepdims=True)
         spread = jnp.mean(center * center, axis=0, keepdims=True)
         ret[h * HEAD : (h + 1) * HEAD, :] = center * lax.rsqrt(spread + EPSILON)
@@ -177,8 +171,6 @@
     others[...] = shares[:, 1 - core].astype(BF16)
     at = pl.multiple_of(place(0, False) * SHARE, SHARE)
     own[...] = jnp.concatenate([tokens[j, pl.ds(at, SHARE), :] for j in range(TP)], axis=1)
-    for copy in out_copies:
-        copy.wait()
 
 
 def retain(blocks, states, wq, wk, wv, wg, wo, mix_gain, head_gain):
@@ -187,26 +179,24 @@
     return pl.pallas_call(
         retain_kernel,
         out_shape=(
-            jax.ShapeDtypeStruct((2, HEAD, HEAD, ROWS), F32),
             jax.ShapeDtypeStruct((Y, SHARE, D), F32),
             jax.ShapeDtypeStruct((Y, SHARE, D), BF16),
             jax.ShapeDtypeStruct((SHARE, D), BF16),
+            jax.ShapeDtypeStruct((128, ROWS), F32),
+            jax.ShapeDtypeStruct((128, ROWS), F32),
         ),
         in_specs=[pl.BlockSpec(memory_space=pltpu.SMEM)]
         + [vmem] * TP + [any_space] * 6 + [vmem] * 4,
-        out_specs=(any_space, vmem, vmem, vmem),
+        out_specs=(vmem,) * 5,
         scratch_shapes=[
             pltpu.VMEM((TP, ROWS, 256), BF16),
             pltpu.VMEM((D, 512), BF16),
             pltpu.VMEM((128, D), BF16),
             pltpu.VMEM((2, HEAD, HEAD, ROWS), F32),
-            pltpu.VMEM((2, HEAD, HEAD, ROWS), F32),
-            pltpu.VMEM((128, ROWS), F32),
             pltpu.VMEM((128, ROWS), F32),
             pltpu.VMEM((128, ROWS), F32),
             pltpu.VMEM((Y, C, SHARE, D), F32),
             pltpu.SemaphoreType.DMA((5,)),
-            pltpu.SemaphoreType.DMA((CHUNKS,)),
             pltpu.SemaphoreType.DMA((CHUNKS,)),
         ],
         compiler_params=pltpu.CompilerParams(vmem_limit_bytes=RETAIN_LIMIT),
@@ -217,6 +207,53 @@
     )
 
 
+def update_kernel(decays, keys, values, states, new_states, old, new, in_sems, out_sems):
+    first_head = 2 * place(0, False)
+    in_copies = [
+        pltpu.make_async_copy(part(states, i), part(old, i), in_sems.at[i]) for i in range(CHUNKS)
+    ]
+    out_copies = [
+        pltpu.make_async_copy(part(new, i), part(new_states, i), out_sems.at[i])
+        for i in range(CHUNKS)
+    ]
+    for copy in in_copies:
+        copy.start()
+    for i in range(CHUNKS):
+        h = i // PER_HEAD
+        value = values[h * HEAD : (h + 1) * HEAD, :]
+        decay = decays[first_head + h]
+        in_copies[i].wait()
+
+        def step(s, carry):
+            k = (i % PER_HEAD) * STEP + s
+            new[h, k] = decay * old[h, k] + keys[pl.ds(h * HEAD + k, 1), :] * value
+            return carry
+
+        lax.fori_loop(0, STEP, step, 0, unroll=8)
+        out_copies[i].start()
+    for copy in out_copies:
+        copy.wait()
+
+
+def update(keys, values, states):
+    any_space = pl.BlockSpec(memory_space=pl.ANY)
+    vmem = pl.BlockSpec(memory_space=pltpu.VMEM)
+    return pl.pallas_call(
+        update_kernel,
+        out_shape=jax.ShapeDtypeStruct((2, HEAD, HEAD, ROWS), F32),
+        in_specs=[pl.BlockSpec(memory_space=pltpu.SMEM), vmem, vmem, any_space],
+        out_specs=any_space,
+        scratch_shapes=[
+            pltpu.VMEM((2, HEAD, HEAD, ROWS), F32),
+            pltpu.VMEM((2, HEAD, HEAD, ROWS), F32),
+            pltpu.SemaphoreType.DMA((CHUNKS,)),
+            pltpu.SemaphoreType.DMA((CHUNKS,)),
+        ],
+        compiler_params=pltpu.CompilerParams(vmem_limit_bytes=RETAIN_LIMIT),
+        name="update",
+    )(in_hbm(DECAYS), keys, values, in_hbm(states))
+
+
 def pair_kernel(mine, others, *outs):
     y = lax.axis_index("y")
     for k in range(Y):
@@ -258,9 +295,11 @@
 
 
 def mixer_kernel(*refs):
-    rows, channel_gain, own_up, own_down = refs[:4]
+    everyone, channel_gain, own_up, own_down = refs[:4]
     ups, downs = refs[4:10], refs[10:16]
-    out, up, down, sems = refs[16:]
+    out, rows, up, down, sems = refs[16:]
+    row_copy = pltpu.make_async_copy(everyone, rows, sems.at[27])
+    row_copy.start()
     up_copies = [pltpu.make_async_copy(own_up, up.at[:, :, pl.ds(0, 256)], sems.at[0])]
     down_copies = [
         pltpu.make_async_copy(
@@ -287,6 +326,7 @@
         )
     for copy in up_copies + down_copies:
         copy.start()
+    row_copy.wait()
     squares = jnp.zeros((ROWS, 256), F32)
     scaled = []
     for j in range(TP):
@@ -323,17 +363,18 @@
     return pl.pallas_call(
         mixer_kernel,
         out_shape=pltpu.VMEM((Z, TP, SHARE, 256), BF16),
-        in_specs=[vmem] * 2 + [any_space] * 14,
+        in_specs=[any_space, vmem] + [any_space] * 14,
         out_specs=vmem,
         scratch_shapes=[
+            pltpu.VMEM((Z, SHARE, D), BF16),
             pltpu.VMEM((16, 128, 1024), BF16),
             pltpu.VMEM((8, 1024, 256), BF16),
-            pltpu.SemaphoreType.DMA((27,)),
+            pltpu.SemaphoreType.DMA((28,)),
         ],
         compiler_params=pltpu.CompilerParams(vmem_limit_bytes=MIXER_LIMIT),
         name="mixer",
     )(
-        in_vmem(rows), in_hbm(channel_gain.reshape(16, 128)), in_hbm(own_up.reshape(16, 128, 256)),
+        in_hbm(rows), in_hbm(channel_gain.reshape(16, 128)), in_hbm(own_up.reshape(16, 128, 256)),
         in_hbm(own_down), *map(in_hbm, ups), *map(in_hbm, downs),
     )
 
@@ -352,27 +393,32 @@
 ):
     swap = [(0, 1), (1, 0)]
     blocks = [tokens] + [lax.ppermute(tokens, "y", shift(Y, by)) for by in (1, 2, 3)]
-    packed = pack(w_up, w_down)
-    left = lax.ppermute(packed, "x", shift(X, 1))
-    right = lax.ppermute(packed, "x", shift(X, 3))
+    packed_up, packed_down = pack(w_up, w_down)
+    left_up = lax.ppermute(packed_up, "x", shift(X, 1))
+    right_down = lax.ppermute(packed_down, "x", shift(X, 3))
     blocks += [lax.ppermute(block, "c", swap) for block in blocks]
-    new_states, mine, others, own = retain(
-        blocks, states.transpose(1, 2, 3, 0), w_query, w_key, w_value, w_gate, w_output,
-        mix_gain, head_gain,
+    states = states.transpose(1, 2, 3, 0)
+    mine, others, own, keys, values = retain(
+        blocks, states, w_query, w_key, w_value, w_gate, w_output, mix_gain, head_gain
     )
     others = lax.ppermute(others, "c", swap)
+    right_up = lax.ppermute(packed_up, "x", shift(X, 3))
+    left_down = lax.ppermute(packed_down, "x", shift(X, 1))
     parts = pair(mine, others)
     parts = [parts[0]] + [lax.ppermute(parts[k], "y", shift(Y, k)) for k in (1, 2, 3)]
     middle = middle_rows(own, parts)
     everyone = to_all(middle, "z")
-    far_up = lax.ppermute(left[:8], "x", shift(X, 1))
-    far_down = lax.ppermute(right[8:], "x", shift(X, 3))
-    left_other, right_other = [lax.ppermute(w, "c", swap) for w in (left, right)]
+    far_up = lax.ppermute(left_up, "x", shift(X, 1))
+    far_down = lax.ppermute(right_down, "x", shift(X, 3))
+    new_states = update(keys, values, states)
+    near_other = [lax.ppermute(w, "c", swap) for w in (left_up, right_down)]
+    near_other += [lax.ppermute(w, "c", swap) for w in (right_up, left_down)]
+    far_up, far_down, *near_other = lax.optimization_barrier((far_up, far_down, *near_other))
     far_other = [lax.ppermute(w, "c", swap) for w in (far_up, far_down)]
     down = mixer(
         everyone, channel_gain, w_up, w_down,
-        (left, left_other, right, right_other, far_up, far_other[0]),
-        (left, left_other, right, right_other, far_down, far_other[1]),
+        (left_up, near_other[0], right_up, near_other[2], far_up, far_other[0]),
+        (left_down, near_other[3], right_down, near_other[1], far_down, far_other[1]),
     )
     down = to_all(down.reshape(Z * TP, SHARE, 256), ("z", "y", "c"))
     layer_out = jnp.sum(down.reshape(Z, ROWS, 256).astype(F32), axis=0).astype(BF16)

time: 95.7 us -> 102 us (1.066)
  waiting for transfers between devices: 17.9 us -> 46.4 us
  blocking collectives: 25.3 us -> 0 us
  Pallas kernels: 13.4 us -> 17.3 us
    all_to_all x1 -> x0, blocking collectives: 25.3 us -> none  [to_all(): return lax.all_to_all(array, axes, 0, 0, tiled=True)]
    all_to_all x1 -> x2, waiting for transfers between devices: 13.9 us -> 28.2 us  [to_all(): return lax.all_to_all(array, axes, 0, 0, tiled=True)]
    ppermute x3, waiting for transfers between devices: 1.66 us -> 10.2 us  [local(): lax.ppermute(parts[k], 'y', shift(Y, k))]
    ppermute x3, starting transfers between devices: 5.41 us -> 0.09 us  [local(): lax.ppermute(parts[k], 'y', shift(Y, k))]
    ppermute x6 -> x10, waiting for transfers between devices: 0.02 us -> 5.13 us  [the longest x1 3.07 us: local(): left_down = lax.ppermute(packed_down, 'x', shift(X, 1))]
    all_to_all x1 -> x2, starting transfers between devices: 8.24 us -> 12.8 us  [to_all(): return lax.all_to_all(array, axes, 0, 0, tiled=True)]
    ppermute x6 -> x10, starting transfers between devices: 8.77 us -> 12.2 us  [the longest x1 3.37 us: local(): right_up = lax.ppermute(packed_up, 'x', shift(X, 3))]
    pallas_call x2 -> x3, Pallas kernels: 7.48 us -> 10.4 us  [the longest x1 5.03 us: retain(): pl.pallas_call(retain_kernel, out_shape=(jax.ShapeDtypeStruct((Y, SHARE,...]
  transfers between devices with their start and end apart: 20 -> 25, of which waited for: 6 -> 9; matrix products, arithmetic and copies ran while one was open for 2% -> 0% of each run, Pallas kernels for 7% -> 10%
where the time goes in v4:
time: 102 us
  waiting for transfers between devices  46.4 us (45%)
  starting transfers between devices  35.8 us (35%)
  Pallas kernels  17.3 us (17%)
    all_to_all x2, waiting for transfers between devices, to_all(): return lax.all_to_all(array, axes, 0, 0, tiled=True)  28.2 us
    all_to_all x2, starting transfers between devices, to_all(): return lax.all_to_all(array, axes, 0, 0, tiled=True)  12.8 us
    ppermute x3, waiting for transfers between devices, local(): lax.ppermute(parts[k], 'y', shift(Y, k))  10.2 us
    pallas_call x1, Pallas kernels, mixer(): pl.pallas_call(mixer_kernel, out_shape=pltpu.VMEM((Z, TP, SHARE, 256), BF...  6 us
    ppermute x4, starting transfers between devices, local(): blocks += [lax.ppermute(block, 'c', swap) for block in blocks]  5.43 us
    pallas_call x1, Pallas kernels, retain(): pl.pallas_call(retain_kernel, out_shape=(jax.ShapeDtypeStruct((Y, SHARE,...  5.03 us
    pallas_call x1, Pallas kernels, update(): pl.pallas_call(update_kernel, out_shape=jax.ShapeDtypeStruct((2, HEAD, HE...  4.16 us
    ppermute x3, starting transfers between devices, local(): lax.ppermute(tokens, 'y', shift(Y, by))  3.77 us
  transfers between devices with their start and end apart: 25, of which 9 were waited for; matrix products, arithmetic and copies ran while one was open for 0% of the time, Pallas kernels for 10%

profile of v4, /device:TPU:1, one launch (start us, length us, event | category | flops | bytes accessed | tf_op | source)
XLA Modules:
  0.0 101.9 jit_solution(4371748029318140590)
XLA Ops:
  0.6 1.2 %pack.1 = (bf16[8,128,256]{2,1,0:T(8,128)(2,1)S(1)}, bf16[8,128,256]{2,1,0:T(8,128)(2,1)S(1)}) custom-call(bf16[16,128,256]{2,1,0:T(8,128)(2,1)} %bitcast.12, bf16[256,2048]{1,0:T(8,128)(2,1)} %refs_3_.1), custom_call_target="tpu_custom_call" | custom-call | tf_op jit(solution)/shard_map/pack/pallas_call | solution.py:62
  1.9 3.4 %collective-permute-start.17 = (bf16[8,128,256]{2,1,0:T(8,128)(2,1)S(1)}, bf16[8,128,256]{2,1,0:T(8,128)(2,1)S(1)}, u32[]{:S(2)}, u32[]{:S(2)}) collective-permute-start(bf16[8,128,256]{2,1,0:T(8,128)(2,1)S(1)} %get-tuple-element.26), channel_id=1, source_target_pairs={{0,24},{8,0},{16,8},{24,16},{1,25},{9,1},{17,9},{25,17},{2,26},{10... | collective-permute-start | bytes 1572872 | tf_op jit(solution)/shard_map/ppermute | solution.py:405
  5.2 2.7 %collective-permute-start.2 = (bf16[128,256]{1,0:T(8,128)(2,1)}, bf16[128,256]{1,0:T(8,128)(2,1)S(1)}, u32[]{:S(2)}, u32[]{:S(2)}) collective-permute-start(bf16[128,256]{1,0:T(8,128)(2,1)} %refs_0_.1), channel_id=1, source_target_pairs={{0,6},{2,0},{4,2},{6,4},{1,7},{3,1},{5,3},{7,5},{8,14},{10,8},{12,... | collective-permute-start | bytes 196616 | tf_op jit(solution)/shard_map/ppermute | solution.py:395
  8.0 0.3 collective-permute-start.1
  8.3 0.7 collective-permute-start
  9.0 1.8 %collective-permute-start.3 = (bf16[128,256]{1,0:T(8,128)(2,1)}, bf16[128,256]{1,0:T(8,128)(2,1)S(1)}, u32[]{:S(2)}, u32[]{:S(2)}) collective-permute-start(bf16[128,256]{1,0:T(8,128)(2,1)} %refs_0_.1), channel_id=1, source_target_pairs={{0,1},{1,0},{2,3},{3,2},{4,5},{5,4},{6,7},{7,6},{8,9},{9,8},{10,11... | collective-permute-start | bytes 196616 | tf_op jit(solution)/shard_map/ppermute | solution.py:399
  10.8 0.6 collective-permute-start.6
  11.4 1.4 %collective-permute-done.1.refs_2_ = bf16[128,256]{1,0:T(8,128)(2,1)S(1)} collective-permute-done((bf16[128,256]{1,0:T(8,128)(2,1)}, bf16[128,256]{1,0:T(8,128)(2,1)S(1)}, u32[]{:S(2)}, u32[]{:S(2)}) %collective-permute-start.1) | collective-permute-done | bytes 65568 | tf_op jit(solution)/shard_map/ppermute | solution.py:395
  12.9 2.3 %collective-permute-start.5 = (bf16[128,256]{1,0:T(8,128)(2,1)S(1)}, bf16[128,256]{1,0:T(8,128)(2,1)S(1)}, u32[]{:S(2)}, u32[]{:S(2)}) collective-permute-start(bf16[128,256]{1,0:T(8,128)(2,1)S(1)} %collective-permute-done.1.refs_2_), channel_id=1, source_target_pairs={{0,1},{1,0},{2,3},{3,2},{4,5},{5,4},{6,7},{7,6},{8,9},{9,8},{10,11... | collective-permute-start | bytes 196616 | tf_op jit(solution)/shard_map/ppermute | solution.py:399
  15.2 0.7 collective-permute-start.4
  16.1 2.6 %collective-permute-start.13 = (bf16[8,128,256]{2,1,0:T(8,128)(2,1)S(1)}, bf16[8,128,256]{2,1,0:T(8,128)(2,1)S(1)}, u32[]{:S(2)}, u32[]{:S(2)}) collective-permute-start(bf16[8,128,256]{2,1,0:T(8,128)(2,1)S(1)} %get-tuple-element.27), channel_id=1, source_target_pairs={{0,24},{8,0},{16,8},{24,16},{1,25},{9,1},{17,9},{25,17},{2,26},{10... | collective-permute-start | bytes 1572872 | tf_op jit(solution)/shard_map/ppermute | solution.py:398
  18.7 0.6 collective-permute-start.18
  19.3 5.0 %retain.1 = (f32[4,16,2048]{2,1,0:T(8,128)S(1)}, bf16[4,16,2048]{2,1,0:T(8,128)(2,1)S(1)}, bf16[16,2048]{1,0:T(8,128)(2,1)S(1)}, f32[128,128]{1,0:T(8,128)S(1)}, f32[128,128]{1,0:T(8,128)S(1)}) custom-call(f32[16]{0:T(128)} %constant.9.clone.decays, bf16[128,256]{1,0:T(8,128)(2,1)} %refs_0_.1, bf16[128,256]{1,0:T(8,128)(2,1)S(1)} %collective-permute-done.refs_1_, ...), custom_call_target="tpu_custom_call" | custom-call | tf_op jit(solution)/shard_map/retain/pallas_call | solution.py:179
  24.6 1.4 %collective-permute-done.7.others = bf16[4,16,2048]{2,1,0:T(8,128)(2,1)S(1)} collective-permute-done((bf16[4,16,2048]{2,1,0:T(8,128)(2,1)S(1)}, bf16[4,16,2048]{2,1,0:T(8,128)(2,1)S(1)}, u32[]{:S(2)}, u32[]{:S(2)}) %collective-permute-start.7) | collective-permute-done | bytes 262176 | tf_op jit(solution)/shard_map/ppermute | solution.py:404
  26.1 4.7 %collective-permute-done.8.refs_0_ = bf16[16,2048]{1,0:T(8,128)(2,1)S(1)} collective-permute-done((bf16[16,2048]{1,0:T(8,128)(2,1)S(1)}, bf16[16,2048]{1,0:T(8,128)(2,1)S(1)}, u32[]{:S(2)}, u32[]{:S(2)}) %collective-permute-start.8) | collective-permute-done | bytes 65568 | tf_op jit(solution)/shard_map/ppermute | solution.py:408
  30.7 4.6 %collective-permute-done.9.refs_1_ = bf16[16,2048]{1,0:T(8,128)(2,1)S(1)} collective-permute-done((bf16[16,2048]{1,0:T(8,128)(2,1)S(1)}, bf16[16,2048]{1,0:T(8,128)(2,1)S(1)}, u32[]{:S(2)}, u32[]{:S(2)}) %collective-permute-start.9) | collective-permute-done | bytes 65568 | tf_op jit(solution)/shard_map/ppermute | solution.py:408
  35.4 2.5 %collective-permute-start.15 = (bf16[8,128,256]{2,1,0:T(8,128)(2,1)S(1)}, bf16[8,128,256]{2,1,0:T(8,128)(2,1)}, u32[]{:S(2)}, u32[]{:S(2)}) collective-permute-start(bf16[8,128,256]{2,1,0:T(8,128)(2,1)S(1)} %collective-permute-done.11.refs_4_), channel_id=1, source_target_pairs={{0,1},{1,0},{2,3},{3,2},{4,5},{5,4},{6,7},{7,6},{8,9},{9,8},{10,11... | collective-permute-start | bytes 1572872 | tf_op jit(solution)/shard_map/ppermute | solution.py:414
  37.8 0.9 collective-permute-done.10.refs_2_
  38.8 3.1 %collective-permute-done.19.refs_10_ = bf16[8,128,256]{2,1,0:T(8,128)(2,1)S(1)} collective-permute-done((bf16[8,128,256]{2,1,0:T(8,128)(2,1)S(1)}, bf16[8,128,256]{2,1,0:T(8,128)(2,1)S(1)}, u32[]{:S(2)}, u32[]{:S(2)}) %collective-permute-start.19) | collective-permute-done | bytes 524320 | tf_op jit(solution)/shard_map/ppermute | solution.py:406
  41.8 0.9 collective-permute-start.20
  42.8 2.1 %collective-permute-start.14 = (bf16[8,128,256]{2,1,0:T(8,128)(2,1)S(1)}, bf16[8,128,256]{2,1,0:T(8,128)(2,1)}, u32[]{:S(2)}, u32[]{:S(2)}) collective-permute-start(bf16[8,128,256]{2,1,0:T(8,128)(2,1)S(1)} %collective-permute-done.13.refs_12_), channel_id=1, source_target_pairs={{0,24},{8,0},{16,8},{24,16},{1,25},{9,1},{17,9},{25,17},{2,26},{10... | collective-permute-start | bytes 1572872 | tf_op jit(solution)/shard_map/ppermute | solution.py:412
  44.9 0.8 middle.1
  45.7 8.2 %all-to-all-start = ((bf16[8,16,2048]{2,1,0:T(8,128)(2,1)}), bf16[8,16,2048]{2,1,0:T(8,128)(2,1)S(1)}, u32[]{:S(2)}, u32[]{:S(2)}) async-start(bf16[8,16,2048]{2,1,0:T(8,128)(2,1)} %middle.1), calls=%async_computation | async-start | bytes 1048576 | tf_op jit(solution)/shard_map/all_to_all | solution.py:387
  53.9 2.0 %collective-permute-done.14.refs_14_ = bf16[8,128,256]{2,1,0:T(8,128)(2,1)} collective-permute-done((bf16[8,128,256]{2,1,0:T(8,128)(2,1)S(1)}, bf16[8,128,256]{2,1,0:T(8,128)(2,1)}, u32[]{:S(2)}, u32[]{:S(2)}) %collective-permute-start.14) | collective-permute-done | bytes 524320 | tf_op jit(solution)/shard_map/ppermute | solution.py:412
  56.0 1.3 %collective-permute-start.21 = (bf16[8,128,256]{2,1,0:T(8,128)(2,1)}, bf16[8,128,256]{2,1,0:T(8,128)(2,1)S(1)}, u32[]{:S(2)}, u32[]{:S(2)}) collective-permute-start(bf16[8,128,256]{2,1,0:T(8,128)(2,1)} %collective-permute-done.12.refs_8_), channel_id=1, source_target_pairs={{0,1},{1,0},{2,3},{3,2},{4,5},{5,4},{6,7},{7,6},{8,9},{9,8},{10,11... | collective-permute-start | bytes 1572872 | tf_op jit(solution)/shard_map/ppermute | solution.py:417
  57.3 14.6 %all-to-all-done.refs_0_ = bf16[8,16,2048]{2,1,0:T(8,128)(2,1)S(1)} async-done(((bf16[8,16,2048]{2,1,0:T(8,128)(2,1)}), bf16[8,16,2048]{2,1,0:T(8,128)(2,1)S(1)}, u32[]{:S(2)}, u32[]{:S(2)}) %all-to-all-start) | async-done | bytes 524320 | tf_op jit(solution)/shard_map/all_to_all | solution.py:387
  71.9 0.7 copy-done
  72.8 6.0 %mixer.1 = bf16[8,8,16,256]{3,2,1,0:T(8,128)(2,1)} custom-call(bf16[8,16,2048]{2,1,0:T(8,128)(2,1)} %copy-done, bf16[16,128]{1,0:T(8,128)(2,1)} %bitcast.17, bf16[16,128,256]{2,1,0:T(8,128)(2,1)} %bitcast.13, bf16[256,2048]{1,0:T(8,128)(2,1)} %refs_3_.1, bf16[8,128,256]{2,1,0:T(8,128)(2,1)} %copy-done.2, ...), custom_call_target="tpu_custom_call" | custom-call | tf_op jit(solution)/shard_map/mixer/pallas_call | solution.py:363
  78.8 4.6 %all-to-all-start.1 = ((bf16[64,16,256]{2,1,0:T(8,128)(2,1)}), bf16[64,16,256]{2,1,0:T(8,128)(2,1)S(1)}, u32[]{:S(2)}, u32[]{:S(2)}) async-start(bf16[64,16,256]{2,1,0:T(8,128)(2,1)} %bitcast.5), calls=%async_computation.1 | async-start | bytes 1048576 | tf_op jit(solution)/shard_map/all_to_all | solution.py:387
  83.4 4.2 %update.1 = f32[2,64,64,128]{3,2,1,0:T(8,128)} custom-call(f32[16]{0:T(128)} %constant.9.clone.decays, f32[128,128]{1,0:T(8,128)S(1)} %get-tuple-element.34.keys, f32[128,128]{1,0:T(8,128)S(1)} %get-tuple-element.35.values, f32[2,64,64,128]{3,2,1,0:T(8,128)} %bitcast.11), custom_call_target="tpu_custom_call" | custom-call | tf_op jit(solution)/shard_map/update/pallas_call | solution.py:241
  87.6 13.6 %all-to-all-done.1 = bf16[64,16,256]{2,1,0:T(8,128)(2,1)S(1)} async-done(((bf16[64,16,256]{2,1,0:T(8,128)(2,1)}), bf16[64,16,256]{2,1,0:T(8,128)(2,1)S(1)}, u32[]{:S(2)}, u32[]{:S(2)}) %all-to-all-start.1) | async-done | bytes 524320 | tf_op jit(solution)/shard_map/all_to_all | solution.py:387
  101.2 0.7 bitcast_reduce_fusion
  (39 shorter events, 0.9 us)
Async XLA Ops:
  1.9 16.8 %collective-permute-start.17 = (bf16[8,128,256]{2,1,0:T(8,128)(2,1)S(1)}, bf16[8,128,256]{2,1,0:T(8,128)(2,1)S(1)}, u32[]{:S(2)}, u32[]{:S(2)}) collective-permute-start(bf16[8,128,256]{2,1,0:T(8,128)(2,1)S(1)} %get-tuple-element.26), channel_id=1, source_target_pairs={{0,24},{8,0},{16,8},{24,16},{1,25},{9,1},{17,9},{25,17},{2,26},{10... | collective-permute-start | bytes 1572872 | tf_op jit(solution)/shard_map/ppermute | solution.py:405
  5.2 5.6 %collective-permute-start.2 = (bf16[128,256]{1,0:T(8,128)(2,1)}, bf16[128,256]{1,0:T(8,128)(2,1)S(1)}, u32[]{:S(2)}, u32[]{:S(2)}) collective-permute-start(bf16[128,256]{1,0:T(8,128)(2,1)} %refs_0_.1), channel_id=1, source_target_pairs={{0,6},{2,0},{4,2},{6,4},{1,7},{3,1},{5,3},{7,5},{8,14},{10,8},{12,... | collective-permute-start | bytes 196616 | tf_op jit(solution)/shard_map/ppermute | solution.py:395
  8.0 4.9 %collective-permute-start.1 = (bf16[128,256]{1,0:T(8,128)(2,1)}, bf16[128,256]{1,0:T(8,128)(2,1)S(1)}, u32[]{:S(2)}, u32[]{:S(2)}) collective-permute-start(bf16[128,256]{1,0:T(8,128)(2,1)} %refs_0_.1), channel_id=1, source_target_pairs={{0,4},{2,6},{4,0},{6,2},{1,5},{3,7},{5,1},{7,3},{8,12},{10,14},{12... | collective-permute-start | bytes 196616 | tf_op jit(solution)/shard_map/ppermute | solution.py:395
  8.3 6.9 %collective-permute-start = (bf16[128,256]{1,0:T(8,128)(2,1)}, bf16[128,256]{1,0:T(8,128)(2,1)S(1)}, u32[]{:S(2)}, u32[]{:S(2)}) collective-permute-start(bf16[128,256]{1,0:T(8,128)(2,1)} %refs_0_.1), channel_id=1, source_target_pairs={{0,2},{2,4},{4,6},{6,0},{1,3},{3,5},{5,7},{7,1},{8,10},{10,12},{12... | collective-permute-start | bytes 196616 | tf_op jit(solution)/shard_map/ppermute | solution.py:395
  9.0 6.9 %collective-permute-start.3 = (bf16[128,256]{1,0:T(8,128)(2,1)}, bf16[128,256]{1,0:T(8,128)(2,1)S(1)}, u32[]{:S(2)}, u32[]{:S(2)}) collective-permute-start(bf16[128,256]{1,0:T(8,128)(2,1)} %refs_0_.1), channel_id=1, source_target_pairs={{0,1},{1,0},{2,3},{3,2},{4,5},{5,4},{6,7},{7,6},{8,9},{9,8},{10,11... | collective-permute-start | bytes 196616 | tf_op jit(solution)/shard_map/ppermute | solution.py:399
  10.8 5.1 %collective-permute-start.6 = (bf16[128,256]{1,0:T(8,128)(2,1)S(1)}, bf16[128,256]{1,0:T(8,128)(2,1)S(1)}, u32[]{:S(2)}, u32[]{:S(2)}) collective-permute-start(bf16[128,256]{1,0:T(8,128)(2,1)S(1)} %collective-permute-done.2.refs_3_), channel_id=1, source_target_pairs={{0,1},{1,0},{2,3},{3,2},{4,5},{5,4},{6,7},{7,6},{8,9},{9,8},{10,11... | collective-permute-start | bytes 196616 | tf_op jit(solution)/shard_map/ppermute | solution.py:399
  12.9 3.2 %collective-permute-start.5 = (bf16[128,256]{1,0:T(8,128)(2,1)S(1)}, bf16[128,256]{1,0:T(8,128)(2,1)S(1)}, u32[]{:S(2)}, u32[]{:S(2)}) collective-permute-start(bf16[128,256]{1,0:T(8,128)(2,1)S(1)} %collective-permute-done.1.refs_2_), channel_id=1, source_target_pairs={{0,1},{1,0},{2,3},{3,2},{4,5},{5,4},{6,7},{7,6},{8,9},{9,8},{10,11... | collective-permute-start | bytes 196616 | tf_op jit(solution)/shard_map/ppermute | solution.py:399
  15.2 4.1 %collective-permute-start.4 = (bf16[128,256]{1,0:T(8,128)(2,1)S(1)}, bf16[128,256]{1,0:T(8,128)(2,1)S(1)}, u32[]{:S(2)}, u32[]{:S(2)}) collective-permute-start(bf16[128,256]{1,0:T(8,128)(2,1)S(1)} %collective-permute-done.refs_1_), channel_id=1, source_target_pairs={{0,1},{1,0},{2,3},{3,2},{4,5},{5,4},{6,7},{7,6},{8,9},{9,8},{10,11... | collective-permute-start | bytes 196616 | tf_op jit(solution)/shard_map/ppermute | solution.py:399
  15.9 19.4 %collective-permute-start.11 = (bf16[8,128,256]{2,1,0:T(8,128)(2,1)S(1)}, bf16[8,128,256]{2,1,0:T(8,128)(2,1)S(1)}, u32[]{:S(2)}, u32[]{:S(2)}) collective-permute-start(bf16[8,128,256]{2,1,0:T(8,128)(2,1)S(1)} %get-tuple-element.26), channel_id=1, source_target_pairs={{0,8},{8,16},{16,24},{24,0},{1,9},{9,17},{17,25},{25,1},{2,10},{10... | collective-permute-start | bytes 1572872 | tf_op jit(solution)/shard_map/ppermute | solution.py:397
  15.9 25.9 %collective-permute-start.19 = (bf16[8,128,256]{2,1,0:T(8,128)(2,1)S(1)}, bf16[8,128,256]{2,1,0:T(8,128)(2,1)S(1)}, u32[]{:S(2)}, u32[]{:S(2)}) collective-permute-start(bf16[8,128,256]{2,1,0:T(8,128)(2,1)S(1)} %get-tuple-element.27), channel_id=1, source_target_pairs={{0,8},{8,16},{16,24},{24,0},{1,9},{9,17},{17,25},{25,1},{2,10},{10... | collective-permute-start | bytes 1572872 | tf_op jit(solution)/shard_map/ppermute | solution.py:406
  16.1 26.6 %collective-permute-start.13 = (bf16[8,128,256]{2,1,0:T(8,128)(2,1)S(1)}, bf16[8,128,256]{2,1,0:T(8,128)(2,1)S(1)}, u32[]{:S(2)}, u32[]{:S(2)}) collective-permute-start(bf16[8,128,256]{2,1,0:T(8,128)(2,1)S(1)} %get-tuple-element.27), channel_id=1, source_target_pairs={{0,24},{8,0},{16,8},{24,16},{1,25},{9,1},{17,9},{25,17},{2,26},{10... | collective-permute-start | bytes 1572872 | tf_op jit(solution)/shard_map/ppermute | solution.py:398
  18.7 27.0 %copy-start.1 = (bf16[8,128,256]{2,1,0:T(8,128)(2,1)}, bf16[8,128,256]{2,1,0:T(8,128)(2,1)S(1)}, u32[]{:S(2)}) copy-start(bf16[8,128,256]{2,1,0:T(8,128)(2,1)S(1)} %collective-permute-done.17.refs_6_) | copy-start | bytes 1572868
  18.7 24.1 %collective-permute-start.18 = (bf16[8,128,256]{2,1,0:T(8,128)(2,1)S(1)}, bf16[8,128,256]{2,1,0:T(8,128)(2,1)S(1)}, u32[]{:S(2)}, u32[]{:S(2)}) collective-permute-start(bf16[8,128,256]{2,1,0:T(8,128)(2,1)S(1)} %collective-permute-done.17.refs_6_), channel_id=1, source_target_pairs={{0,1},{1,0},{2,3},{3,2},{4,5},{5,4},{6,7},{7,6},{8,9},{9,8},{10,11... | collective-permute-start | bytes 1572872 | tf_op jit(solution)/shard_map/ppermute | solution.py:415
  24.3 1.6 %collective-permute-start.7 = (bf16[4,16,2048]{2,1,0:T(8,128)(2,1)S(1)}, bf16[4,16,2048]{2,1,0:T(8,128)(2,1)S(1)}, u32[]{:S(2)}, u32[]{:S(2)}) collective-permute-start(bf16[4,16,2048]{2,1,0:T(8,128)(2,1)S(1)} %get-tuple-element.21), channel_id=1, source_target_pairs={{0,1},{1,0},{2,3},{3,2},{4,5},{5,4},{6,7},{7,6},{8,9},{9,8},{10,11... | collective-permute-start | bytes 786440 | tf_op jit(solution)/shard_map/ppermute | solution.py:404
  26.0 4.8 %collective-permute-start.8 = (bf16[16,2048]{1,0:T(8,128)(2,1)S(1)}, bf16[16,2048]{1,0:T(8,128)(2,1)S(1)}, u32[]{:S(2)}, u32[]{:S(2)}) collective-permute-start(bf16[16,2048]{1,0:T(8,128)(2,1)S(1)} %get-tuple-element.23), channel_id=1, source_target_pairs={{0,2},{2,4},{4,6},{6,0},{1,3},{3,5},{5,7},{7,1},{8,10},{10,12},{12... | collective-permute-start | bytes 196616 | tf_op jit(solution)/shard_map/ppermute | solution.py:408
  30.7 4.6 %collective-permute-start.9 = (bf16[16,2048]{1,0:T(8,128)(2,1)S(1)}, bf16[16,2048]{1,0:T(8,128)(2,1)S(1)}, u32[]{:S(2)}, u32[]{:S(2)}) collective-permute-start(bf16[16,2048]{1,0:T(8,128)(2,1)S(1)} %get-tuple-element.24), channel_id=1, source_target_pairs={{0,4},{2,6},{4,0},{6,2},{1,5},{3,7},{5,1},{7,3},{8,12},{10,14},{12... | collective-permute-start | bytes 196616 | tf_op jit(solution)/shard_map/ppermute | solution.py:408
  35.3 3.4 %collective-permute-start.10 = (bf16[16,2048]{1,0:T(8,128)(2,1)S(1)}, bf16[16,2048]{1,0:T(8,128)(2,1)S(1)}, u32[]{:S(2)}, u32[]{:S(2)}) collective-permute-start(bf16[16,2048]{1,0:T(8,128)(2,1)S(1)} %get-tuple-element.25), channel_id=1, source_target_pairs={{0,6},{2,0},{4,2},{6,4},{1,7},{3,1},{5,3},{7,5},{8,14},{10,8},{12,... | collective-permute-start | bytes 196616 | tf_op jit(solution)/shard_map/ppermute | solution.py:408
  35.4 36.5 %copy-start.2 = (bf16[8,128,256]{2,1,0:T(8,128)(2,1)}, bf16[8,128,256]{2,1,0:T(8,128)(2,1)S(1)}, u32[]{:S(2)}) copy-start(bf16[8,128,256]{2,1,0:T(8,128)(2,1)S(1)} %collective-permute-done.11.refs_4_) | copy-start | bytes 1572868
  35.4 18.6 %collective-permute-start.15 = (bf16[8,128,256]{2,1,0:T(8,128)(2,1)S(1)}, bf16[8,128,256]{2,1,0:T(8,128)(2,1)}, u32[]{:S(2)}, u32[]{:S(2)}) collective-permute-start(bf16[8,128,256]{2,1,0:T(8,128)(2,1)S(1)} %collective-permute-done.11.refs_4_), channel_id=1, source_target_pairs={{0,1},{1,0},{2,3},{3,2},{4,5},{5,4},{6,7},{7,6},{8,9},{9,8},{10,11... | collective-permute-start | bytes 1572872 | tf_op jit(solution)/shard_map/ppermute | solution.py:414
  38.8 15.2 %collective-permute-start.12 = (bf16[8,128,256]{2,1,0:T(8,128)(2,1)S(1)}, bf16[8,128,256]{2,1,0:T(8,128)(2,1)}, u32[]{:S(2)}, u32[]{:S(2)}) collective-permute-start(bf16[8,128,256]{2,1,0:T(8,128)(2,1)S(1)} %collective-permute-done.11.refs_4_), channel_id=1, source_target_pairs={{0,8},{8,16},{16,24},{24,0},{1,9},{9,17},{17,25},{25,1},{2,10},{10... | collective-permute-start | bytes 1572872 | tf_op jit(solution)/shard_map/ppermute | solution.py:411
  41.8 30.1 %copy-start.3 = (bf16[8,128,256]{2,1,0:T(8,128)(2,1)}, bf16[8,128,256]{2,1,0:T(8,128)(2,1)S(1)}, u32[]{:S(2)}) copy-start(bf16[8,128,256]{2,1,0:T(8,128)(2,1)S(1)} %collective-permute-done.19.refs_10_) | copy-start | bytes 1572868
  41.8 12.1 %collective-permute-start.20 = (bf16[8,128,256]{2,1,0:T(8,128)(2,1)S(1)}, bf16[8,128,256]{2,1,0:T(8,128)(2,1)}, u32[]{:S(2)}, u32[]{:S(2)}) collective-permute-start(bf16[8,128,256]{2,1,0:T(8,128)(2,1)S(1)} %collective-permute-done.19.refs_10_), channel_id=1, source_target_pairs={{0,1},{1,0},{2,3},{3,2},{4,5},{5,4},{6,7},{7,6},{8,9},{9,8},{10,11... | collective-permute-start | bytes 1572872 | tf_op jit(solution)/shard_map/ppermute | solution.py:415
  42.7 29.2 %copy-start.4 = (bf16[8,128,256]{2,1,0:T(8,128)(2,1)}, bf16[8,128,256]{2,1,0:T(8,128)(2,1)S(1)}, u32[]{:S(2)}) copy-start(bf16[8,128,256]{2,1,0:T(8,128)(2,1)S(1)} %collective-permute-done.13.refs_12_) | copy-start | bytes 1572868
  42.7 11.2 %collective-permute-start.16 = (bf16[8,128,256]{2,1,0:T(8,128)(2,1)S(1)}, bf16[8,128,256]{2,1,0:T(8,128)(2,1)}, u32[]{:S(2)}, u32[]{:S(2)}) collective-permute-start(bf16[8,128,256]{2,1,0:T(8,128)(2,1)S(1)} %collective-permute-done.13.refs_12_), channel_id=1, source_target_pairs={{0,1},{1,0},{2,3},{3,2},{4,5},{5,4},{6,7},{7,6},{8,9},{9,8},{10,11... | collective-permute-start | bytes 1572872 | tf_op jit(solution)/shard_map/ppermute | solution.py:414
  42.8 29.1 %copy-start.5 = (bf16[8,128,256]{2,1,0:T(8,128)(2,1)}, bf16[8,128,256]{2,1,0:T(8,128)(2,1)S(1)}, u32[]{:S(2)}) copy-start(bf16[8,128,256]{2,1,0:T(8,128)(2,1)S(1)} %collective-permute-done.18.refs_7_) | copy-start | bytes 1572868
  42.8 13.2 %collective-permute-start.14 = (bf16[8,128,256]{2,1,0:T(8,128)(2,1)S(1)}, bf16[8,128,256]{2,1,0:T(8,128)(2,1)}, u32[]{:S(2)}, u32[]{:S(2)}) collective-permute-start(bf16[8,128,256]{2,1,0:T(8,128)(2,1)S(1)} %collective-permute-done.13.refs_12_), channel_id=1, source_target_pairs={{0,24},{8,0},{16,8},{24,16},{1,25},{9,1},{17,9},{25,17},{2,26},{10... | collective-permute-start | bytes 1572872 | tf_op jit(solution)/shard_map/ppermute | solution.py:412
  45.7 26.1 %all-to-all-start = ((bf16[8,16,2048]{2,1,0:T(8,128)(2,1)}), bf16[8,16,2048]{2,1,0:T(8,128)(2,1)S(1)}, u32[]{:S(2)}, u32[]{:S(2)}) async-start(bf16[8,16,2048]{2,1,0:T(8,128)(2,1)} %middle.1), calls=%async_computation | async-start | bytes 1048576 | tf_op jit(solution)/shard_map/all_to_all | solution.py:387
  56.0 15.9 %collective-permute-start.21 = (bf16[8,128,256]{2,1,0:T(8,128)(2,1)}, bf16[8,128,256]{2,1,0:T(8,128)(2,1)S(1)}, u32[]{:S(2)}, u32[]{:S(2)}) collective-permute-start(bf16[8,128,256]{2,1,0:T(8,128)(2,1)} %collective-permute-done.12.refs_8_), channel_id=1, source_target_pairs={{0,1},{1,0},{2,3},{3,2},{4,5},{5,4},{6,7},{7,6},{8,9},{9,8},{10,11... | collective-permute-start | bytes 1572872 | tf_op jit(solution)/shard_map/ppermute | solution.py:417
  57.3 14.6 %collective-permute-start.22 = (bf16[8,128,256]{2,1,0:T(8,128)(2,1)}, bf16[8,128,256]{2,1,0:T(8,128)(2,1)}, u32[]{:S(2)}, u32[]{:S(2)}) collective-permute-start(bf16[8,128,256]{2,1,0:T(8,128)(2,1)} %collective-permute-done.14.refs_14_), channel_id=1, source_target_pairs={{0,1},{1,0},{2,3},{3,2},{4,5},{5,4},{6,7},{7,6},{8,9},{9,8},{10,11... | collective-permute-start | bytes 1572872 | tf_op jit(solution)/shard_map/ppermute | solution.py:417
  71.9 0.8 copy-start
  71.9 1.0 copy-start.6
  78.8 22.4 %all-to-all-start.1 = ((bf16[64,16,256]{2,1,0:T(8,128)(2,1)}), bf16[64,16,256]{2,1,0:T(8,128)(2,1)S(1)}, u32[]{:S(2)}, u32[]{:S(2)}) async-start(bf16[64,16,256]{2,1,0:T(8,128)(2,1)} %bitcast.5), calls=%async_computation.1 | async-start | bytes 1048576 | tf_op jit(solution)/shard_map/all_to_all | solution.py:387

commit v5 on v4

--- a/solution.py
+++ b/solution.py
@@ -294,36 +294,46 @@
     )(*map(in_vmem, (own, *parts)))
 
 
-def mixer_kernel(*refs):
-    everyone, channel_gain, own_up, own_down = refs[:4]
-    ups, downs = refs[4:10], refs[10:16]
-    out, rows, up, down, sems = refs[16:]
-    row_copy = pltpu.make_async_copy(everyone, rows, sems.at[27])
-    row_copy.start()
-    up_copies = [pltpu.make_async_copy(own_up, up.at[:, :, pl.ds(0, 256)], sems.at[0])]
-    down_copies = [
-        pltpu.make_async_copy(
-            own_down.at[:, pl.ds(256 * j, 256)], down.at[j, pl.ds(0, 256)], sems.at[1 + j]
-        )
-        for j in range(8)
-    ]
-    for p in range(6):
-        at = 256 + 128 * p
+def piece_copies(ups, downs, up, down, at, sems):
+    up_copies, down_copies = [], []
+    for p in range(len(ups)):
+        to = at + 128 * p
         for i in range(2):
             up_copies.append(
                 pltpu.make_async_copy(
-                    ups[p].at[pl.ds(0, 8), :, pl.ds(128 * i, 128)],
-                    up.at[pl.ds(8 * i, 8), :, pl.ds(at, 128)],
-                    sems.at[9 + 3 * p + i],
+                    ups[p].at[:, :, pl.ds(128 * i, 128)],
+                    up.at[pl.ds(8 * i, 8), :, pl.ds(to, 128)],
+                    sems.at[3 * p + i],
                 )
             )
         down_copies.append(
-            pltpu.make_async_copy(
-                downs[p].at[pl.ds(downs[p].shape[0] - 8, 8)],
-                down.at[:, pl.ds(at, 128), :],
-                sems.at[9 + 3 * p + 2],
-            )
+            pltpu.make_async_copy(downs[p], down.at[:, pl.ds(to, 128), :], sems.at[3 * p + 2])
         )
+    return up_copies, down_copies
+
+
+def hidden_units(scaled, up, n, second_rms):
+    weight = up[:, :, 256 * n : 256 * n + 256].reshape(D, 256)
+    hidden = second_rms * jnp.dot(scaled, weight, preferred_element_type=F32)
+    return jnp.square(jax.nn.relu(hidden)).astype(BF16)
+
+
+def mixer_kernel(*refs):
+    everyone, channel_gain, own_up, own_down = refs[:4]
+    ups, downs = refs[4:8], refs[8:12]
+    base, scaled_out, rms_out, rows, up, down, own_sems, sems = refs[12:]
+    row_copy = pltpu.make_async_copy(everyone, rows, own_sems.at[0])
+    row_copy.start()
+    up_copies, down_copies = piece_copies(ups, downs, up, down, 256, sems)
+    up_copies.insert(
+        0, pltpu.make_async_copy(own_up, up.at[:, :, pl.ds(0, 256)], own_sems.at[1])
+    )
+    down_copies += [
+        pltpu.make_async_copy(
+            own_down.at[:, pl.ds(256 * j, 256)], down.at[j, pl.ds(0, 256)], own_sems.at[2 + j]
+        )
+        for j in range(8)
+    ]
     for copy in up_copies + down_copies:
         copy.start()
     row_copy.wait()
@@ -334,17 +344,14 @@
         squares += wide * wide
         scaled.append((wide * gain_row(channel_gain, j)).astype(BF16))
     second_rms = lax.rsqrt(jnp.sum(squares, axis=1, keepdims=True) / D + EPSILON)
+    rms_out[...] = jnp.broadcast_to(second_rms, (ROWS, 128))
     scaled = jnp.concatenate(scaled, axis=1)
+    scaled_out[...] = scaled
     activated = []
-    for n in range(4):
+    for n in range(3):
         for copy in up_copies[0:1] if n == 0 else up_copies[4 * n - 3 : 4 * n + 1]:
             copy.wait()
-        hidden = second_rms * jnp.dot(
-            scaled,
-            up[:, :, 256 * n : 256 * n + 256].reshape(D, 256),
-            preferred_element_type=F32,
-        )
-        activated.append(jnp.square(jax.nn.relu(hidden)).astype(BF16))
+        activated.append(hidden_units(scaled, up, n, second_rms))
     activated = jnp.concatenate(activated, axis=1)
     for copy in down_copies:
         copy.wait()
@@ -353,8 +360,7 @@
     for j in range(TP):
         part = jnp.dot(activated, down[j], preferred_element_type=F32)
         own = rows[:, :, 256 * j : 256 * j + 256].reshape(ROWS, 256).astype(F32)
-        part = part + jnp.where(mine, own, 0.0)
-        out[:, j] = part.astype(BF16).reshape(Z, SHARE, 256)
+        base[j] = part + jnp.where(mine, own, 0.0)
 
 
 def mixer(rows, channel_gain, own_up, own_down, ups, downs):
@@ -362,21 +368,60 @@
     vmem = pl.BlockSpec(memory_space=pltpu.VMEM)
     return pl.pallas_call(
         mixer_kernel,
-        out_shape=pltpu.VMEM((Z, TP, SHARE, 256), BF16),
-        in_specs=[any_space, vmem] + [any_space] * 14,
-        out_specs=vmem,
+        out_shape=(
+            jax.ShapeDtypeStruct((TP, ROWS, 256), F32),
+            jax.ShapeDtypeStruct((ROWS, D), BF16),
+            jax.ShapeDtypeStruct((ROWS, 128), F32),
+        ),
+        in_specs=[any_space, vmem] + [any_space] * 10,
+        out_specs=(vmem,) * 3,
         scratch_shapes=[
             pltpu.VMEM((Z, SHARE, D), BF16),
-            pltpu.VMEM((16, 128, 1024), BF16),
-            pltpu.VMEM((8, 1024, 256), BF16),
-            pltpu.SemaphoreType.DMA((28,)),
+            pltpu.VMEM((16, 128, 768), BF16),
+            pltpu.VMEM((8, 768, 256), BF16),
+            pltpu.SemaphoreType.DMA((10,)),
+            pltpu.SemaphoreType.DMA((12,)),
         ],
         compiler_params=pltpu.CompilerParams(vmem_limit_bytes=MIXER_LIMIT),
         name="mixer",
     )(
-        in_hbm(rows), in_hbm(channel_gain.reshape(16, 128)), in_hbm(own_up.reshape(16, 128, 256)),
-        in_hbm(own_down), *map(in_hbm, ups), *map(in_hbm, downs),
-    )
+        rows, in_hbm(channel_gain.reshape(16, 128)), in_hbm(own_up.reshape(16, 128, 256)),
+        in_hbm(own_down), *ups, *downs,
+    )
+
+
+def finish_kernel(base, scaled, rms, *refs):
+    ups, downs = refs[:2], refs[2:4]
+    out, up, down, sems = refs[4:]
+    up_copies, down_copies = piece_copies(ups, downs, up, down, 0, sems)
+    for copy in up_copies + down_copies:
+        copy.start()
+    for copy in up_copies:
+        copy.wait()
+    activated = hidden_units(scaled[...], up, 0, rms[:, 0:1])
+    for copy in down_copies:
+        copy.wait()
+    for j in range(TP):
+        part = base[j] + jnp.dot(activated, down[j], preferred_element_type=F32)
+        out[:, j] = part.astype(BF16).reshape(Z, SHARE, 256)
+
+
+def finish(base, scaled, rms, ups, downs):
+    any_space = pl.BlockSpec(memory_space=pl.ANY)
+    vmem = pl.BlockSpec(memory_space=pltpu.VMEM)
+    return pl.pallas_call(
+        finish_kernel,
+        out_shape=jax.ShapeDtypeStruct((Z, TP, SHARE, 256), BF16),
+        in_specs=[vmem] * 3 + [any_space] * 4,
+        out_specs=vmem,
+        scratch_shapes=[
+            pltpu.VMEM((16, 128, 256), BF16),
+            pltpu.VMEM((8, 256, 256), BF16),
+            pltpu.SemaphoreType.DMA((6,)),
+        ],
+        compiler_params=pltpu.CompilerParams(vmem_limit_bytes=MIXER_LIMIT),
+        name="finish",
+    )(in_vmem(base), in_vmem(scaled), in_vmem(rms), *ups, *downs)
 
 
 def shift(count, by):
@@ -415,11 +460,15 @@
     near_other += [lax.ppermute(w, "c", swap) for w in (right_up, left_down)]
     far_up, far_down, *near_other = lax.optimization_barrier((far_up, far_down, *near_other))
     far_other = [lax.ppermute(w, "c", swap) for w in (far_up, far_down)]
-    down = mixer(
+    near_other = [in_hbm(w) for w in near_other]
+    right_up, left_down = in_hbm(right_up), in_hbm(left_down)
+    base, scaled, rms = mixer(
         everyone, channel_gain, w_up, w_down,
-        (left_up, near_other[0], right_up, near_other[2], far_up, far_other[0]),
-        (left_down, near_other[3], right_down, near_other[1], far_down, far_other[1]),
-    )
+        (left_up, near_other[0], right_up, near_other[2]),
+        (left_down, near_other[3], right_down, near_other[1]),
+    )
+    far_up, far_down = in_hbm(far_up), in_hbm(far_down)
+    down = finish(base, scaled, rms, (far_up, far_other[0]), (far_down, far_other[1]))
     down = to_all(down.reshape(Z * TP, SHARE, 256), ("z", "y", "c"))
     layer_out = jnp.sum(down.reshape(Z, ROWS, 256).astype(F32), axis=0).astype(BF16)
     return (layer_out, new_states.transpose(3, 0, 1, 2))

time: 102 us -> 103 us (level)
    pallas_call x1 -> x2, Pallas kernels: 6 us -> 6.82 us  [the longest x1 4.08 us: mixer(): pl.pallas_call(mixer_kernel, out_shape=(jax.ShapeDtypeStruct((TP, ROWS, 2...]
  transfers between devices with their start and end apart: 25 -> 25, of which waited for: 9 -> 9; matrix products, arithmetic and copies ran while one was open for 0% -> 0% of each run, Pallas kernels for 10% -> 14%
where the time goes in v5:
time: 103 us
  waiting for transfers between devices  45.7 us (44%)
  starting transfers between devices  35.7 us (35%)
  Pallas kernels  18.1 us (18%)
  local copies, waits for them, and re-layouts  1.57 us (2%)
    all_to_all x2, waiting for transfers between devices, to_all(): return lax.all_to_all(array, axes, 0, 0, tiled=True)  28.3 us
    all_to_all x2, starting transfers between devices, to_all(): return lax.all_to_all(array, axes, 0, 0, tiled=True)  12.8 us
    ppermute x3, waiting for transfers between devices, local(): lax.ppermute(parts[k], 'y', shift(Y, k))  10.4 us
    ppermute x4, starting transfers between devices, local(): blocks += [lax.ppermute(block, 'c', swap) for block in blocks]  5.43 us
    pallas_call x1, Pallas kernels, retain(): pl.pallas_call(retain_kernel, out_shape=(jax.ShapeDtypeStruct((Y, SHARE,...  5.03 us
    pallas_call x1, Pallas kernels, update(): pl.pallas_call(update_kernel, out_shape=jax.ShapeDtypeStruct((2, HEAD, HE...  4.16 us
    pallas_call x1, Pallas kernels, mixer(): pl.pallas_call(mixer_kernel, out_shape=(jax.ShapeDtypeStruct((TP, ROWS, 2...  4.08 us
    ppermute x3, starting transfers between devices, local(): lax.ppermute(tokens, 'y', shift(Y, by))  3.77 us
  transfers between devices with their start and end apart: 25, of which 9 were waited for; matrix products, arithmetic and copies ran while one was open for 0% of the time, Pallas kernels for 14%

profile of v5, /device:TPU:1, one launch (start us, length us, event | category | flops | bytes accessed | tf_op | source)
XLA Modules:
  0.0 102.6 jit_solution(17708838496963903703)
XLA Ops:
  0.6 1.2 %pack.1 = (bf16[8,128,256]{2,1,0:T(8,128)(2,1)S(1)}, bf16[8,128,256]{2,1,0:T(8,128)(2,1)S(1)}) custom-call(bf16[16,128,256]{2,1,0:T(8,128)(2,1)} %bitcast.13, bf16[256,2048]{1,0:T(8,128)(2,1)} %refs_3_.1), custom_call_target="tpu_custom_call" | custom-call | tf_op jit(solution)/shard_map/pack/pallas_call | solution.py:62
  1.9 3.4 %collective-permute-start.17 = (bf16[8,128,256]{2,1,0:T(8,128)(2,1)S(1)}, bf16[8,128,256]{2,1,0:T(8,128)(2,1)S(1)}, u32[]{:S(2)}, u32[]{:S(2)}) collective-permute-start(bf16[8,128,256]{2,1,0:T(8,128)(2,1)S(1)} %get-tuple-element.29), channel_id=1, source_target_pairs={{0,24},{8,0},{16,8},{24,16},{1,25},{9,1},{17,9},{25,17},{2,26},{10... | collective-permute-start | bytes 1572872 | tf_op jit(solution)/shard_map/ppermute | solution.py:450
  5.2 2.7 %collective-permute-start.2 = (bf16[128,256]{1,0:T(8,128)(2,1)}, bf16[128,256]{1,0:T(8,128)(2,1)S(1)}, u32[]{:S(2)}, u32[]{:S(2)}) collective-permute-start(bf16[128,256]{1,0:T(8,128)(2,1)} %refs_0_.1), channel_id=1, source_target_pairs={{0,6},{2,0},{4,2},{6,4},{1,7},{3,1},{5,3},{7,5},{8,14},{10,8},{12,... | collective-permute-start | bytes 196616 | tf_op jit(solution)/shard_map/ppermute | solution.py:440
  8.3 0.7 collective-permute-start
  9.0 1.8 %collective-permute-start.3 = (bf16[128,256]{1,0:T(8,128)(2,1)}, bf16[128,256]{1,0:T(8,128)(2,1)S(1)}, u32[]{:S(2)}, u32[]{:S(2)}) collective-permute-start(bf16[128,256]{1,0:T(8,128)(2,1)} %refs_0_.1), channel_id=1, source_target_pairs={{0,1},{1,0},{2,3},{3,2},{4,5},{5,4},{6,7},{7,6},{8,9},{9,8},{10,11... | collective-permute-start | bytes 196616 | tf_op jit(solution)/shard_map/ppermute | solution.py:444
  10.8 0.6 collective-permute-start.6
  11.4 1.4 %collective-permute-done.1.refs_2_ = bf16[128,256]{1,0:T(8,128)(2,1)S(1)} collective-permute-done((bf16[128,256]{1,0:T(8,128)(2,1)}, bf16[128,256]{1,0:T(8,128)(2,1)S(1)}, u32[]{:S(2)}, u32[]{:S(2)}) %collective-permute-start.1) | collective-permute-done | bytes 65568 | tf_op jit(solution)/shard_map/ppermute | solution.py:440
  12.9 2.3 %collective-permute-start.5 = (bf16[128,256]{1,0:T(8,128)(2,1)S(1)}, bf16[128,256]{1,0:T(8,128)(2,1)S(1)}, u32[]{:S(2)}, u32[]{:S(2)}) collective-permute-start(bf16[128,256]{1,0:T(8,128)(2,1)S(1)} %collective-permute-done.1.refs_2_), channel_id=1, source_target_pairs={{0,1},{1,0},{2,3},{3,2},{4,5},{5,4},{6,7},{7,6},{8,9},{9,8},{10,11... | collective-permute-start | bytes 196616 | tf_op jit(solution)/shard_map/ppermute | solution.py:444
  15.2 0.7 collective-permute-start.4
  16.1 2.6 %collective-permute-start.13 = (bf16[8,128,256]{2,1,0:T(8,128)(2,1)S(1)}, bf16[8,128,256]{2,1,0:T(8,128)(2,1)S(1)}, u32[]{:S(2)}, u32[]{:S(2)}) collective-permute-start(bf16[8,128,256]{2,1,0:T(8,128)(2,1)S(1)} %get-tuple-element.30), channel_id=1, source_target_pairs={{0,24},{8,0},{16,8},{24,16},{1,25},{9,1},{17,9},{25,17},{2,26},{10... | collective-permute-start | bytes 1572872 | tf_op jit(solution)/shard_map/ppermute | solution.py:443
  19.3 5.0 %retain.1 = (f32[4,16,2048]{2,1,0:T(8,128)S(1)}, bf16[4,16,2048]{2,1,0:T(8,128)(2,1)S(1)}, bf16[16,2048]{1,0:T(8,128)(2,1)S(1)}, f32[128,128]{1,0:T(8,128)S(1)}, f32[128,128]{1,0:T(8,128)S(1)}) custom-call(f32[16]{0:T(128)} %constant.9.clone.decays, bf16[128,256]{1,0:T(8,128)(2,1)} %refs_0_.1, bf16[128,256]{1,0:T(8,128)(2,1)S(1)} %collective-permute-done.refs_1_, ...), custom_call_target="tpu_custom_call" | custom-call | tf_op jit(solution)/shard_map/retain/pallas_call | solution.py:179
  24.6 1.4 %collective-permute-done.7.others = bf16[4,16,2048]{2,1,0:T(8,128)(2,1)S(1)} collective-permute-done((bf16[4,16,2048]{2,1,0:T(8,128)(2,1)S(1)}, bf16[4,16,2048]{2,1,0:T(8,128)(2,1)S(1)}, u32[]{:S(2)}, u32[]{:S(2)}) %collective-permute-start.7) | collective-permute-done | bytes 262176 | tf_op jit(solution)/shard_map/ppermute | solution.py:449
  26.1 4.7 %collective-permute-done.8.refs_0_ = bf16[16,2048]{1,0:T(8,128)(2,1)S(1)} collective-permute-done((bf16[16,2048]{1,0:T(8,128)(2,1)S(1)}, bf16[16,2048]{1,0:T(8,128)(2,1)S(1)}, u32[]{:S(2)}, u32[]{:S(2)}) %collective-permute-start.8) | collective-permute-done | bytes 65568 | tf_op jit(solution)/shard_map/ppermute | solution.py:453
  30.7 4.6 %collective-permute-done.9.refs_1_ = bf16[16,2048]{1,0:T(8,128)(2,1)S(1)} collective-permute-done((bf16[16,2048]{1,0:T(8,128)(2,1)S(1)}, bf16[16,2048]{1,0:T(8,128)(2,1)S(1)}, u32[]{:S(2)}, u32[]{:S(2)}) %collective-permute-start.9) | collective-permute-done | bytes 65568 | tf_op jit(solution)/shard_map/ppermute | solution.py:453
  35.4 2.4 %collective-permute-start.15 = (bf16[8,128,256]{2,1,0:T(8,128)(2,1)S(1)}, bf16[8,128,256]{2,1,0:T(8,128)(2,1)}, u32[]{:S(2)}, u32[]{:S(2)}) collective-permute-start(bf16[8,128,256]{2,1,0:T(8,128)(2,1)S(1)} %collective-permute-done.11.refs_4_), channel_id=1, source_target_pairs={{0,1},{1,0},{2,3},{3,2},{4,5},{5,4},{6,7},{7,6},{8,9},{9,8},{10,11... | collective-permute-start | bytes 1572872 | tf_op jit(solution)/shard_map/ppermute | solution.py:459
  37.7 1.1 %collective-permute-done.10.refs_2_ = bf16[16,2048]{1,0:T(8,128)(2,1)S(1)} collective-permute-done((bf16[16,2048]{1,0:T(8,128)(2,1)S(1)}, bf16[16,2048]{1,0:T(8,128)(2,1)S(1)}, u32[]{:S(2)}, u32[]{:S(2)}) %collective-permute-start.10) | collective-permute-done | bytes 65568 | tf_op jit(solution)/shard_map/ppermute | solution.py:453
  38.9 3.1 %collective-permute-done.19.refs_8_ = bf16[8,128,256]{2,1,0:T(8,128)(2,1)} collective-permute-done((bf16[8,128,256]{2,1,0:T(8,128)(2,1)S(1)}, bf16[8,128,256]{2,1,0:T(8,128)(2,1)}, u32[]{:S(2)}, u32[]{:S(2)}) %collective-permute-start.19) | collective-permute-done | bytes 524320 | tf_op jit(solution)/shard_map/ppermute | solution.py:451
  41.9 0.9 collective-permute-start.20
  42.8 0.8 copy-done.1
  43.6 2.1 %collective-permute-start.14 = (bf16[8,128,256]{2,1,0:T(8,128)(2,1)S(1)}, bf16[8,128,256]{2,1,0:T(8,128)(2,1)S(1)}, u32[]{:S(2)}, u32[]{:S(2)}) collective-permute-start(bf16[8,128,256]{2,1,0:T(8,128)(2,1)S(1)} %collective-permute-done.13.refs_10_), channel_id=1, source_target_pairs={{0,24},{8,0},{16,8},{24,16},{1,25},{9,1},{17,9},{25,17},{2,26},{10... | collective-permute-start | bytes 1572872 | tf_op jit(solution)/shard_map/ppermute | solution.py:457
  45.7 0.8 middle.1
  46.5 8.2 %all-to-all-start = ((bf16[8,16,2048]{2,1,0:T(8,128)(2,1)}), bf16[8,16,2048]{2,1,0:T(8,128)(2,1)S(1)}, u32[]{:S(2)}, u32[]{:S(2)}) async-start(bf16[8,16,2048]{2,1,0:T(8,128)(2,1)} %middle.1), calls=%async_computation | async-start | bytes 1048576 | tf_op jit(solution)/shard_map/all_to_all | solution.py:432
  54.7 0.8 copy-done.2
  55.5 1.1 %collective-permute-done.14.refs_2_ = bf16[8,128,256]{2,1,0:T(8,128)(2,1)S(1)} collective-permute-done((bf16[8,128,256]{2,1,0:T(8,128)(2,1)S(1)}, bf16[8,128,256]{2,1,0:T(8,128)(2,1)S(1)}, u32[]{:S(2)}, u32[]{:S(2)}) %collective-permute-start.14) | collective-permute-done | bytes 524320 | tf_op jit(solution)/shard_map/ppermute | solution.py:457
  56.6 1.4 %collective-permute-start.21 = (bf16[8,128,256]{2,1,0:T(8,128)(2,1)}, bf16[8,128,256]{2,1,0:T(8,128)(2,1)S(1)}, u32[]{:S(2)}, u32[]{:S(2)}) collective-permute-start(bf16[8,128,256]{2,1,0:T(8,128)(2,1)} %collective-permute-done.12.refs_0_), channel_id=1, source_target_pairs={{0,1},{1,0},{2,3},{3,2},{4,5},{5,4},{6,7},{7,6},{8,9},{9,8},{10,11... | collective-permute-start | bytes 1572872 | tf_op jit(solution)/shard_map/ppermute | solution.py:462
  57.9 14.7 %all-to-all-done.refs_0_ = bf16[8,16,2048]{2,1,0:T(8,128)(2,1)S(1)} async-done(((bf16[8,16,2048]{2,1,0:T(8,128)(2,1)}), bf16[8,16,2048]{2,1,0:T(8,128)(2,1)S(1)}, u32[]{:S(2)}, u32[]{:S(2)}) %all-to-all-start) | async-done | bytes 524320 | tf_op jit(solution)/shard_map/all_to_all | solution.py:432
  72.6 4.1 %mixer.1 = (f32[8,128,256]{2,1,0:T(8,128)S(1)}, bf16[128,2048]{1,0:T(8,128)(2,1)S(1)}, f32[128,128]{1,0:T(8,128)S(1)}) custom-call(bf16[8,16,2048]{2,1,0:T(8,128)(2,1)S(1)} %all-to-all-done.refs_0_, bf16[16,128]{1,0:T(8,128)(2,1)} %bitcast.17, bf16[16,128,256]{2,1,0:T(8,128)(2,1)} %bitcast.14, bf16[256,2048]{1,0:T(8,128)(2,1)} %refs_3_.1, ...), custom_call_target="tpu_custom_call" | custom-call | tf_op jit(solution)/shard_map/mixer/pallas_call | solution.py:369
  76.7 2.7 %finish.1 = bf16[8,8,16,256]{3,2,1,0:T(8,128)(2,1)} custom-call(f32[8,128,256]{2,1,0:T(8,128)S(1)} %get-tuple-element.35.base, bf16[128,2048]{1,0:T(8,128)(2,1)S(1)} %get-tuple-element.36.scaled, f32[128,128]{1,0:T(8,128)S(1)} %get-tuple-element.37.rms, bf16[8,128,256]{2,1,0:T(8,128)(2,1)} %collective-permute-done.12.refs_0_, ...), custom_call_target="tpu_custom_call" | custom-call | tf_op jit(solution)/shard_map/finish/pallas_call | solution.py:412
  79.5 4.6 %all-to-all-start.1 = ((bf16[64,16,256]{2,1,0:T(8,128)(2,1)}), bf16[64,16,256]{2,1,0:T(8,128)(2,1)S(1)}, u32[]{:S(2)}, u32[]{:S(2)}) async-start(bf16[64,16,256]{2,1,0:T(8,128)(2,1)} %bitcast.5), calls=%async_computation.1 | async-start | bytes 1048576 | tf_op jit(solution)/shard_map/all_to_all | solution.py:432
  84.1 4.2 %update.1 = f32[2,64,64,128]{3,2,1,0:T(8,128)} custom-call(f32[16]{0:T(128)} %constant.9.clone.decays, f32[128,128]{1,0:T(8,128)S(1)} %get-tuple-element.40.keys, f32[128,128]{1,0:T(8,128)S(1)} %get-tuple-element.41.values, f32[2,64,64,128]{3,2,1,0:T(8,128)} %bitcast.11), custom_call_target="tpu_custom_call" | custom-call | tf_op jit(solution)/shard_map/update/pallas_call | solution.py:241
  88.2 13.6 %all-to-all-done.1 = bf16[64,16,256]{2,1,0:T(8,128)(2,1)S(1)} async-done(((bf16[64,16,256]{2,1,0:T(8,128)(2,1)}), bf16[64,16,256]{2,1,0:T(8,128)(2,1)S(1)}, u32[]{:S(2)}, u32[]{:S(2)}) %all-to-all-start.1) | async-done | bytes 524320 | tf_op jit(solution)/shard_map/all_to_all | solution.py:432
  101.9 0.7 bitcast_reduce_fusion
  (34 shorter events, 1.6 us)
Async XLA Ops:
  1.9 16.8 %collective-permute-start.17 = (bf16[8,128,256]{2,1,0:T(8,128)(2,1)S(1)}, bf16[8,128,256]{2,1,0:T(8,128)(2,1)S(1)}, u32[]{:S(2)}, u32[]{:S(2)}) collective-permute-start(bf16[8,128,256]{2,1,0:T(8,128)(2,1)S(1)} %get-tuple-element.29), channel_id=1, source_target_pairs={{0,24},{8,0},{16,8},{24,16},{1,25},{9,1},{17,9},{25,17},{2,26},{10... | collective-permute-start | bytes 1572872 | tf_op jit(solution)/shard_map/ppermute | solution.py:450
  5.2 5.6 %collective-permute-start.2 = (bf16[128,256]{1,0:T(8,128)(2,1)}, bf16[128,256]{1,0:T(8,128)(2,1)S(1)}, u32[]{:S(2)}, u32[]{:S(2)}) collective-permute-start(bf16[128,256]{1,0:T(8,128)(2,1)} %refs_0_.1), channel_id=1, source_target_pairs={{0,6},{2,0},{4,2},{6,4},{1,7},{3,1},{5,3},{7,5},{8,14},{10,8},{12,... | collective-permute-start | bytes 196616 | tf_op jit(solution)/shard_map/ppermute | solution.py:440
  8.0 4.9 %collective-permute-start.1 = (bf16[128,256]{1,0:T(8,128)(2,1)}, bf16[128,256]{1,0:T(8,128)(2,1)S(1)}, u32[]{:S(2)}, u32[]{:S(2)}) collective-permute-start(bf16[128,256]{1,0:T(8,128)(2,1)} %refs_0_.1), channel_id=1, source_target_pairs={{0,4},{2,6},{4,0},{6,2},{1,5},{3,7},{5,1},{7,3},{8,12},{10,14},{12... | collective-permute-start | bytes 196616 | tf_op jit(solution)/shard_map/ppermute | solution.py:440
  8.3 6.9 %collective-permute-start = (bf16[128,256]{1,0:T(8,128)(2,1)}, bf16[128,256]{1,0:T(8,128)(2,1)S(1)}, u32[]{:S(2)}, u32[]{:S(2)}) collective-permute-start(bf16[128,256]{1,0:T(8,128)(2,1)} %refs_0_.1), channel_id=1, source_target_pairs={{0,2},{2,4},{4,6},{6,0},{1,3},{3,5},{5,7},{7,1},{8,10},{10,12},{12... | collective-permute-start | bytes 196616 | tf_op jit(solution)/shard_map/ppermute | solution.py:440
  9.0 6.9 %collective-permute-start.3 = (bf16[128,256]{1,0:T(8,128)(2,1)}, bf16[128,256]{1,0:T(8,128)(2,1)S(1)}, u32[]{:S(2)}, u32[]{:S(2)}) collective-permute-start(bf16[128,256]{1,0:T(8,128)(2,1)} %refs_0_.1), channel_id=1, source_target_pairs={{0,1},{1,0},{2,3},{3,2},{4,5},{5,4},{6,7},{7,6},{8,9},{9,8},{10,11... | collective-permute-start | bytes 196616 | tf_op jit(solution)/shard_map/ppermute | solution.py:444
  10.8 5.1 %collective-permute-start.6 = (bf16[128,256]{1,0:T(8,128)(2,1)S(1)}, bf16[128,256]{1,0:T(8,128)(2,1)S(1)}, u32[]{:S(2)}, u32[]{:S(2)}) collective-permute-start(bf16[128,256]{1,0:T(8,128)(2,1)S(1)} %collective-permute-done.2.refs_3_), channel_id=1, source_target_pairs={{0,1},{1,0},{2,3},{3,2},{4,5},{5,4},{6,7},{7,6},{8,9},{9,8},{10,11... | collective-permute-start | bytes 196616 | tf_op jit(solution)/shard_map/ppermute | solution.py:444
  12.9 3.2 %collective-permute-start.5 = (bf16[128,256]{1,0:T(8,128)(2,1)S(1)}, bf16[128,256]{1,0:T(8,128)(2,1)S(1)}, u32[]{:S(2)}, u32[]{:S(2)}) collective-permute-start(bf16[128,256]{1,0:T(8,128)(2,1)S(1)} %collective-permute-done.1.refs_2_), channel_id=1, source_target_pairs={{0,1},{1,0},{2,3},{3,2},{4,5},{5,4},{6,7},{7,6},{8,9},{9,8},{10,11... | collective-permute-start | bytes 196616 | tf_op jit(solution)/shard_map/ppermute | solution.py:444
  15.2 4.1 %collective-permute-start.4 = (bf16[128,256]{1,0:T(8,128)(2,1)S(1)}, bf16[128,256]{1,0:T(8,128)(2,1)S(1)}, u32[]{:S(2)}, u32[]{:S(2)}) collective-permute-start(bf16[128,256]{1,0:T(8,128)(2,1)S(1)} %collective-permute-done.refs_1_), channel_id=1, source_target_pairs={{0,1},{1,0},{2,3},{3,2},{4,5},{5,4},{6,7},{7,6},{8,9},{9,8},{10,11... | collective-permute-start | bytes 196616 | tf_op jit(solution)/shard_map/ppermute | solution.py:444
  15.9 19.4 %collective-permute-start.11 = (bf16[8,128,256]{2,1,0:T(8,128)(2,1)S(1)}, bf16[8,128,256]{2,1,0:T(8,128)(2,1)S(1)}, u32[]{:S(2)}, u32[]{:S(2)}) collective-permute-start(bf16[8,128,256]{2,1,0:T(8,128)(2,1)S(1)} %get-tuple-element.29), channel_id=1, source_target_pairs={{0,8},{8,16},{16,24},{24,0},{1,9},{9,17},{17,25},{25,1},{2,10},{10... | collective-permute-start | bytes 1572872 | tf_op jit(solution)/shard_map/ppermute | solution.py:442
  15.9 26.0 %collective-permute-start.19 = (bf16[8,128,256]{2,1,0:T(8,128)(2,1)S(1)}, bf16[8,128,256]{2,1,0:T(8,128)(2,1)}, u32[]{:S(2)}, u32[]{:S(2)}) collective-permute-start(bf16[8,128,256]{2,1,0:T(8,128)(2,1)S(1)} %get-tuple-element.30), channel_id=1, source_target_pairs={{0,8},{8,16},{16,24},{24,0},{1,9},{9,17},{17,25},{25,1},{2,10},{10... | collective-permute-start | bytes 1572872 | tf_op jit(solution)/shard_map/ppermute | solution.py:451
  16.1 26.7 %collective-permute-start.13 = (bf16[8,128,256]{2,1,0:T(8,128)(2,1)S(1)}, bf16[8,128,256]{2,1,0:T(8,128)(2,1)S(1)}, u32[]{:S(2)}, u32[]{:S(2)}) collective-permute-start(bf16[8,128,256]{2,1,0:T(8,128)(2,1)S(1)} %get-tuple-element.30), channel_id=1, source_target_pairs={{0,24},{8,0},{16,8},{24,16},{1,25},{9,1},{17,9},{25,17},{2,26},{10... | collective-permute-start | bytes 1572872 | tf_op jit(solution)/shard_map/ppermute | solution.py:443
  18.7 27.8 %copy-start = (bf16[8,128,256]{2,1,0:T(8,128)(2,1)}, bf16[8,128,256]{2,1,0:T(8,128)(2,1)S(1)}, u32[]{:S(2)}) copy-start(bf16[8,128,256]{2,1,0:T(8,128)(2,1)S(1)} %collective-permute-done.17.refs_6_) | copy-start | bytes 1572868
  18.7 24.1 %collective-permute-start.18 = (bf16[8,128,256]{2,1,0:T(8,128)(2,1)S(1)}, bf16[8,128,256]{2,1,0:T(8,128)(2,1)S(1)}, u32[]{:S(2)}, u32[]{:S(2)}) collective-permute-start(bf16[8,128,256]{2,1,0:T(8,128)(2,1)S(1)} %collective-permute-done.17.refs_6_), channel_id=1, source_target_pairs={{0,1},{1,0},{2,3},{3,2},{4,5},{5,4},{6,7},{7,6},{8,9},{9,8},{10,11... | collective-permute-start | bytes 1572872 | tf_op jit(solution)/shard_map/ppermute | solution.py:460
  24.3 1.6 %collective-permute-start.7 = (bf16[4,16,2048]{2,1,0:T(8,128)(2,1)S(1)}, bf16[4,16,2048]{2,1,0:T(8,128)(2,1)S(1)}, u32[]{:S(2)}, u32[]{:S(2)}) collective-permute-start(bf16[4,16,2048]{2,1,0:T(8,128)(2,1)S(1)} %get-tuple-element.24), channel_id=1, source_target_pairs={{0,1},{1,0},{2,3},{3,2},{4,5},{5,4},{6,7},{7,6},{8,9},{9,8},{10,11... | collective-permute-start | bytes 786440 | tf_op jit(solution)/shard_map/ppermute | solution.py:449
  26.0 4.8 %collective-permute-start.8 = (bf16[16,2048]{1,0:T(8,128)(2,1)S(1)}, bf16[16,2048]{1,0:T(8,128)(2,1)S(1)}, u32[]{:S(2)}, u32[]{:S(2)}) collective-permute-start(bf16[16,2048]{1,0:T(8,128)(2,1)S(1)} %get-tuple-element.26), channel_id=1, source_target_pairs={{0,2},{2,4},{4,6},{6,0},{1,3},{3,5},{5,7},{7,1},{8,10},{10,12},{12... | collective-permute-start | bytes 196616 | tf_op jit(solution)/shard_map/ppermute | solution.py:453
  30.7 4.6 %collective-permute-start.9 = (bf16[16,2048]{1,0:T(8,128)(2,1)S(1)}, bf16[16,2048]{1,0:T(8,128)(2,1)S(1)}, u32[]{:S(2)}, u32[]{:S(2)}) collective-permute-start(bf16[16,2048]{1,0:T(8,128)(2,1)S(1)} %get-tuple-element.27), channel_id=1, source_target_pairs={{0,4},{2,6},{4,0},{6,2},{1,5},{3,7},{5,1},{7,3},{8,12},{10,14},{12... | collective-permute-start | bytes 196616 | tf_op jit(solution)/shard_map/ppermute | solution.py:453
  35.3 3.5 %collective-permute-start.10 = (bf16[16,2048]{1,0:T(8,128)(2,1)S(1)}, bf16[16,2048]{1,0:T(8,128)(2,1)S(1)}, u32[]{:S(2)}, u32[]{:S(2)}) collective-permute-start(bf16[16,2048]{1,0:T(8,128)(2,1)S(1)} %get-tuple-element.28), channel_id=1, source_target_pairs={{0,6},{2,0},{4,2},{6,4},{1,7},{3,1},{5,3},{7,5},{8,14},{10,8},{12,... | collective-permute-start | bytes 196616 | tf_op jit(solution)/shard_map/ppermute | solution.py:453
  35.4 19.3 %collective-permute-start.15 = (bf16[8,128,256]{2,1,0:T(8,128)(2,1)S(1)}, bf16[8,128,256]{2,1,0:T(8,128)(2,1)}, u32[]{:S(2)}, u32[]{:S(2)}) collective-permute-start(bf16[8,128,256]{2,1,0:T(8,128)(2,1)S(1)} %collective-permute-done.11.refs_4_), channel_id=1, source_target_pairs={{0,1},{1,0},{2,3},{3,2},{4,5},{5,4},{6,7},{7,6},{8,9},{9,8},{10,11... | collective-permute-start | bytes 1572872 | tf_op jit(solution)/shard_map/ppermute | solution.py:459
  38.9 15.8 %collective-permute-start.12 = (bf16[8,128,256]{2,1,0:T(8,128)(2,1)S(1)}, bf16[8,128,256]{2,1,0:T(8,128)(2,1)}, u32[]{:S(2)}, u32[]{:S(2)}) collective-permute-start(bf16[8,128,256]{2,1,0:T(8,128)(2,1)S(1)} %collective-permute-done.11.refs_4_), channel_id=1, source_target_pairs={{0,8},{8,16},{16,24},{24,0},{1,9},{9,17},{17,25},{25,1},{2,10},{10... | collective-permute-start | bytes 1572872 | tf_op jit(solution)/shard_map/ppermute | solution.py:456
  41.9 12.8 %collective-permute-start.20 = (bf16[8,128,256]{2,1,0:T(8,128)(2,1)}, bf16[8,128,256]{2,1,0:T(8,128)(2,1)}, u32[]{:S(2)}, u32[]{:S(2)}) collective-permute-start(bf16[8,128,256]{2,1,0:T(8,128)(2,1)} %collective-permute-done.19.refs_8_), channel_id=1, source_target_pairs={{0,1},{1,0},{2,3},{3,2},{4,5},{5,4},{6,7},{7,6},{8,9},{9,8},{10,11... | collective-permute-start | bytes 1572872 | tf_op jit(solution)/shard_map/ppermute | solution.py:460
  42.8 11.9 %collective-permute-start.16 = (bf16[8,128,256]{2,1,0:T(8,128)(2,1)S(1)}, bf16[8,128,256]{2,1,0:T(8,128)(2,1)S(1)}, u32[]{:S(2)}, u32[]{:S(2)}) collective-permute-start(bf16[8,128,256]{2,1,0:T(8,128)(2,1)S(1)} %collective-permute-done.13.refs_10_), channel_id=1, source_target_pairs={{0,1},{1,0},{2,3},{3,2},{4,5},{5,4},{6,7},{7,6},{8,9},{9,8},{10,11... | collective-permute-start | bytes 1572872 | tf_op jit(solution)/shard_map/ppermute | solution.py:459
  42.8 0.8 copy-start.1
  43.6 13.0 %collective-permute-start.14 = (bf16[8,128,256]{2,1,0:T(8,128)(2,1)S(1)}, bf16[8,128,256]{2,1,0:T(8,128)(2,1)S(1)}, u32[]{:S(2)}, u32[]{:S(2)}) collective-permute-start(bf16[8,128,256]{2,1,0:T(8,128)(2,1)S(1)} %collective-permute-done.13.refs_10_), channel_id=1, source_target_pairs={{0,24},{8,0},{16,8},{24,16},{1,25},{9,1},{17,9},{25,17},{2,26},{10... | collective-permute-start | bytes 1572872 | tf_op jit(solution)/shard_map/ppermute | solution.py:457
  46.5 26.1 %all-to-all-start = ((bf16[8,16,2048]{2,1,0:T(8,128)(2,1)}), bf16[8,16,2048]{2,1,0:T(8,128)(2,1)S(1)}, u32[]{:S(2)}, u32[]{:S(2)}) async-start(bf16[8,16,2048]{2,1,0:T(8,128)(2,1)} %middle.1), calls=%async_computation | async-start | bytes 1048576 | tf_op jit(solution)/shard_map/all_to_all | solution.py:432
  54.7 0.8 copy-start.2
  56.6 20.2 %copy-start.3 = (bf16[8,128,256]{2,1,0:T(8,128)(2,1)}, bf16[8,128,256]{2,1,0:T(8,128)(2,1)S(1)}, u32[]{:S(2)}) copy-start(bf16[8,128,256]{2,1,0:T(8,128)(2,1)S(1)} %collective-permute-done.14.refs_2_) | copy-start | bytes 1572868
  56.6 20.1 %collective-permute-start.21 = (bf16[8,128,256]{2,1,0:T(8,128)(2,1)}, bf16[8,128,256]{2,1,0:T(8,128)(2,1)S(1)}, u32[]{:S(2)}, u32[]{:S(2)}) collective-permute-start(bf16[8,128,256]{2,1,0:T(8,128)(2,1)} %collective-permute-done.12.refs_0_), channel_id=1, source_target_pairs={{0,1},{1,0},{2,3},{3,2},{4,5},{5,4},{6,7},{7,6},{8,9},{9,8},{10,11... | collective-permute-start | bytes 1572872 | tf_op jit(solution)/shard_map/ppermute | solution.py:462
  57.9 18.8 %collective-permute-start.22 = (bf16[8,128,256]{2,1,0:T(8,128)(2,1)S(1)}, bf16[8,128,256]{2,1,0:T(8,128)(2,1)S(1)}, u32[]{:S(2)}, u32[]{:S(2)}) collective-permute-start(bf16[8,128,256]{2,1,0:T(8,128)(2,1)S(1)} %collective-permute-done.14.refs_2_), channel_id=1, source_target_pairs={{0,1},{1,0},{2,3},{3,2},{4,5},{5,4},{6,7},{7,6},{8,9},{9,8},{10,11... | collective-permute-start | bytes 1572872 | tf_op jit(solution)/shard_map/ppermute | solution.py:462
  79.5 22.4 %all-to-all-start.1 = ((bf16[64,16,256]{2,1,0:T(8,128)(2,1)}), bf16[64,16,256]{2,1,0:T(8,128)(2,1)S(1)}, u32[]{:S(2)}, u32[]{:S(2)}) async-start(bf16[64,16,256]{2,1,0:T(8,128)(2,1)} %bitcast.5), calls=%async_computation.1 | async-start | bytes 1048576 | tf_op jit(solution)/shard_map/all_to_all | solution.py:432

commit v6 on v4

--- a/solution.py
+++ b/solution.py
@@ -374,8 +374,8 @@
         compiler_params=pltpu.CompilerParams(vmem_limit_bytes=MIXER_LIMIT),
         name="mixer",
     )(
-        in_hbm(rows), in_hbm(channel_gain.reshape(16, 128)), in_hbm(own_up.reshape(16, 128, 256)),
-        in_hbm(own_down), *map(in_hbm, ups), *map(in_hbm, downs),
+        rows, in_hbm(channel_gain.reshape(16, 128)), in_hbm(own_up.reshape(16, 128, 256)),
+        in_hbm(own_down), *ups, *downs,
     )
 
 
@@ -396,7 +396,8 @@
     packed_up, packed_down = pack(w_up, w_down)
     left_up = lax.ppermute(packed_up, "x", shift(X, 1))
     right_down = lax.ppermute(packed_down, "x", shift(X, 3))
-    blocks += [lax.ppermute(block, "c", swap) for block in blocks]
+    other = lax.ppermute(tokens, "c", swap)
+    blocks += [other] + [lax.ppermute(block, "c", swap) for block in blocks[1:]]
     states = states.transpose(1, 2, 3, 0)
     mine, others, own, keys, values = retain(
         blocks, states, w_query, w_key, w_value, w_gate, w_output, mix_gain, head_gain
@@ -410,11 +411,14 @@
     everyone = to_all(middle, "z")
     far_up = lax.ppermute(left_up, "x", shift(X, 1))
     far_down = lax.ppermute(right_down, "x", shift(X, 3))
-    new_states = update(keys, values, states)
     near_other = [lax.ppermute(w, "c", swap) for w in (left_up, right_down)]
     near_other += [lax.ppermute(w, "c", swap) for w in (right_up, left_down)]
-    far_up, far_down, *near_other = lax.optimization_barrier((far_up, far_down, *near_other))
+    keys, *near_other = lax.optimization_barrier((keys, *near_other))
+    new_states = update(keys, values, states)
     far_other = [lax.ppermute(w, "c", swap) for w in (far_up, far_down)]
+    near_other = [in_hbm(w) for w in near_other]
+    right_up, left_down = in_hbm(right_up), in_hbm(left_down)
+    far_up, far_down = in_hbm(far_up), in_hbm(far_down)
     down = mixer(
         everyone, channel_gain, w_up, w_down,
         (left_up, near_other[0], right_up, near_other[2], far_up, far_other[0]),

time: 102 us -> 94.1 us (0.923)
  waiting for transfers between devices: 46.4 us -> 29.6 us
  starting transfers between devices: 35.8 us -> 44.7 us
    all_to_all x2, waiting for transfers between devices: 28.2 us -> 20.1 us  [to_all(): return lax.all_to_all(array, axes, 0, 0, tiled=True)]
    ppermute x3, waiting for transfers between devices: 10.2 us -> 4.8 us  [local(): lax.ppermute(parts[k], 'y', shift(Y, k))]
    all_to_all x2, starting transfers between devices: 12.8 us -> 17.5 us  [to_all(): return lax.all_to_all(array, axes, 0, 0, tiled=True)]
    ppermute x3, starting transfers between devices: 0.09 us -> 4.65 us  [local(): lax.ppermute(parts[k], 'y', shift(Y, k))]
    ppermute x1, waiting for transfers between devices: 3.07 us -> 0.01 us  [local(): left_down = lax.ppermute(packed_down, 'x', shift(X, 1))]
    ppermute x4, starting transfers between devices: 5.43 us -> 2.96 us  [the longest x1 2.36 us: local(): other = lax.ppermute(tokens, 'c', swap)]
    ppermute x4, waiting for transfers between devices: 0.01 us -> 2.12 us  [the longest x3 1.1 us: local(): blocks += [other] + [lax.ppermute(block, 'c', swap) for block in blocks[1:]]]
    ppermute x1, waiting for transfers between devices: 2.04 us -> 0.01 us  [local(): far_down = lax.ppermute(right_down, 'x', shift(X, 3))]
  transfers between devices with their start and end apart: 25 -> 25, of which waited for: 9 -> 10; matrix products, arithmetic and copies ran while one was open for 0% -> 0% of each run, Pallas kernels for 10% -> 12%
where the time goes in v6:
time: 94.1 us; the launch traced here: 93.7 us
  starting transfers between devices  44.7 us (48%)
  waiting for transfers between devices  29.6 us (31%)
  Pallas kernels  16.8 us (18%)
  local copies, waits for them, and re-layouts  1.18 us (1%)
    all_to_all x2, waiting for transfers between devices, to_all(): return lax.all_to_all(array, axes, 0, 0, tiled=True)  20.1 us
    all_to_all x2, starting transfers between devices, to_all(): return lax.all_to_all(array, axes, 0, 0, tiled=True)  17.5 us
    pallas_call x1, Pallas kernels, mixer(): pl.pallas_call(mixer_kernel, out_shape=pltpu.VMEM((Z, TP, SHARE, 256), BF...  5.48 us
    pallas_call x1, Pallas kernels, retain(): pl.pallas_call(retain_kernel, out_shape=(jax.ShapeDtypeStruct((Y, SHARE,...  5.03 us
    ppermute x3, waiting for transfers between devices, local(): lax.ppermute(parts[k], 'y', shift(Y, k))  4.8 us
    ppermute x3, starting transfers between devices, local(): lax.ppermute(tokens, 'y', shift(Y, by))  4.67 us
    ppermute x3, starting transfers between devices, local(): lax.ppermute(parts[k], 'y', shift(Y, k))  4.65 us
    pallas_call x1, Pallas kernels, update(): pl.pallas_call(update_kernel, out_shape=jax.ShapeDtypeStruct((2, HEAD, HE...  4.16 us
  transfers between devices with their start and end apart: 25, of which 10 were waited for; matrix products, arithmetic and copies ran while one was open for 0% of the time, Pallas kernels for 12%

profile of v6, /device:TPU:1, one launch (start us, length us, event | category | flops | bytes accessed | tf_op | source)
XLA Modules:
  0.0 93.7 jit_solution(14809578446109425804)
XLA Ops:
  0.6 3.6 %collective-permute-start.2 = (bf16[128,256]{1,0:T(8,128)(2,1)}, bf16[128,256]{1,0:T(8,128)(2,1)S(1)}, u32[]{:S(2)}, u32[]{:S(2)}) collective-permute-start(bf16[128,256]{1,0:T(8,128)(2,1)} %refs_0_.1), channel_id=1, source_target_pairs={{0,6},{2,0},{4,2},{6,4},{1,7},{3,1},{5,3},{7,5},{8,14},{10,8},{12,... | collective-permute-start | bytes 196616 | tf_op jit(solution)/shard_map/ppermute | solution.py:395
  4.6 0.7 collective-permute-start
  5.3 1.2 %pack.1 = (bf16[8,128,256]{2,1,0:T(8,128)(2,1)S(1)}, bf16[8,128,256]{2,1,0:T(8,128)(2,1)S(1)}) custom-call(bf16[16,128,256]{2,1,0:T(8,128)(2,1)} %bitcast.12, bf16[256,2048]{1,0:T(8,128)(2,1)} %refs_3_.1), custom_call_target="tpu_custom_call" | custom-call | tf_op jit(solution)/shard_map/pack/pallas_call | solution.py:62
  6.5 2.6 %collective-permute-start.15 = (bf16[8,128,256]{2,1,0:T(8,128)(2,1)S(1)}, bf16[8,128,256]{2,1,0:T(8,128)(2,1)S(1)}, u32[]{:S(2)}, u32[]{:S(2)}) collective-permute-start(bf16[8,128,256]{2,1,0:T(8,128)(2,1)S(1)} %get-tuple-element.25), channel_id=1, source_target_pairs={{0,24},{8,0},{16,8},{24,16},{1,25},{9,1},{17,9},{25,17},{2,26},{10... | collective-permute-start | bytes 1572872 | tf_op jit(solution)/shard_map/ppermute | solution.py:406
  9.1 2.7 %collective-permute-start.13 = (bf16[8,128,256]{2,1,0:T(8,128)(2,1)S(1)}, bf16[8,128,256]{2,1,0:T(8,128)(2,1)S(1)}, u32[]{:S(2)}, u32[]{:S(2)}) collective-permute-start(bf16[8,128,256]{2,1,0:T(8,128)(2,1)S(1)} %get-tuple-element.27), channel_id=1, source_target_pairs={{0,24},{8,0},{16,8},{24,16},{1,25},{9,1},{17,9},{25,17},{2,26},{10... | collective-permute-start | bytes 1572872 | tf_op jit(solution)/shard_map/ppermute | solution.py:398
  11.8 2.4 %collective-permute-start.3 = (bf16[128,256]{1,0:T(8,128)(2,1)}, bf16[128,256]{1,0:T(8,128)(2,1)S(1)}, u32[]{:S(2)}, u32[]{:S(2)}) collective-permute-start(bf16[128,256]{1,0:T(8,128)(2,1)} %refs_0_.1), channel_id=1, source_target_pairs={{0,1},{1,0},{2,3},{3,2},{4,5},{5,4},{6,7},{7,6},{8,9},{9,8},{10,11... | collective-permute-start | bytes 196616 | tf_op jit(solution)/shard_map/ppermute | solution.py:399
  14.2 1.0 %collective-permute-done.3.refs_4_ = bf16[128,256]{1,0:T(8,128)(2,1)S(1)} collective-permute-done((bf16[128,256]{1,0:T(8,128)(2,1)}, bf16[128,256]{1,0:T(8,128)(2,1)S(1)}, u32[]{:S(2)}, u32[]{:S(2)}) %collective-permute-start.3) | collective-permute-done | bytes 65568 | tf_op jit(solution)/shard_map/ppermute | solution.py:399
  15.8 0.7 collective-permute-done.5.refs_6_
  16.5 0.4 collective-permute-done.4.refs_5_
  16.9 5.0 %retain.1 = (f32[4,16,2048]{2,1,0:T(8,128)S(1)}, bf16[4,16,2048]{2,1,0:T(8,128)(2,1)S(1)}, bf16[16,2048]{1,0:T(8,128)(2,1)S(1)}, f32[128,128]{1,0:T(8,128)S(1)}, f32[128,128]{1,0:T(8,128)S(1)}) custom-call(f32[16]{0:T(128)} %constant.9.clone.decays, bf16[128,256]{1,0:T(8,128)(2,1)} %refs_0_.1, bf16[128,256]{1,0:T(8,128)(2,1)S(1)} %collective-permute-done.refs_1_, ...), custom_call_target="tpu_custom_call" | custom-call | tf_op jit(solution)/shard_map/retain/pallas_call | solution.py:179
  22.1 1.4 %collective-permute-done.7.others = bf16[4,16,2048]{2,1,0:T(8,128)(2,1)S(1)} collective-permute-done((bf16[4,16,2048]{2,1,0:T(8,128)(2,1)S(1)}, bf16[4,16,2048]{2,1,0:T(8,128)(2,1)S(1)}, u32[]{:S(2)}, u32[]{:S(2)}) %collective-permute-start.7) | collective-permute-done | bytes 262176 | tf_op jit(solution)/shard_map/ppermute | solution.py:405
  23.6 1.7 %collective-permute-start.8 = (bf16[16,2048]{1,0:T(8,128)(2,1)S(1)}, bf16[16,2048]{1,0:T(8,128)(2,1)S(1)}, u32[]{:S(2)}, u32[]{:S(2)}) collective-permute-start(bf16[16,2048]{1,0:T(8,128)(2,1)S(1)} %get-tuple-element.22), channel_id=1, source_target_pairs={{0,2},{2,4},{4,6},{6,0},{1,3},{3,5},{5,7},{7,1},{8,10},{10,12},{12... | collective-permute-start | bytes 196616 | tf_op jit(solution)/shard_map/ppermute | solution.py:409
  25.2 3.1 %collective-permute-done.8.refs_0_ = bf16[16,2048]{1,0:T(8,128)(2,1)S(1)} collective-permute-done((bf16[16,2048]{1,0:T(8,128)(2,1)S(1)}, bf16[16,2048]{1,0:T(8,128)(2,1)S(1)}, u32[]{:S(2)}, u32[]{:S(2)}) %collective-permute-start.8) | collective-permute-done | bytes 65568 | tf_op jit(solution)/shard_map/ppermute | solution.py:409
  28.4 1.0 %collective-permute-start.9 = (bf16[16,2048]{1,0:T(8,128)(2,1)S(1)}, bf16[16,2048]{1,0:T(8,128)(2,1)S(1)}, u32[]{:S(2)}, u32[]{:S(2)}) collective-permute-start(bf16[16,2048]{1,0:T(8,128)(2,1)S(1)} %get-tuple-element.23), channel_id=1, source_target_pairs={{0,4},{2,6},{4,0},{6,2},{1,5},{3,7},{5,1},{7,3},{8,12},{10,14},{12... | collective-permute-start | bytes 196616 | tf_op jit(solution)/shard_map/ppermute | solution.py:409
  29.4 1.0 %collective-permute-start.16 = (bf16[8,128,256]{2,1,0:T(8,128)(2,1)S(1)}, bf16[8,128,256]{2,1,0:T(8,128)(2,1)}, u32[]{:S(2)}, u32[]{:S(2)}) collective-permute-start(bf16[8,128,256]{2,1,0:T(8,128)(2,1)S(1)} %collective-permute-done.15.refs_6_), channel_id=1, source_target_pairs={{0,1},{1,0},{2,3},{3,2},{4,5},{5,4},{6,7},{7,6},{8,9},{9,8},{10,11... | collective-permute-start | bytes 1572872 | tf_op jit(solution)/shard_map/ppermute | solution.py:415
  30.4 3.1 %collective-permute-start.21 = (bf16[8,128,256]{2,1,0:T(8,128)(2,1)S(1)}, bf16[8,128,256]{2,1,0:T(8,128)(2,1)}, u32[]{:S(2)}, u32[]{:S(2)}) collective-permute-start(bf16[8,128,256]{2,1,0:T(8,128)(2,1)S(1)} %collective-permute-done.13.refs_12_), channel_id=1, source_target_pairs={{0,24},{8,0},{16,8},{24,16},{1,25},{9,1},{17,9},{25,17},{2,26},{10... | collective-permute-start | bytes 1572872 | tf_op jit(solution)/shard_map/ppermute | solution.py:413
  33.5 2.0 %collective-permute-start.10 = (bf16[16,2048]{1,0:T(8,128)(2,1)S(1)}, bf16[16,2048]{1,0:T(8,128)(2,1)S(1)}, u32[]{:S(2)}, u32[]{:S(2)}) collective-permute-start(bf16[16,2048]{1,0:T(8,128)(2,1)S(1)} %get-tuple-element.24), channel_id=1, source_target_pairs={{0,6},{2,0},{4,2},{6,4},{1,7},{3,1},{5,3},{7,5},{8,14},{10,8},{12,... | collective-permute-start | bytes 196616 | tf_op jit(solution)/shard_map/ppermute | solution.py:409
  35.5 1.7 %collective-permute-done.10.refs_2_ = bf16[16,2048]{1,0:T(8,128)(2,1)S(1)} collective-permute-done((bf16[16,2048]{1,0:T(8,128)(2,1)S(1)}, bf16[16,2048]{1,0:T(8,128)(2,1)S(1)}, u32[]{:S(2)}, u32[]{:S(2)}) %collective-permute-start.10) | collective-permute-done | bytes 65568 | tf_op jit(solution)/shard_map/ppermute | solution.py:409
  37.2 0.8 middle.1
  38.0 8.2 %all-to-all-start = ((bf16[8,16,2048]{2,1,0:T(8,128)(2,1)}), bf16[8,16,2048]{2,1,0:T(8,128)(2,1)S(1)}, u32[]{:S(2)}, u32[]{:S(2)}) async-start(bf16[8,16,2048]{2,1,0:T(8,128)(2,1)} %middle.1), calls=%async_computation | async-start | bytes 1048576 | tf_op jit(solution)/shard_map/all_to_all | solution.py:387
  46.2 3.5 %collective-permute-start.12 = (bf16[8,128,256]{2,1,0:T(8,128)(2,1)S(1)}, bf16[8,128,256]{2,1,0:T(8,128)(2,1)S(1)}, u32[]{:S(2)}, u32[]{:S(2)}) collective-permute-start(bf16[8,128,256]{2,1,0:T(8,128)(2,1)S(1)} %collective-permute-done.11.refs_4_), channel_id=1, source_target_pairs={{0,1},{1,0},{2,3},{3,2},{4,5},{5,4},{6,7},{7,6},{8,9},{9,8},{10,11... | collective-permute-start | bytes 1572872 | tf_op jit(solution)/shard_map/ppermute | solution.py:414
  49.8 0.4 collective-permute-start.14
  50.2 0.6 collective-permute-done.19.refs_8_
  50.9 1.3 %collective-permute-start.20 = (bf16[8,128,256]{2,1,0:T(8,128)(2,1)}, bf16[8,128,256]{2,1,0:T(8,128)(2,1)S(1)}, u32[]{:S(2)}, u32[]{:S(2)}) collective-permute-start(bf16[8,128,256]{2,1,0:T(8,128)(2,1)} %collective-permute-done.19.refs_8_), channel_id=1, source_target_pairs={{0,1},{1,0},{2,3},{3,2},{4,5},{5,4},{6,7},{7,6},{8,9},{9,8},{10,11... | collective-permute-start | bytes 1572872 | tf_op jit(solution)/shard_map/ppermute | solution.py:418
  52.2 0.6 collective-permute-done.14.refs_13_
  53.1 0.8 copy-done.3
  53.9 6.6 %all-to-all-done.refs_0_ = bf16[8,16,2048]{2,1,0:T(8,128)(2,1)S(1)} async-done(((bf16[8,16,2048]{2,1,0:T(8,128)(2,1)}), bf16[8,16,2048]{2,1,0:T(8,128)(2,1)S(1)}, u32[]{:S(2)}, u32[]{:S(2)}) %all-to-all-start) | async-done | bytes 524320 | tf_op jit(solution)/shard_map/all_to_all | solution.py:387
  60.5 5.5 %mixer.1 = bf16[8,8,16,256]{3,2,1,0:T(8,128)(2,1)} custom-call(bf16[8,16,2048]{2,1,0:T(8,128)(2,1)S(1)} %all-to-all-done.refs_0_, bf16[16,128]{1,0:T(8,128)(2,1)} %bitcast.17, bf16[16,128,256]{2,1,0:T(8,128)(2,1)} %bitcast.13, bf16[256,2048]{1,0:T(8,128)(2,1)} %refs_3_.1, bf16[8,128,256]{2,1,0:T(8,128)(2,1)S(1)} %collective-permute-done.11.refs_4_, ...), custom_call_target="tpu_custom_call" | custom-call | tf_op jit(solution)/shard_map/mixer/pallas_call | solution.py:363
  66.0 9.3 %all-to-all-start.1 = ((bf16[64,16,256]{2,1,0:T(8,128)(2,1)}), bf16[64,16,256]{2,1,0:T(8,128)(2,1)S(1)}, u32[]{:S(2)}, u32[]{:S(2)}) async-start(bf16[64,16,256]{2,1,0:T(8,128)(2,1)} %bitcast.5), calls=%async_computation.1 | async-start | bytes 1048576 | tf_op jit(solution)/shard_map/all_to_all | solution.py:387
  75.3 4.2 %update.1 = f32[2,64,64,128]{3,2,1,0:T(8,128)} custom-call(f32[16]{0:T(128)} %constant.9.clone.decays, f32[128,128]{1,0:T(8,128)S(1)} %get-tuple-element.32.keys, f32[128,128]{1,0:T(8,128)S(1)} %get-tuple-element.33.values, f32[2,64,64,128]{3,2,1,0:T(8,128)} %bitcast.11), custom_call_target="tpu_custom_call" | custom-call | tf_op jit(solution)/shard_map/update/pallas_call | solution.py:241
  79.5 13.5 %all-to-all-done.1 = bf16[64,16,256]{2,1,0:T(8,128)(2,1)S(1)} async-done(((bf16[64,16,256]{2,1,0:T(8,128)(2,1)}), bf16[64,16,256]{2,1,0:T(8,128)(2,1)S(1)}, u32[]{:S(2)}, u32[]{:S(2)}) %all-to-all-start.1) | async-done | bytes 524320 | tf_op jit(solution)/shard_map/all_to_all | solution.py:387
  93.0 0.7 bitcast_reduce_fusion
  (33 shorter events, 1.8 us)
Async XLA Ops:
  0.6 8.5 %collective-permute-start.2 = (bf16[128,256]{1,0:T(8,128)(2,1)}, bf16[128,256]{1,0:T(8,128)(2,1)S(1)}, u32[]{:S(2)}, u32[]{:S(2)}) collective-permute-start(bf16[128,256]{1,0:T(8,128)(2,1)} %refs_0_.1), channel_id=1, source_target_pairs={{0,6},{2,0},{4,2},{6,4},{1,7},{3,1},{5,3},{7,5},{8,14},{10,8},{12,... | collective-permute-start | bytes 196616 | tf_op jit(solution)/shard_map/ppermute | solution.py:395
  4.3 7.5 %collective-permute-start.1 = (bf16[128,256]{1,0:T(8,128)(2,1)}, bf16[128,256]{1,0:T(8,128)(2,1)S(1)}, u32[]{:S(2)}, u32[]{:S(2)}) collective-permute-start(bf16[128,256]{1,0:T(8,128)(2,1)} %refs_0_.1), channel_id=1, source_target_pairs={{0,4},{2,6},{4,0},{6,2},{1,5},{3,7},{5,1},{7,3},{8,12},{10,14},{12... | collective-permute-start | bytes 196616 | tf_op jit(solution)/shard_map/ppermute | solution.py:395
  4.6 9.5 %collective-permute-start = (bf16[128,256]{1,0:T(8,128)(2,1)}, bf16[128,256]{1,0:T(8,128)(2,1)S(1)}, u32[]{:S(2)}, u32[]{:S(2)}) collective-permute-start(bf16[128,256]{1,0:T(8,128)(2,1)} %refs_0_.1), channel_id=1, source_target_pairs={{0,2},{2,4},{4,6},{6,0},{1,3},{3,5},{5,7},{7,1},{8,10},{10,12},{12... | collective-permute-start | bytes 196616 | tf_op jit(solution)/shard_map/ppermute | solution.py:395
  6.5 22.8 %collective-permute-start.15 = (bf16[8,128,256]{2,1,0:T(8,128)(2,1)S(1)}, bf16[8,128,256]{2,1,0:T(8,128)(2,1)S(1)}, u32[]{:S(2)}, u32[]{:S(2)}) collective-permute-start(bf16[8,128,256]{2,1,0:T(8,128)(2,1)S(1)} %get-tuple-element.25), channel_id=1, source_target_pairs={{0,24},{8,0},{16,8},{24,16},{1,25},{9,1},{17,9},{25,17},{2,26},{10... | collective-permute-start | bytes 1572872 | tf_op jit(solution)/shard_map/ppermute | solution.py:406
  9.1 21.3 %collective-permute-start.11 = (bf16[8,128,256]{2,1,0:T(8,128)(2,1)S(1)}, bf16[8,128,256]{2,1,0:T(8,128)(2,1)S(1)}, u32[]{:S(2)}, u32[]{:S(2)}) collective-permute-start(bf16[8,128,256]{2,1,0:T(8,128)(2,1)S(1)} %get-tuple-element.25), channel_id=1, source_target_pairs={{0,8},{8,16},{16,24},{24,0},{1,9},{9,17},{17,25},{25,1},{2,10},{10... | collective-permute-start | bytes 1572872 | tf_op jit(solution)/shard_map/ppermute | solution.py:397
  9.1 21.3 %collective-permute-start.13 = (bf16[8,128,256]{2,1,0:T(8,128)(2,1)S(1)}, bf16[8,128,256]{2,1,0:T(8,128)(2,1)S(1)}, u32[]{:S(2)}, u32[]{:S(2)}) collective-permute-start(bf16[8,128,256]{2,1,0:T(8,128)(2,1)S(1)} %get-tuple-element.27), channel_id=1, source_target_pairs={{0,24},{8,0},{16,8},{24,16},{1,25},{9,1},{17,9},{25,17},{2,26},{10... | collective-permute-start | bytes 1572872 | tf_op jit(solution)/shard_map/ppermute | solution.py:398
  11.8 3.5 %collective-permute-start.3 = (bf16[128,256]{1,0:T(8,128)(2,1)}, bf16[128,256]{1,0:T(8,128)(2,1)S(1)}, u32[]{:S(2)}, u32[]{:S(2)}) collective-permute-start(bf16[128,256]{1,0:T(8,128)(2,1)} %refs_0_.1), channel_id=1, source_target_pairs={{0,1},{1,0},{2,3},{3,2},{4,5},{5,4},{6,7},{7,6},{8,9},{9,8},{10,11... | collective-permute-start | bytes 196616 | tf_op jit(solution)/shard_map/ppermute | solution.py:399
  14.1 1.5 %collective-permute-start.6 = (bf16[128,256]{1,0:T(8,128)(2,1)S(1)}, bf16[128,256]{1,0:T(8,128)(2,1)S(1)}, u32[]{:S(2)}, u32[]{:S(2)}) collective-permute-start(bf16[128,256]{1,0:T(8,128)(2,1)S(1)} %collective-permute-done.2.refs_3_), channel_id=1, source_target_pairs={{0,1},{1,0},{2,3},{3,2},{4,5},{5,4},{6,7},{7,6},{8,9},{9,8},{10,11... | collective-permute-start | bytes 196616 | tf_op jit(solution)/shard_map/ppermute | solution.py:400
  15.2 1.3 %collective-permute-start.5 = (bf16[128,256]{1,0:T(8,128)(2,1)S(1)}, bf16[128,256]{1,0:T(8,128)(2,1)S(1)}, u32[]{:S(2)}, u32[]{:S(2)}) collective-permute-start(bf16[128,256]{1,0:T(8,128)(2,1)S(1)} %collective-permute-done.1.refs_2_), channel_id=1, source_target_pairs={{0,1},{1,0},{2,3},{3,2},{4,5},{5,4},{6,7},{7,6},{8,9},{9,8},{10,11... | collective-permute-start | bytes 196616 | tf_op jit(solution)/shard_map/ppermute | solution.py:400
  15.6 1.3 %collective-permute-start.4 = (bf16[128,256]{1,0:T(8,128)(2,1)S(1)}, bf16[128,256]{1,0:T(8,128)(2,1)S(1)}, u32[]{:S(2)}, u32[]{:S(2)}) collective-permute-start(bf16[128,256]{1,0:T(8,128)(2,1)S(1)} %collective-permute-done.refs_1_), channel_id=1, source_target_pairs={{0,1},{1,0},{2,3},{3,2},{4,5},{5,4},{6,7},{7,6},{8,9},{9,8},{10,11... | collective-permute-start | bytes 196616 | tf_op jit(solution)/shard_map/ppermute | solution.py:400
  21.9 1.6 %collective-permute-start.7 = (bf16[4,16,2048]{2,1,0:T(8,128)(2,1)S(1)}, bf16[4,16,2048]{2,1,0:T(8,128)(2,1)S(1)}, u32[]{:S(2)}, u32[]{:S(2)}) collective-permute-start(bf16[4,16,2048]{2,1,0:T(8,128)(2,1)S(1)} %get-tuple-element.20), channel_id=1, source_target_pairs={{0,1},{1,0},{2,3},{3,2},{4,5},{5,4},{6,7},{7,6},{8,9},{9,8},{10,11... | collective-permute-start | bytes 786440 | tf_op jit(solution)/shard_map/ppermute | solution.py:405
  23.6 4.8 %collective-permute-start.8 = (bf16[16,2048]{1,0:T(8,128)(2,1)S(1)}, bf16[16,2048]{1,0:T(8,128)(2,1)S(1)}, u32[]{:S(2)}, u32[]{:S(2)}) collective-permute-start(bf16[16,2048]{1,0:T(8,128)(2,1)S(1)} %get-tuple-element.22), channel_id=1, source_target_pairs={{0,2},{2,4},{4,6},{6,0},{1,3},{3,5},{5,7},{7,1},{8,10},{10,12},{12... | collective-permute-start | bytes 196616 | tf_op jit(solution)/shard_map/ppermute | solution.py:409
  25.2 24.5 %collective-permute-start.17 = (bf16[8,128,256]{2,1,0:T(8,128)(2,1)S(1)}, bf16[8,128,256]{2,1,0:T(8,128)(2,1)}, u32[]{:S(2)}, u32[]{:S(2)}) collective-permute-start(bf16[8,128,256]{2,1,0:T(8,128)(2,1)S(1)} %get-tuple-element.27), channel_id=1, source_target_pairs={{0,8},{8,16},{16,24},{24,0},{1,9},{9,17},{17,25},{25,1},{2,10},{10... | collective-permute-start | bytes 1572872 | tf_op jit(solution)/shard_map/ppermute | solution.py:407
  28.4 5.1 %collective-permute-start.9 = (bf16[16,2048]{1,0:T(8,128)(2,1)S(1)}, bf16[16,2048]{1,0:T(8,128)(2,1)S(1)}, u32[]{:S(2)}, u32[]{:S(2)}) collective-permute-start(bf16[16,2048]{1,0:T(8,128)(2,1)S(1)} %get-tuple-element.23), channel_id=1, source_target_pairs={{0,4},{2,6},{4,0},{6,2},{1,5},{3,7},{5,1},{7,3},{8,12},{10,14},{12... | collective-permute-start | bytes 196616 | tf_op jit(solution)/shard_map/ppermute | solution.py:409
  29.4 31.2 %copy-start = (bf16[8,128,256]{2,1,0:T(8,128)(2,1)}, bf16[8,128,256]{2,1,0:T(8,128)(2,1)S(1)}, u32[]{:S(2)}) copy-start(bf16[8,128,256]{2,1,0:T(8,128)(2,1)S(1)} %collective-permute-done.15.refs_6_) | copy-start | bytes 1572868
  29.4 20.5 %collective-permute-start.16 = (bf16[8,128,256]{2,1,0:T(8,128)(2,1)S(1)}, bf16[8,128,256]{2,1,0:T(8,128)(2,1)}, u32[]{:S(2)}, u32[]{:S(2)}) collective-permute-start(bf16[8,128,256]{2,1,0:T(8,128)(2,1)S(1)} %collective-permute-done.15.refs_6_), channel_id=1, source_target_pairs={{0,1},{1,0},{2,3},{3,2},{4,5},{5,4},{6,7},{7,6},{8,9},{9,8},{10,11... | collective-permute-start | bytes 1572872 | tf_op jit(solution)/shard_map/ppermute | solution.py:415
  30.4 20.5 %collective-permute-start.19 = (bf16[8,128,256]{2,1,0:T(8,128)(2,1)S(1)}, bf16[8,128,256]{2,1,0:T(8,128)(2,1)}, u32[]{:S(2)}, u32[]{:S(2)}) collective-permute-start(bf16[8,128,256]{2,1,0:T(8,128)(2,1)S(1)} %collective-permute-done.11.refs_4_), channel_id=1, source_target_pairs={{0,8},{8,16},{16,24},{24,0},{1,9},{9,17},{17,25},{25,1},{2,10},{10... | collective-permute-start | bytes 1572872 | tf_op jit(solution)/shard_map/ppermute | solution.py:412
  30.4 21.8 %collective-permute-start.21 = (bf16[8,128,256]{2,1,0:T(8,128)(2,1)S(1)}, bf16[8,128,256]{2,1,0:T(8,128)(2,1)}, u32[]{:S(2)}, u32[]{:S(2)}) collective-permute-start(bf16[8,128,256]{2,1,0:T(8,128)(2,1)S(1)} %collective-permute-done.13.refs_12_), channel_id=1, source_target_pairs={{0,24},{8,0},{16,8},{24,16},{1,25},{9,1},{17,9},{25,17},{2,26},{10... | collective-permute-start | bytes 1572872 | tf_op jit(solution)/shard_map/ppermute | solution.py:413
  33.5 3.7 %collective-permute-start.10 = (bf16[16,2048]{1,0:T(8,128)(2,1)S(1)}, bf16[16,2048]{1,0:T(8,128)(2,1)S(1)}, u32[]{:S(2)}, u32[]{:S(2)}) collective-permute-start(bf16[16,2048]{1,0:T(8,128)(2,1)S(1)} %get-tuple-element.24), channel_id=1, source_target_pairs={{0,6},{2,0},{4,2},{6,4},{1,7},{3,1},{5,3},{7,5},{8,14},{10,8},{12,... | collective-permute-start | bytes 196616 | tf_op jit(solution)/shard_map/ppermute | solution.py:409
  38.0 22.5 %all-to-all-start = ((bf16[8,16,2048]{2,1,0:T(8,128)(2,1)}), bf16[8,16,2048]{2,1,0:T(8,128)(2,1)S(1)}, u32[]{:S(2)}, u32[]{:S(2)}) async-start(bf16[8,16,2048]{2,1,0:T(8,128)(2,1)} %middle.1), calls=%async_computation | async-start | bytes 1048576 | tf_op jit(solution)/shard_map/all_to_all | solution.py:387
  46.2 6.0 %collective-permute-start.12 = (bf16[8,128,256]{2,1,0:T(8,128)(2,1)S(1)}, bf16[8,128,256]{2,1,0:T(8,128)(2,1)S(1)}, u32[]{:S(2)}, u32[]{:S(2)}) collective-permute-start(bf16[8,128,256]{2,1,0:T(8,128)(2,1)S(1)} %collective-permute-done.11.refs_4_), channel_id=1, source_target_pairs={{0,1},{1,0},{2,3},{3,2},{4,5},{5,4},{6,7},{7,6},{8,9},{9,8},{10,11... | collective-permute-start | bytes 1572872 | tf_op jit(solution)/shard_map/ppermute | solution.py:414
  49.7 2.4 %collective-permute-start.18 = (bf16[8,128,256]{2,1,0:T(8,128)(2,1)}, bf16[8,128,256]{2,1,0:T(8,128)(2,1)S(1)}, u32[]{:S(2)}, u32[]{:S(2)}) collective-permute-start(bf16[8,128,256]{2,1,0:T(8,128)(2,1)} %collective-permute-done.17.refs_10_), channel_id=1, source_target_pairs={{0,1},{1,0},{2,3},{3,2},{4,5},{5,4},{6,7},{7,6},{8,9},{9,8},{10,11... | collective-permute-start | bytes 1572872 | tf_op jit(solution)/shard_map/ppermute | solution.py:415
  49.8 2.9 %collective-permute-start.14 = (bf16[8,128,256]{2,1,0:T(8,128)(2,1)S(1)}, bf16[8,128,256]{2,1,0:T(8,128)(2,1)S(1)}, u32[]{:S(2)}, u32[]{:S(2)}) collective-permute-start(bf16[8,128,256]{2,1,0:T(8,128)(2,1)S(1)} %collective-permute-done.13.refs_12_), channel_id=1, source_target_pairs={{0,1},{1,0},{2,3},{3,2},{4,5},{5,4},{6,7},{7,6},{8,9},{9,8},{10,11... | collective-permute-start | bytes 1572872 | tf_op jit(solution)/shard_map/ppermute | solution.py:414
  50.9 9.7 %collective-permute-start.20 = (bf16[8,128,256]{2,1,0:T(8,128)(2,1)}, bf16[8,128,256]{2,1,0:T(8,128)(2,1)S(1)}, u32[]{:S(2)}, u32[]{:S(2)}) collective-permute-start(bf16[8,128,256]{2,1,0:T(8,128)(2,1)} %collective-permute-done.19.refs_8_), channel_id=1, source_target_pairs={{0,1},{1,0},{2,3},{3,2},{4,5},{5,4},{6,7},{7,6},{8,9},{9,8},{10,11... | collective-permute-start | bytes 1572872 | tf_op jit(solution)/shard_map/ppermute | solution.py:418
  52.1 8.4 %collective-permute-start.22 = (bf16[8,128,256]{2,1,0:T(8,128)(2,1)}, bf16[8,128,256]{2,1,0:T(8,128)(2,1)S(1)}, u32[]{:S(2)}, u32[]{:S(2)}) collective-permute-start(bf16[8,128,256]{2,1,0:T(8,128)(2,1)} %collective-permute-done.21.refs_14_), channel_id=1, source_target_pairs={{0,1},{1,0},{2,3},{3,2},{4,5},{5,4},{6,7},{7,6},{8,9},{9,8},{10,11... | collective-permute-start | bytes 1572872 | tf_op jit(solution)/shard_map/ppermute | solution.py:418
  52.1 0.8 copy-start.1
  52.2 1.0 %copy-start.2 = (bf16[8,128,256]{2,1,0:T(8,128)(2,1)}, bf16[8,128,256]{2,1,0:T(8,128)(2,1)S(1)}, u32[]{:S(2)}) copy-start(bf16[8,128,256]{2,1,0:T(8,128)(2,1)S(1)} %collective-permute-done.18.refs_11_) | copy-start | bytes 1572868
  53.1 0.8 copy-start.3
  66.0 27.0 %all-to-all-start.1 = ((bf16[64,16,256]{2,1,0:T(8,128)(2,1)}), bf16[64,16,256]{2,1,0:T(8,128)(2,1)S(1)}, u32[]{:S(2)}, u32[]{:S(2)}) async-start(bf16[64,16,256]{2,1,0:T(8,128)(2,1)} %bitcast.5), calls=%async_computation.1 | async-start | bytes 1048576 | tf_op jit(solution)/shard_map/all_to_all | solution.py:387
